TPU v7x, 256 devices: a 4x2x16 block of a 4x16x16 slice. The times are simulated.
256 devices in a mesh: grp: 2 (over y), sp: 16 (over z), fs: 4 (over x), tp: 2 (over core).
Axes of the slice: x: 4, y: 2, z: 16, core: 2. Of those that a mesh axis runs over, the one named last changes fastest.
The devices are a block of a 4x16x16 slice.
Arguments:
- inputs: bfloat16 [16, 2048, 2048], P(('grp', 'fs'), 'sp', 'tp'), parts along dimension 0, may hold values from -20 to 20
- input_norm_gain: bfloat16 [2048], replicated, may hold values from 0.099609375 to 1.8984375
- softmax_query_matrix: bfloat16 [2048, 1024], P('fs', 'tp'), may hold values from -0.088388348 to 0.088388348
- softmax_key_matrix: bfloat16 [2048, 1024], P('fs', 'tp'), may hold values from -3.557631 to 3.557631
- softmax_value_matrix: bfloat16 [2048, 1024], P('fs', 'tp'), may hold values from -0.125 to 0.125
- running_forget_gate: float32 [16, 2048, 16], P(('grp', 'fs'), None, 'tp'), parts along dimension 0, may hold values from -105 to 0, as said below
- receptance_weight: bfloat16 [2048, 1024], P('fs', 'tp'), may hold values from -0.125 to 0.125
- linear_key_weight: bfloat16 [2048, 1024], P('fs', 'tp'), may hold values from -0.125 to 0.125
- linear_value_weight: bfloat16 [2048, 1024], P('fs', 'tp'), may hold values from -0.125 to 0.125
- decay_lower_map: bfloat16 [2048, 128], replicated, may hold values from -0.125 to 0.125
- decay_upper_map: bfloat16 [128, 1024], replicated, may hold values from -1 to 1
- decay_offset_base: float32 [1024], replicated, may hold values from -12 to -2
- decay_extra_log: float32 [16, 2048, 16], P(('grp', 'fs'), 'sp', 'tp'), parts along dimension 0, may hold values from -1 to 0
- rate_lower_map: bfloat16 [2048, 128], replicated, may hold values from -0.125 to 0.125
- rate_upper_map: bfloat16 [128, 1024], replicated, may hold values from -1 to 1
- rate_offset_base: float32 [1024], replicated, may hold values from -2 to 2
- linear_head_gain: bfloat16 [1024], replicated, may hold values from 0.099609375 to 1.8984375
- starting_state: float32 [16, 16, 64, 64], P(('grp', 'fs'), 'tp'), parts along dimension 0, may hold values from -144.81547 to 144.81547
- softmax_output_weight: bfloat16 [2048, 1024], P(None, 'tp'), may hold values from -1.5 to 1.5
- linear_output_weight: bfloat16 [2048, 1024], P(None, 'tp'), may hold values from -0.125 to 0.125
Outputs:
- mixed: bfloat16 [16, 2048, 2048], P(('grp', 'fs', 'tp'), 'sp'), parts along dimension 0
There are 2 independent parts, one for each index of `grp`. A program takes and returns all parts, laid end to end along the dimension named above; an argument that names none is the same for every part. Nothing has to cross between parts.
Inputs may be any that keep to these rules, and one draw needn't show every extreme that they name: `running_forget_gate`: never rising along positions.
All inputs are finite; a program needn't handle non-finite values.
Results may differ from a plain program's by a relative error of at most 0.0095.
The roundings to bfloat16 on the way count: a program that leaves them out, or rounds other values in their place, can miss the bound.
Values may be sent and summed in bfloat16 or wider, within the bound.
No kernel may reach another device: no remote copies, remote signals or barrier semaphores. Data moves between devices by JAX's collectives and lax.ppermute only.
A program may use at most 128 MiB of HBM per device.

v0:
```python
import jax
import jax.numpy as jnp
from jax import lax
from jax.sharding import PartitionSpec as P

HEAD_CHANNELS = 64


span_len = 16
out_dims = (((2,), (1,)), ((), ()))


def from_everyone(x, axis):
    copies = jnp.broadcast_to(x, (lax.axis_size(axis), *x.shape))
    return lax.all_to_all(copies, axis, split_axis=0, concat_axis=0, tiled=True)


def laid_out(pieces, dim):
    lengths = list(pieces.shape[1:])
    lengths[dim] *= pieces.shape[0]
    return jnp.moveaxis(pieces, 0, dim).reshape(lengths)


def collect(x, axis, dim):
    pieces = from_everyone(x, axis)
    return laid_out(pieces, dim)


def sent_together(arrays, axis, dim, along):
    ends, at = ([], 0)
    for a in arrays[:-1]:
        at += a.shape[along]
        ends.append(at)
    both = jnp.concatenate(arrays, axis=along)
    return tuple(jnp.split(lax.all_gather(both, axis, axis=dim, tiled=True), ends, axis=along))


def prefix(x, axis, join, neutral):
    place = lax.axis_index(axis)
    gathered = jax.tree.map(
        lambda a, kind: lax.all_gather(a.astype(kind), axis), x, (jnp.bfloat16, jnp.bfloat16)
    )
    state = jax.tree.map(lambda a, e: jnp.zeros_like(a) + jnp.asarray(e, a.dtype), x, neutral)

    def one(lap, state):
        return join(
            state,
            jax.tree.map(
                lambda a, own: lax.dynamic_index_in_dim(a, lap, 0, False).astype(own.dtype),
                gathered,
                x,
            ),
        )

    return lax.fori_loop(0, place, one, state)


def in_blocks(x, dim, size):
    lengths = x.shape
    pieces = x.reshape(*lengths[:dim], size, lengths[dim] // size, *lengths[dim + 1 :])
    return jnp.moveaxis(pieces, dim, 0)


def summed_on_arrival(x, axis, dim):
    size = lax.axis_size(axis)
    pieces = lax.all_to_all(in_blocks(x, dim, size), axis, 0, 0, tiled=True)
    return jnp.sum(pieces.astype(jnp.float32), axis=0)


def to_stored(values):
    return lax.optimization_barrier(values.astype(jnp.bfloat16)).astype(jnp.float32)


def key_block(length):
    block_size = min(length, 512)
    while length % block_size:
        block_size = block_size - 1
    return block_size


def attend_factory(queries, query_gates, running_forget_gate, first_query, last_query):
    seq_count, tok_count, head_count, head_width = queries.shape
    scaling = head_width ** (-0.5)
    query_place = first_query + jnp.arange(tok_count)

    def attend(carried, pieces, start):
        key_rows, value_rows = pieces
        length = key_rows.shape[1]
        block_size = key_block(length)

        def sweep(running):

            def one_block(block_index, running):
                top_prev, total_prev, accum_prev = running
                begin = block_index * block_size
                key_part = lax.dynamic_slice_in_dim(
                    key_rows, block_index * block_size, block_size, 1
                )
                value_part = lax.dynamic_slice_in_dim(
                    value_rows, block_index * block_size, block_size, 1
                )
                key_part = key_part.reshape(seq_count, block_size, head_count, head_width)
                value_part = value_part.reshape(seq_count, block_size, head_count, head_width)
                key_gates = lax.dynamic_slice_in_dim(
                    running_forget_gate, begin, block_size, 1
                ).transpose(0, 2, 1)
                score = (
                    jnp.einsum(
                        "sqhd,skhd->shqk", queries, key_part, preferred_element_type=jnp.float32
                    )
                    * scaling
                )
                score = score + query_gates[:, :, :, None] - key_gates[:, :, None, :]
                live = query_place[:, None] >= (begin + jnp.arange(block_size))[None, :]
                peak = jnp.maximum(top_prev, jnp.max(jnp.where(live, score, -1e30), axis=-1))
                weights = jnp.where(live, jnp.exp(score - peak[..., None]), 0.0)
                fading = jnp.exp(top_prev - peak)
                total_next = total_prev * fading + jnp.sum(weights, axis=-1)
                accum_next = accum_prev * fading[..., None] + jnp.einsum(
                    "shqk,skhd->shqd",
                    weights.astype(jnp.bfloat16),
                    value_part,
                    preferred_element_type=jnp.float32,
                )
                return (peak, total_next, accum_next)

            return lax.fori_loop(0, length // block_size, one_block, running)

        needed = jnp.logical_and(start >= 0, start <= last_query)
        return lax.cond(needed, sweep, lambda running: running, carried)

    return attend


def span_pass(start_state, receptance, decay_logged, lin_keys, lin_values, zeta, beta, want_out):
    seq_count, tok_count, head_count, head_width = lin_keys.shape
    spans = tok_count // span_len

    def arrange(values):
        return values.reshape(seq_count, spans, span_len, head_count, values.shape[-1]).transpose(
            1, 0, 3, 2, 4
        )

    strict = jnp.tril(jnp.ones((span_len, span_len), jnp.float32), -1)
    upto = jnp.tril(jnp.ones((span_len, span_len), jnp.float32), 0)
    identity = jnp.eye(span_len, dtype=jnp.float32)

    def pair_mix(left, right, mask):
        return jnp.einsum("shtn,shjn->shtj", left, right) * mask

    def apply_mix(matrix, values):
        return jnp.einsum("shtj,shjv->shtv", matrix, values)

    def advance(carried, items):
        rec_span, decay_span, key_span, value_span, zeta_span, beta_span = items
        cumulative = jnp.cumsum(decay_span, axis=2)
        previous = cumulative - decay_span
        rising = jnp.exp(-cumulative)
        zeta_faded = zeta_span * jnp.exp(previous)
        beta_risen = beta_span * rising
        key_risen = key_span * rising
        within = pair_mix(zeta_faded, beta_risen, strict)
        inverse = identity + within
        power = within
        for repeat in range(3):
            power = apply_mix(power, power)
            inverse = inverse + apply_mix(inverse, power)
        right_side = jnp.einsum("shtn,shvn->shtv", zeta_faded, carried) + apply_mix(
            pair_mix(zeta_faded, key_risen, strict), value_span
        )
        pulled = apply_mix(inverse, right_side)
        ending = jnp.exp(cumulative[:, :, -1:, :])
        next_state = (
            carried * ending
            + jnp.einsum("shjv,shjn->shvn", pulled, beta_risen * ending)
            + jnp.einsum("shjv,shjn->shvn", value_span, key_risen * ending)
        )
        if want_out:
            rec_faded = rec_span * jnp.exp(cumulative)
            outputs = (
                jnp.einsum("shtn,shvn->shtv", rec_faded, carried)
                + apply_mix(pair_mix(rec_faded, beta_risen, upto), pulled)
                + apply_mix(pair_mix(rec_faded, key_risen, upto), value_span)
            )
            return (next_state, outputs)
        return (next_state, None)

    items = tuple(
        (arrange(values) for values in (receptance, decay_logged, lin_keys, lin_values, zeta, beta))
    )
    final_state, outputs = lax.scan(advance, start_state, items)
    if want_out:
        outputs = outputs.transpose(1, 0, 3, 2, 4).reshape(
            seq_count, tok_count, head_count, outputs.shape[-1]
        )
    return (final_state, outputs)


def compose(earlier, later):
    return (
        jnp.einsum("shij,shjk->shik", earlier[0], later[0]),
        jnp.einsum("shij,shjk->shik", earlier[1], later[0]) + later[1],
    )


def per_device(
    inputs,
    input_norm_gain,
    softmax_query_matrix,
    softmax_key_matrix,
    softmax_value_matrix,
    running_forget_gate,
    receptance_weight,
    linear_key_weight,
    linear_value_weight,
    decay_lower_map,
    decay_upper_map,
    decay_offset_base,
    decay_extra_log,
    rate_lower_map,
    rate_upper_map,
    rate_offset_base,
    linear_head_gain,
    starting_state,
    softmax_output_weight,
    linear_output_weight,
):
    whole = collect(inputs, "tp", 2)
    seq_count, tok_count, model_width = whole.shape
    values_in = whole.astype(jnp.float32)
    scaling = lax.rsqrt(jnp.mean(values_in * values_in, axis=-1, keepdims=True) + 1e-06)
    normed = (values_in * scaling * input_norm_gain.astype(jnp.float32)).astype(jnp.bfloat16)
    flat_rows = normed.reshape(seq_count * tok_count, model_width)
    w_query, w_key, w_value, w_recept, w_lkey, w_lvalue = sent_together(
        (
            softmax_query_matrix,
            softmax_key_matrix,
            softmax_value_matrix,
            receptance_weight,
            linear_key_weight,
            linear_value_weight,
        ),
        "fs",
        0,
        1,
    )

    def project(weight):
        return jnp.dot(flat_rows, weight, preferred_element_type=jnp.float32)

    fox_heads = w_query.shape[1] // HEAD_CHANNELS
    queries = (
        project(w_query)
        .astype(jnp.bfloat16)
        .reshape(seq_count, tok_count, fox_heads, HEAD_CHANNELS)
    )
    key_flat = (
        project(w_key).astype(jnp.bfloat16).reshape(seq_count, tok_count, fox_heads * HEAD_CHANNELS)
    )
    value_flat = (
        project(w_value)
        .astype(jnp.bfloat16)
        .reshape(seq_count, tok_count, fox_heads * HEAD_CHANNELS)
    )
    position = lax.axis_index("sp")
    first_query = position * tok_count
    last_query = first_query + tok_count - 1
    query_gates = lax.dynamic_slice_in_dim(
        running_forget_gate, first_query, tok_count, 1
    ).transpose(0, 2, 1)
    attend = attend_factory(queries, query_gates, running_forget_gate, first_query, last_query)
    empty = (
        jnp.full((seq_count, fox_heads, tok_count), -1e30, jnp.float32),
        jnp.zeros((seq_count, fox_heads, tok_count), jnp.float32),
        jnp.zeros((seq_count, fox_heads, tok_count, HEAD_CHANNELS), jnp.float32),
    )
    running = attend(empty, sent_together((key_flat, value_flat), "sp", 1, 0), jnp.int32(0))
    top_final, total_final, accum_final = running
    fox_out = (accum_final / total_final[..., None]).astype(jnp.bfloat16)
    fox_out = fox_out.transpose(0, 2, 1, 3).reshape(seq_count, tok_count, fox_heads * HEAD_CHANNELS)
    lin_cols = w_recept.shape[1]
    lin_heads = lin_cols // HEAD_CHANNELS
    col_start = lax.axis_index("tp") * lin_cols

    def own_columns(table, axis):
        return lax.dynamic_slice_in_dim(table, col_start, lin_cols, axis)

    receptance = to_stored(project(w_recept)).reshape(
        seq_count, tok_count, lin_heads, HEAD_CHANNELS
    )
    lin_keys = to_stored(project(w_lkey)).reshape(seq_count, tok_count, lin_heads, HEAD_CHANNELS)
    lin_values = to_stored(project(w_lvalue)).reshape(
        seq_count, tok_count, lin_heads, HEAD_CHANNELS
    )
    decay_low = jnp.tanh(project(decay_lower_map)).astype(jnp.bfloat16)
    decay_preact = own_columns(decay_offset_base, 0) + jnp.dot(
        decay_low, own_columns(decay_upper_map, 1), preferred_element_type=jnp.float32
    )
    decay_logged = (-jnp.exp(-jax.nn.softplus(-decay_preact) - 0.5)).reshape(
        seq_count, tok_count, lin_heads, HEAD_CHANNELS
    )
    decay_logged = decay_logged + decay_extra_log[..., None]
    rate_low = project(rate_lower_map).astype(jnp.bfloat16)
    rate = jax.nn.sigmoid(
        own_columns(rate_offset_base, 0)
        + jnp.dot(rate_low, own_columns(rate_upper_map, 1), preferred_element_type=jnp.float32)
    )
    rate = rate.reshape(seq_count, tok_count, lin_heads, HEAD_CHANNELS)
    unit = lin_keys * lax.rsqrt(jnp.sum(lin_keys * lin_keys, axis=-1, keepdims=True) + 1e-06)
    zeta = -unit
    beta = unit * rate
    blank = jnp.zeros((seq_count, lin_heads, HEAD_CHANNELS, HEAD_CHANNELS), jnp.float32)
    identity = jnp.broadcast_to(
        jnp.eye(HEAD_CHANNELS, dtype=jnp.float32),
        (seq_count, lin_heads, HEAD_CHANNELS, HEAD_CHANNELS),
    )
    start_rows = jnp.concatenate((blank, identity), axis=2)
    values_wide = jnp.concatenate((lin_values, jnp.zeros_like(lin_values)), axis=3)
    ends, nothing = span_pass(
        start_rows, receptance, decay_logged, lin_keys, values_wide, zeta, beta, False
    )
    offset_map = ends[:, :, :HEAD_CHANNELS]
    carry_map = ends[:, :, HEAD_CHANNELS:]
    prior_map, prior_offset = prefix((carry_map, offset_map), "sp", compose, (identity, blank))
    incoming = jnp.einsum("shij,shjk->shik", starting_state, prior_map) + prior_offset
    final_state, lin_raw = span_pass(
        incoming, receptance, decay_logged, lin_keys, lin_values, zeta, beta, True
    )
    center = jnp.mean(lin_raw, axis=-1, keepdims=True)
    spread = jnp.mean(jnp.square(lin_raw - center), axis=-1, keepdims=True)
    gains = own_columns(linear_head_gain, 0).astype(jnp.float32).reshape(lin_heads, HEAD_CHANNELS)
    lin_out = ((lin_raw - center) * lax.rsqrt(spread + 0.00064) * gains).astype(jnp.bfloat16)
    lin_out = lin_out.reshape(seq_count, tok_count, lin_cols)
    mixed = summed_on_arrival(
        (
            lax.dot_general(
                fox_out, softmax_output_weight, out_dims, preferred_element_type=jnp.float32
            )
            + lax.dot_general(
                lin_out, linear_output_weight, out_dims, preferred_element_type=jnp.float32
            )
        ).astype(jnp.bfloat16),
        "tp",
        0,
    )
    return mixed.astype(jnp.bfloat16)


def solution(mesh):
    placed = (
        P(("grp", "fs"), "sp", "tp"),
        P(),
        P("fs", "tp"),
        P("fs", "tp"),
        P("fs", "tp"),
        P(("grp", "fs"), None, "tp"),
        P("fs", "tp"),
        P("fs", "tp"),
        P("fs", "tp"),
        P(),
        P(),
        P(),
        P(("grp", "fs"), "sp", "tp"),
        P(),
        P(),
        P(),
        P(),
        P(("grp", "fs"), "tp", None, None),
        P(None, "tp"),
        P(None, "tp"),
    )
    return jax.shard_map(
        per_device,
        mesh=mesh,
        in_specs=placed,
        out_specs=P(("grp", "fs", "tp"), "sp", None),
        check_vma=False,
    )
```

profile of v0, /device:TPU:33, one launch (start us, length us, event | category | flops | bytes accessed | tf_op | source)
XLA Modules:
  0.0 582.4 jit_solution(8903582980980468005)
XLA Ops:
  17.4 24.0 %all-to-all-start = ((bf16[2,2,128,1024]{3,2,1,0:T(8,128)(2,1)}), bf16[2,2,128,1024]{3,2,1,0:T(8,128)(2,1)S(1)}, u32[]{:S(2)}, u32[]{:S(2)}) async-start(bf16[2,2,128,1024]{3,2,1,0:T(8,128)(2,1)} %broadcast_in_dim.100), calls=%async_computation | async-start | bytes 2097152 | tf_op jit(solution)/shard_map/all_to_all | solution.py:15
  49.9 2.9 fusion.130
  55.1 2.8 fusion.155
  62.4 93.1 %all-gather.7.cloned.1.call-done = bf16[2048,3072]{1,0:T(8,128)(2,1)} async-done(((bf16[512,3072]{1,0:T(8,128)(2,1)}), bf16[2048,3072]{1,0:T(8,128)(2,1)}) %all-gather.7.cloned.1.call-update) | async-done | bytes 12582928 | tf_op jit(solution)/shard_map/all_gather | solution.py:35
  155.5 2.6 fusion.140
  162.7 2.6 fusion.146
  170.4 3.7 fusion.150
  175.8 47.5 %while.57 = (s32[]{:T(128)}, f32[2,8,128,64]{2,3,1,0:T(8,128)S(1)}, f32[8,2,8,16,64]{4,2,3,1,0:T(8,128)}, f32[8,2,8,16,64]{4,2,3,1,0:T(8,128)}, f32[8,2,8,16,64]...) while((s32[]{:T(128)}, f32[2,8,128,64]{2,3,1,0:T(8,128)S(1)}, ...), condition=%wide.region_10.11_spmd.clone.clone, body=%wide.region_8.10_spmd.clone.clone.sunk | while | flops 17449984 | bytes 4396709 | solution.py:191
  228.1 3.4 fusion.131
  232.7 3.0 fusion.134
  239.3 3.0 fusion.137
  242.3 50.4 %all-gather.11.cloned.1.call-done = bf16[32,8,64,64]{3,2,1,0:T(8,128)(2,1)} async-done(((bf16[2,8,64,64]{3,2,1,0:T(8,128)(2,1)}), bf16[32,8,64,64]{3,2,1,0:T(8,128)(2,1)}) %all-gather.11.cloned.1.call-update) | async-done | bytes 2097168 | tf_op jit(solution)/shard_map/all_gather | solution.py:41
  292.7 75.1 %all-gather.13.cloned.1.call-done = bf16[32,8,64,64]{3,2,1,0:T(8,128)(2,1)} async-done(((bf16[2,8,64,64]{3,2,1,0:T(8,128)(2,1)}), bf16[32,8,64,64]{3,2,1,0:T(8,128)(2,1)}) %all-gather.13.cloned.1.call-update) | async-done | bytes 2097168 | tf_op jit(solution)/shard_map/all_gather | solution.py:41
  369.5 78.7 %while.58 = (s32[]{:T(128)}, f32[2,8,64,64]{3,2,1,0:T(8,128)S(1)}, f32[8,2,8,16,64]{4,3,2,1,0:T(8,128)}, f32[8,2,8,16,64]{4,2,3,1,0:T(8,128)}, f32[8,2,8,16,64]{...) while((s32[]{:T(128)}, f32[2,8,64,64]{3,2,1,0:T(8,128)S(1)}, ...), condition=%wide.region_15.16_spmd.clone.clone, body=%wide.region_13.15_spmd.clone.clone.sunk | while | flops 14157314 | bytes 3812017 | solution.py:191
  448.2 2.7 copy.174
  458.0 34.3 %all-gather.9.cloned.1.call-done = bf16[4,2048,512]{1,2,0:T(8,128)(2,1)} async-done(((bf16[4,128,512]{1,2,0:T(8,128)(2,1)}), bf16[4,2048,512]{1,2,0:T(8,128)(2,1)}) %all-gather.9.cloned.1.call-update) | async-done | bytes 8388624 | tf_op jit(solution)/shard_map/all_gather | solution.py:35
  492.3 66.1 %conditional.1 = (f32[2,8,128]{2,1,0:T(8,128)}, f32[2,8,128,64]{2,3,1,0:T(8,128)}) conditional(s32[]{:T(128)} %convert_element_type.97, () %tuple.39, (bf16[4,2048,512]{1,2,0:T(8,128)(2,1)}, bf16[256,512]{1,0:T(8,128)(2,1)S(1)}, s32[]{:T(128)}, s32[128]{0:T(128)S(1)}, f32[2,8,128]{2,1,0:T(8,128)S(1)}, /*index=5*/f32[2,2048,8]{1,2,0:T(8,128)}) %tuple.168), branch_computations={%region_1.0_spmd, %region_2.7_spmd} | conditional | flops 286730880 | bytes 55375728 | solution.py:130
  492.3 6.1 %fusion.163 = (bf16[2,2048,512]{1,2,0:T(8,128)(2,1)}, bf16[2,2048,512]{1,2,0:T(8,128)(2,1)}) fusion(bf16[4,2048,512]{1,2,0:T(8,128)(2,1)} %get-tuple-element.307), kind=kLoop, calls=%fused_computation.227 | loop fusion | bytes 16777216 | tf_op jit(solution)/shard_map/split | solution.py:35
  499.1 59.3 %while.55 = (s32[]{:T(128)}, f32[2,8,128]{2,1,0:T(8,128)S(1)}, f32[2,8,128]{2,1,0:T(8,128)}, f32[2,8,128,64]{2,3,1,0:T(8,128)}, s32[128]{0:T(128)S(1)}, /*index=...) while((s32[]{:T(128)}, f32[2,8,128]{2,1,0:T(8,128)S(1)}, ...), condition=%wide.region_6.6_spmd.clone, body=%wide.region_3.5_spmd.clone.sunk | while | flops 286730752 | bytes 37548772 | solution.py:127
  501.7 3.2 fusion.389
  504.9 4.0 fusion.390
  509.5 2.9 fusion.392
  515.1 3.2 fusion.389
  518.3 4.0 fusion.390
  523.6 4.2 fusion.392
  530.4 3.2 fusion.389
  533.6 4.0 fusion.390
  538.9 4.2 fusion.392
  545.7 3.2 fusion.389
  548.9 4.0 fusion.390
  554.2 4.2 fusion.392
  561.4 13.3 %all_to_all.10 = bf16[2,1,128,2048]{3,2,1,0:T(8,128)(2,1)S(1)} all-to-all(bf16[2,1,128,2048]{3,2,1,0:T(8,128)(2,1)S(1)} %fusion.108), channel_id=1, replica_groups=mesh['grp'=2,'sp'=16,'fs'=4,'tp'=2] {'tp'}, dimensions={0} | all-to-all | bytes 2097152 | tf_op jit(solution)/shard_map/all_to_all | solution.py:66
  (449 shorter events, 199.9 us)
Async XLA Ops:
  6.5 553.1 %copy-start = (bf16[2048,512]{1,0:T(8,128)(2,1)S(1)}, bf16[2048,512]{1,0:T(8,128)(2,1)}, u32[]{:S(2)}) copy-start(bf16[2048,512]{1,0:T(8,128)(2,1)} %param.48) | copy-start | bytes 6291460
  6.6 7.9 %copy-start.13 = (bf16[512,512]{1,0:T(8,128)(2,1)S(1)}, bf16[512,512]{1,0:T(8,128)(2,1)}, u32[]{:S(2)}) copy-start(bf16[512,512]{1,0:T(8,128)(2,1)} %param.37) | copy-start | bytes 1572868
  6.6 148.9 %all-gather.7.cloned.1.call-start = ((), (), s32[]{:S(2)}) async-start(), calls=%async_computation.2 | async-start | bytes 15728640 | tf_op jit(solution)/shard_map/all_gather | solution.py:35
  6.6 8.8 %copy-start.14 = (bf16[512,512]{1,0:T(8,128)(2,1)S(1)}, bf16[512,512]{1,0:T(8,128)(2,1)}, u32[]{:S(2)}) copy-start(bf16[512,512]{1,0:T(8,128)(2,1)} %param.38) | copy-start | bytes 1572868
  8.6 7.6 %copy-start.11 = (bf16[2,128,1024]{2,1,0:T(8,128)(2,1)S(1)}, bf16[2,128,1024]{2,1,0:T(8,128)(2,1)}, u32[]{:S(2)}) copy-start(bf16[2,128,1024]{2,1,0:T(8,128)(2,1)} %param.30) | copy-start | bytes 1572868
  17.4 25.7 %all-to-all-start = ((bf16[2,2,128,1024]{3,2,1,0:T(8,128)(2,1)}), bf16[2,2,128,1024]{3,2,1,0:T(8,128)(2,1)S(1)}, u32[]{:S(2)}, u32[]{:S(2)}) async-start(bf16[2,2,128,1024]{3,2,1,0:T(8,128)(2,1)} %broadcast_in_dim.100), calls=%async_computation | async-start | bytes 2097152 | tf_op jit(solution)/shard_map/all_to_all | solution.py:15
  41.4 251.3 %all-gather.11.cloned.1.call-start = ((), (), s32[]{:S(2)}) async-start(), calls=%async_computation.4 | async-start | bytes 4456448 | tf_op jit(solution)/shard_map/all_gather | solution.py:41
  43.4 3.9 copy-start.20
  43.4 3.9 copy-start.21
  45.0 4.8 copy-start.24
  47.6 7.4 %copy-start.22 = (f32[1024]{0:T(1024)S(1)}, f32[1024]{0:T(1024)}, u32[]{:S(2)}) copy-start(f32[1024]{0:T(1024)} %param.41) | copy-start | bytes 12292
  49.9 8.1 %copy-start.9 = (bf16[256,2048]{1,0:T(8,128)(2,1)}, bf16[256,2048]{1,0:T(8,128)(2,1)S(1)}, u32[]{:S(2)}) copy-start(bf16[256,2048]{1,0:T(8,128)(2,1)S(1)} %multiply_convert_fusion) | copy-start | bytes 3145732
  52.8 7.4 %copy-start.19 = (f32[2,128,8]{1,2,0:T(8,128)S(1)}, f32[2,128,8]{1,2,0:T(8,128)}, u32[]{:S(2)}) copy-start(f32[2,128,8]{1,2,0:T(8,128)} %param.42) | copy-start | bytes 24580
  169.2 4.9 copy-start.12
  169.5 4.6 copy-start.3
  169.5 4.6 copy-start.4
  175.8 49.8 %copy-start.23 = (bf16[1024]{0:T(1024)(128)(2,1)S(1)}, bf16[1024]{0:T(1024)(128)(2,1)}, u32[]{:S(2)}) copy-start(bf16[1024]{0:T(1024)(128)(2,1)} %param.46) | copy-start | bytes 6148
  224.5 143.4 %all-gather.13.cloned.1.call-start = ((), (), s32[]{:S(2)}) async-start(), calls=%async_computation.5 | async-start | bytes 4456448 | tf_op jit(solution)/shard_map/all_gather | solution.py:41
  225.3 267.0 %all-gather.9.cloned.1.call-start = ((), (), s32[]{:S(2)}) async-start(), calls=%async_computation.3 | async-start | bytes 8912896 | tf_op jit(solution)/shard_map/all_gather | solution.py:35
  228.1 4.5 copy-start.10
  235.7 132.2 %copy-start.16 = (f32[64,64]{0,1:T(8,128)S(1)}, f32[64,64]{0,1:T(8,128)}, u32[]{:S(2)}) copy-start(f32[64,64]{0,1:T(8,128)} %copy-done.15) | copy-start | bytes 49156
  448.2 5.0 copy-start.2
  450.9 41.4 %copy-start.17 = (bf16[256,512]{1,0:T(8,128)(2,1)S(1)}, bf16[256,512]{1,0:T(8,128)(2,1)}, u32[]{:S(2)}) copy-start(bf16[256,512]{1,0:T(8,128)(2,1)} %fusion.137) | copy-start | bytes 786436
  504.9 4.6 copy-start.1
  518.3 5.3 copy-start.1
  533.6 5.3 copy-start.1
  548.9 5.3 copy-start.1
  558.4 2.1 copy-start.5
  558.4 2.1 copy-start.6
  558.4 2.1 copy-start.7
  558.4 2.2 copy-start.8
  558.4 2.2 copy-start.18
  (1 other events, 0.6 us)
Sparse Core Ops, SparseCore 0:
  16.4 139.0 all-gather.6
  224.6 68.0 all-gather.10
  294.5 73.2 all-gather.12
  369.5 122.7 all-gather.8
where the time goes:
time: 589 us; the launch traced here: 582 us
  waiting for transfers between devices  256 us (43%)
  matrix products  121 us (21%)
  other arithmetic  85.7 us (15%)
  local copies, waits for them, and re-layouts  66.6 us (11%)
  starting transfers between devices  24.3 us (4%)
  between operations  13.6 us (2%)
  blocking collectives  13.3 us (2%)
    all_gather x2, waiting for transfers between devices, sent_together(): lax.all_gather(both, axis, axis=dim, tiled=True)  127 us
    all_gather x2, waiting for transfers between devices, prefix(): lax.all_gather(a.astype(kind), axis)  126 us
    dot_general x128, matrix products, apply_mix(): return jnp.einsum('shtj,shjv->shtv', matrix, values)  41.7 us
    mul x16, other arithmetic, advance(): key_risen * ending  24.7 us
    all_to_all x1, starting transfers between devices, from_everyone(): return lax.all_to_all(copies, axis, split_axis=0, concat_axis=0, tiled=True)  24 us
    dot_general x6, matrix products, project(): return jnp.dot(flat_rows, weight, preferred_element_type=jnp.float32)  17.2 us
    reduce_sum x4, other arithmetic, one_block(): total_next = total_prev * fading + jnp.sum(weights, axis=-1)  15.9 us
    dot_general x4, matrix products, one_block(): jnp.einsum('shqk,skhd->shqd', weights.astype(jnp.bfloat16), value_part, p...  15.4 us
  transfers between devices with their start and end apart: 5, of which 5 were waited for; matrix products, arithmetic and copies ran while one was open for 22% of the time, Pallas kernels for 0%

commit v1 on v0

v1 whole, which is shorter than its diff:
```python
import functools

import jax
import jax.numpy as jnp
from jax import lax
from jax.experimental import pallas as pl
from jax.experimental.pallas import tpu as pltpu
from jax.sharding import PartitionSpec as P

HEAD_CHANNELS = 64
CHUNK = 64
F32 = jnp.float32
BF16 = jnp.bfloat16
VMEM_BYTES = 56 * 1024 * 1024

MM = (((1,), (0,)), ((), ()))
NT = (((1,), (1,)), ((), ()))
TN = (((0,), (0,)), ((), ()))


def mul(left, right, dims=MM):
    return lax.dot_general(
        left.astype(BF16), right.astype(BF16), dims, preferred_element_type=F32
    )


def places(shape, dim):
    return lax.broadcasted_iota(jnp.int32, shape, dim)


def attention_kernel(blocks_ref, gate_ref, out_ref, key_scr, value_scr):
    count, _, width = blocks_ref.shape
    channels = HEAD_CHANNELS
    for i in range(count):
        gate = gate_ref[:, i * width : (i + 1) * width]
        high = gate.astype(BF16).astype(F32)
        rest = gate - high
        middle = rest.astype(BF16).astype(F32)
        low = rest - middle
        row = places((channels, width), 0)
        extra = jnp.where(row == 0, high, jnp.where(row == 1, middle, jnp.where(row == 2, low, 0.0)))
        key_rows = blocks_ref[i, channels : 2 * channels, :].astype(F32)
        key_scr[i * width : (i + 1) * width, :] = jnp.concatenate((key_rows, extra), 0).T.astype(BF16)
        value_scr[:, i * width : (i + 1) * width] = blocks_ref[i, 2 * channels :, :]
    step = 2 * width
    row = places((channels, step), 0)
    tail = jnp.where(row < 3, -1.0, 0.0).astype(BF16)
    live = places((step, step), 0) <= places((step, step), 1)
    for i in range(count // 2):
        query = jnp.concatenate(
            (blocks_ref[2 * i, :channels, :], blocks_ref[2 * i + 1, :channels, :]), 1
        )
        query = (query.astype(F32) * channels ** (-0.5)).astype(BF16)
        query = jnp.concatenate((query, tail), 0)
        before = i * step
        own = lax.dot_general(
            key_scr[before : before + step, :], query, MM, preferred_element_type=F32
        )
        own = jnp.where(live, own, -1e30)
        top = jnp.max(own, axis=0, keepdims=True)
        if before:
            past = lax.dot_general(key_scr[:before, :], query, MM, preferred_element_type=F32)
            top = jnp.maximum(top, jnp.max(past, axis=0, keepdims=True))
        weight = jnp.exp(own - top)
        total = jnp.sum(weight, axis=0, keepdims=True)
        mixed = lax.dot_general(
            value_scr[:, before : before + step],
            weight.astype(BF16),
            MM,
            preferred_element_type=F32,
        )
        if before:
            weight = jnp.exp(past - top)
            total = total + jnp.sum(weight, axis=0, keepdims=True)
            mixed = mixed + lax.dot_general(
                value_scr[:, :before], weight.astype(BF16), MM, preferred_element_type=F32
            )
        mixed = (mixed / total).astype(BF16)
        out_ref[2 * i] = mixed[:, :width]
        out_ref[2 * i + 1] = mixed[:, width:]


def attention(blocks, gate):
    count, rows, width = blocks.shape
    whole = pl.BlockSpec(memory_space=pltpu.VMEM)
    return pl.pallas_call(
        attention_kernel,
        out_shape=jax.ShapeDtypeStruct((count, HEAD_CHANNELS, width), BF16),
        in_specs=[whole, whole],
        out_specs=whole,
        scratch_shapes=[
            pltpu.VMEM((count * width, 2 * HEAD_CHANNELS), BF16),
            pltpu.VMEM((HEAD_CHANNELS, count * width), BF16),
        ],
        compiler_params=pltpu.CompilerParams(vmem_limit_bytes=VMEM_BYTES),
        cost_estimate=pl.CostEstimate(
            flops=4 * HEAD_CHANNELS * (count * width) ** 2,
            bytes_accessed=4 * count * rows * width,
            transcendentals=(count * width) ** 2 // 2,
        ),
        name="attention",
    )(blocks, gate)


def chunk_masks(size):
    row, col = places((2 * size, 2 * size), 0), places((2 * size, 2 * size), 1)
    same = row // CHUNK == col // CHUNK
    return row, col, same


def maps_kernel(proj_ref, log_ref, rate_ref, q_ref, o_ref, maps_ref):
    size = proj_ref.shape[0]
    cols = log_ref.shape[1]
    lanes = 2 * HEAD_CHANNELS
    pairs = cols // lanes
    row, col, same = chunk_masks(size)
    strict = same & (row > col)
    upto = same & (row >= col)
    merges = []
    block = 2
    while block < CHUNK:
        merges.append((row // (2 * block) == col // (2 * block)) & (row // block > col // block))
        block *= 2
    pairs_of_two = (row // 2 == col // 2) & (row > col)
    identity = (row == col).astype(F32)
    lane = places((size, lanes), 1)
    first_head = lane < HEAD_CHANNELS
    head_block = (places((lanes, lanes), 0) < HEAD_CHANNELS) == (
        places((lanes, lanes), 1) < HEAD_CHANNELS
    )
    diagonal = places((lanes, lanes), 0) == places((lanes, lanes), 1)
    small_row, small_col = places((size, size), 0), places((size, size), 1)
    running = ((small_row // CHUNK == small_col // CHUNK) & (small_row >= small_col)).astype(F32)
    head_sum = head_block.astype(F32)
    tops, bottoms = slice(0, CHUNK), slice(CHUNK, 2 * CHUNK)

    def stacked(values):
        return jnp.concatenate(
            (jnp.where(first_head, values, 0.0), jnp.where(first_head, 0.0, values)), 0
        )

    def each_chunk(values, at):
        return jnp.concatenate(
            [jnp.broadcast_to(values[c + at : c + at + 1], (CHUNK, lanes)) for c in (0, CHUNK)], 0
        )

    held = []
    for p in range(pairs):
        at = slice(p * lanes, (p + 1) * lanes)
        rec = proj_ref[:, p * lanes : (p + 1) * lanes].astype(F32)
        key = proj_ref[:, cols + p * lanes : cols + (p + 1) * lanes].astype(F32)
        value = proj_ref[:, 2 * cols + p * lanes : 2 * cols + (p + 1) * lanes].astype(F32)
        logged = log_ref[:, at]
        squares = lax.dot_general(
            key * key, head_sum, MM, precision=lax.Precision.HIGHEST, preferred_element_type=F32
        )
        unit = key * lax.rsqrt(squares + 1e-06)
        beta = unit * rate_ref[:, at]
        total = lax.dot_general(
            running, logged, MM, precision=lax.Precision.HIGHEST, preferred_element_type=F32
        )
        middle = each_chunk(total, CHUNK // 2 - 1)
        ending = each_chunk(total, CHUNK - 1)
        previous = total - logged
        fall = jnp.exp(middle - total)
        to_end = jnp.exp(ending - total)
        zeta = -unit
        left = jnp.concatenate(
            (stacked(zeta * jnp.exp(previous - middle)), stacked(rec * jnp.exp(total - middle))), 0
        )
        right = jnp.concatenate((beta * fall, key * fall), 0)
        held.append(
            dict(
                grams=mul(left, right, NT),
                zeta_true=zeta * jnp.exp(previous),
                rec_true=rec * jnp.exp(total),
                beta_end=beta * to_end,
                key_end=key * to_end,
                value=value,
                ending=jnp.exp(total),
            )
        )
    for h in held:
        grams = h.pop("grams")
        blank = jnp.zeros((size, size), F32)

        def spread(first, second, mask):
            both = jnp.concatenate(
                (
                    jnp.concatenate((first, blank), 1),
                    jnp.concatenate((blank, second), 1),
                ),
                0,
            )
            return jnp.where(mask, both, 0.0).astype(BF16)

        h["zb"] = spread(grams[:size, :size], grams[size : 2 * size, :size], strict)
        h["zk"] = spread(grams[:size, size:], grams[size : 2 * size, size:], strict)
        h["rb"] = spread(grams[2 * size : 3 * size, :size], grams[3 * size :, :size], upto)
        h["rk"] = spread(grams[2 * size : 3 * size, size:], grams[3 * size :, size:], upto)
        h["inverse"] = identity + jnp.where(pairs_of_two, h["zb"].astype(F32), 0.0)
        h["from_values"] = mul(
            jnp.concatenate((h["zk"], h["rk"]), 0), stacked(h["value"])
        )
    for merge in merges:
        for h in held:
            inner = mul(jnp.where(merge, h["zb"].astype(F32), 0.0), h["inverse"])
            h["inner"] = inner
        for h in held:
            h["inverse"] = h["inverse"] + mul(h["inverse"], h["inner"])
    for h in held:
        right = jnp.concatenate((stacked(h["zeta_true"]), h["from_values"][: 2 * size]), 1)
        h["pulled"] = mul(h["inverse"], right)
    for p, h in enumerate(held):
        start = jnp.concatenate((stacked(h["rec_true"]), h["from_values"][2 * size :]), 1)
        seen = start + mul(h["rb"], h["pulled"])
        seen = seen[:size] + seen[size:]
        pulled = h["pulled"][:size] + h["pulled"][size:]
        query, ready = seen[:, :lanes], seen[:, lanes:]
        maps = []
        for part, last in ((tops, CHUNK - 1), (bottoms, 2 * CHUNK - 1)):
            moved = mul(pulled[part], h["beta_end"][part], TN)
            added = mul(h["value"][part], h["key_end"][part], TN)
            kept = jnp.where(diagonal, h["ending"][last : last + 1], 0.0)
            maps.append(
                (
                    kept + jnp.where(head_block, moved[:lanes], 0.0),
                    jnp.where(head_block, moved[lanes:] + added, 0.0),
                )
            )
        both = mul(jnp.concatenate(maps[0], 0), maps[1][0])
        carry = both[:lanes]
        offset = both[lanes:] + maps[1][1]
        later = mul(query[bottoms], jnp.concatenate(maps[0], 0), NT)
        query = jnp.concatenate((query[tops], later[:, :lanes]), 0)
        ready = jnp.concatenate((ready[tops], ready[bottoms] + later[:, lanes:]), 0)
        at = slice(p * lanes, (p + 1) * lanes)
        q_ref[:, at] = query.astype(BF16)
        o_ref[:, at] = ready
        half = places((HEAD_CHANNELS, lanes), 1) < HEAD_CHANNELS
        turned_offset = pltpu.roll(offset, HEAD_CHANNELS, 1)
        turned_carry = pltpu.roll(carry, HEAD_CHANNELS, 1)
        maps_ref[2 * p] = jnp.where(
            half, carry[:HEAD_CHANNELS], turned_offset[:HEAD_CHANNELS]
        ).astype(BF16)
        maps_ref[2 * p + 1] = jnp.where(
            half, turned_carry[HEAD_CHANNELS:], offset[HEAD_CHANNELS:]
        ).astype(BF16)


def position_maps(proj, logged, rate, tok_count):
    rows, cols = logged.shape
    seqs = rows // tok_count
    heads = cols // HEAD_CHANNELS
    lanes = 2 * HEAD_CHANNELS
    return pl.pallas_call(
        maps_kernel,
        grid=(seqs,),
        out_shape=(
            jax.ShapeDtypeStruct((rows, cols), BF16),
            jax.ShapeDtypeStruct((rows, cols), F32),
            jax.ShapeDtypeStruct((seqs * heads, HEAD_CHANNELS, lanes), BF16),
        ),
        in_specs=[
            pl.BlockSpec((tok_count, 3 * cols), lambda s: (s, 0)),
            pl.BlockSpec((tok_count, cols), lambda s: (s, 0)),
            pl.BlockSpec((tok_count, cols), lambda s: (s, 0)),
        ],
        out_specs=(
            pl.BlockSpec((tok_count, cols), lambda s: (s, 0)),
            pl.BlockSpec((tok_count, cols), lambda s: (s, 0)),
            pl.BlockSpec((heads, HEAD_CHANNELS, lanes), lambda s: (s, 0, 0)),
        ),
        compiler_params=pltpu.CompilerParams(vmem_limit_bytes=VMEM_BYTES),
        cost_estimate=pl.CostEstimate(
            flops=rows * cols * 2 * 256 * 20,
            bytes_accessed=rows * cols * 20,
            transcendentals=6 * rows * cols,
        ),
        name="position_maps",
    )(proj, logged, rate)


def states_kernel(maps_ref, start_ref, out_ref):
    count = maps_ref.shape[0]
    n = HEAD_CHANNELS
    state = start_ref[...]
    for i in range(count):
        out_ref[i] = jnp.concatenate((state[: n // 2], state[n // 2 :]), 1).astype(BF16)
        if i + 1 < count:
            pair = maps_ref[i]
            high = state.astype(BF16)
            low = (state - high.astype(F32)).astype(BF16)
            moved = mul(jnp.concatenate((high, low), 0), pair[:, :n])
            state = moved[:n] + moved[n:] + pair[:, n:].astype(F32)


def states_ahead(maps, start):
    count = maps.shape[0]
    whole = pl.BlockSpec(memory_space=pltpu.VMEM)
    return pl.pallas_call(
        states_kernel,
        out_shape=jax.ShapeDtypeStruct((count, HEAD_CHANNELS // 2, 2 * HEAD_CHANNELS), BF16),
        in_specs=[whole, whole],
        out_specs=whole,
        cost_estimate=pl.CostEstimate(
            flops=count * 4 * HEAD_CHANNELS**3, bytes_accessed=1 << 19, transcendentals=0
        ),
        name="states_ahead",
    )(maps, start)


def closing_kernel(back_ref, q_ref, o_ref, gain_ref, fox_w_ref, lin_w_ref, out_ref, act_scr):
    n = HEAD_CHANNELS
    lanes = 2 * n
    rows, cols = q_ref.shape
    count, _, tok_count = back_ref.shape
    heads = cols // n
    seqs = rows // tok_count

    @pl.when(pl.program_id(0) == 0)
    def _():
        head_block = (places((lanes, lanes), 0) < n) == (places((lanes, lanes), 1) < n)
        average = jnp.where(head_block, 1.0 / n, 0.0).astype(BF16)
        first = places((n // 2, lanes), 1) < n

        def mean(values):
            high = values.astype(BF16)
            low = (values - high.astype(F32)).astype(BF16)
            return mul(high, average) + mul(low, average)

        for s in range(seqs):
            here = slice(s * tok_count, (s + 1) * tok_count)
            for p in range(heads // 2):
                at = slice(p * lanes, (p + 1) * lanes)
                j = s * heads + 2 * p
                fox = jnp.concatenate((back_ref[j, :n, :], back_ref[j + 1, :n, :]), 0)
                act_scr[here, at] = fox.astype(F32).T.astype(BF16)
                parts = []
                for k in range(2):
                    packed = back_ref[j + k, n:, :].astype(F32)
                    turned = pltpu.roll(packed, n, 1)
                    upper, lower = (packed, turned) if k == 0 else (turned, packed)
                    if k == 0:
                        parts += [jnp.where(first, packed, 0.0), jnp.where(first, turned, 0.0)]
                    else:
                        parts += [jnp.where(first, 0.0, turned), jnp.where(first, 0.0, packed)]
                state = jnp.concatenate(parts, 0)
                raw = mul(q_ref[here, at], state, NT) + o_ref[here, at]
                centred = raw - mean(raw)
                spread = mean(centred * centred)
                lin = centred * lax.rsqrt(spread + 0.00064) * gain_ref[:, at].astype(F32)
                act_scr[here, slice(cols + p * lanes, cols + (p + 1) * lanes)] = lin.astype(BF16)

    out_ref[...] = (
        lax.dot_general(act_scr[:, :cols], fox_w_ref[...], NT, preferred_element_type=F32)
        + lax.dot_general(act_scr[:, cols:], lin_w_ref[...], NT, preferred_element_type=F32)
    ).astype(BF16)


def closing(back, query, ready, gain, fox_w, lin_w):
    rows, cols = query.shape
    width = fox_w.shape[0]
    tile = 512
    whole = pl.BlockSpec(memory_space=pltpu.VMEM)
    return pl.pallas_call(
        closing_kernel,
        grid=(width // tile,),
        out_shape=jax.ShapeDtypeStruct((rows, width), BF16),
        in_specs=[
            whole,
            whole,
            whole,
            whole,
            pl.BlockSpec((tile, cols), lambda i: (i, 0)),
            pl.BlockSpec((tile, cols), lambda i: (i, 0)),
        ],
        out_specs=pl.BlockSpec((rows, tile), lambda i: (0, i)),
        scratch_shapes=[pltpu.VMEM((rows, 2 * cols), BF16)],
        compiler_params=pltpu.CompilerParams(vmem_limit_bytes=VMEM_BYTES),
        cost_estimate=pl.CostEstimate(
            flops=4 * rows * cols * width,
            bytes_accessed=4 * cols * width + 2 * rows * width,
            transcendentals=0,
        ),
        name="closing",
    )(back, query, ready, gain, fox_w, lin_w)


def gathered(arrays, axis):
    return lax.all_gather(jnp.concatenate(arrays, axis=1), axis, axis=0, tiled=True)


def per_device(
    inputs,
    input_norm_gain,
    softmax_query_matrix,
    softmax_key_matrix,
    softmax_value_matrix,
    running_forget_gate,
    receptance_weight,
    linear_key_weight,
    linear_value_weight,
    decay_lower_map,
    decay_upper_map,
    decay_offset_base,
    decay_extra_log,
    rate_lower_map,
    rate_upper_map,
    rate_offset_base,
    linear_head_gain,
    starting_state,
    softmax_output_weight,
    linear_output_weight,
):
    n = HEAD_CHANNELS
    seq_count, tok_count, half_width = inputs.shape
    rows = seq_count * tok_count
    cols = softmax_query_matrix.shape[1]
    heads = cols // n
    place = lax.axis_index("sp")
    col_start = lax.axis_index("tp") * cols

    fox_w = gathered((softmax_query_matrix, softmax_key_matrix, softmax_value_matrix), "fs")
    lin_w = gathered((receptance_weight, linear_key_weight, linear_value_weight), "fs")

    flat = inputs.reshape(rows, half_width)
    tp = lax.axis_size("tp")
    both = lax.all_to_all(
        jnp.broadcast_to(flat, (tp, rows, half_width)), "tp", 0, 0, tiled=True
    )
    whole = jnp.moveaxis(both, 0, 1).reshape(rows, tp * half_width).astype(F32)
    scaling = lax.rsqrt(jnp.mean(whole * whole, axis=-1, keepdims=True) + 1e-06)
    normed = (whole * scaling * input_norm_gain.astype(F32)).astype(BF16)

    def project(weight):
        return jnp.dot(normed, weight, preferred_element_type=F32)

    def own_columns(table, axis):
        return lax.dynamic_slice_in_dim(table, col_start, cols, axis)

    decay_low = jnp.tanh(project(decay_lower_map)).astype(BF16)
    decay_preact = own_columns(decay_offset_base, 0) + jnp.dot(
        decay_low, own_columns(decay_upper_map, 1), preferred_element_type=F32
    )
    extra = jnp.repeat(decay_extra_log.reshape(rows, heads), n, axis=1)
    decay_logged = -jnp.exp(-jax.nn.softplus(-decay_preact) - 0.5) + extra
    rate_low = project(rate_lower_map).astype(BF16)
    rate = jax.nn.sigmoid(
        own_columns(rate_offset_base, 0)
        + jnp.dot(rate_low, own_columns(rate_upper_map, 1), preferred_element_type=F32)
    )
    gate_rows = running_forget_gate.transpose(0, 2, 1).reshape(seq_count * heads, 1, -1)
    gate = lax.dynamic_index_in_dim(gate_rows, place, 0, False)
    start = lax.dynamic_index_in_dim(
        starting_state.reshape(seq_count * heads, n, n), place, 0, False
    )

    fox = lax.dot_general(
        fox_w, normed, (((0,), (1,)), ((), ())), preferred_element_type=F32
    ).astype(BF16)
    fox = fox.reshape(3, heads, n, seq_count, tok_count).transpose(3, 1, 0, 2, 4)
    fox = fox.reshape(seq_count * heads, 3 * n, tok_count)
    fox = lax.all_to_all(fox, "sp", 0, 0, tiled=True)
    fox_out = attention(fox, gate)

    lin = project(lin_w).astype(BF16)
    query, ready, maps = position_maps(lin, decay_logged, rate, tok_count)
    maps = lax.all_to_all(maps, "sp", 0, 0, tiled=True)
    states = states_ahead(maps, start)
    back = lax.all_to_all(jnp.concatenate((fox_out, states), 1), "sp", 0, 0, tiled=True)
    gain = own_columns(linear_head_gain, 0).reshape(1, cols)
    partial = closing(back, query, ready, gain, softmax_output_weight, linear_output_weight)
    pieces = lax.all_to_all(
        partial.reshape(seq_count, tok_count, -1), "tp", 0, 0, tiled=True
    )
    mixed = jnp.sum(
        pieces.reshape(tp, seq_count // tp, tok_count, -1).astype(F32), axis=0
    )
    return mixed.astype(BF16)


def solution(mesh):
    placed = (
        P(("grp", "fs"), "sp", "tp"),
        P(),
        P("fs", "tp"),
        P("fs", "tp"),
        P("fs", "tp"),
        P(("grp", "fs"), None, "tp"),
        P("fs", "tp"),
        P("fs", "tp"),
        P("fs", "tp"),
        P(),
        P(),
        P(),
        P(("grp", "fs"), "sp", "tp"),
        P(),
        P(),
        P(),
        P(),
        P(("grp", "fs"), "tp", None, None),
        P(None, "tp"),
        P(None, "tp"),
    )
    return jax.shard_map(
        per_device,
        mesh=mesh,
        in_specs=placed,
        out_specs=P(("grp", "fs", "tp"), "sp", None),
        check_vma=False,
    )
```

time: 589 us -> 291 us (0.49)
  waiting for transfers between devices: 256 us -> 145 us
  matrix products: 121 us -> 13.4 us
  other arithmetic: 85.7 us -> 7.55 us
  local copies, waits for them, and re-layouts: 66.6 us -> 8.08 us
  starting transfers between devices: 24.3 us -> 60.6 us
  Pallas kernels: 0 us -> 29.5 us
    all_gather x4 -> x2, waiting for transfers between devices: 253 us -> 98.5 us  [gathered(): lax.all_gather(jnp.concatenate(arrays, axis=1), axis, axis=0, tiled=True)]
    dot_general x201 -> x2, matrix products: 116 us -> 10.1 us  [the longest x1 5.49 us: project(): return jnp.dot(normed, weight, preferred_element_type=F32)]
    all_to_all x1 -> x4, waiting for transfers between devices: 1.74 us -> 46.6 us  [the longest x1 28.2 us: per_device(): fox = lax.all_to_all(fox, 'sp', 0, 0, tiled=True)]
    all_to_all x1 -> x4, starting transfers between devices: 24 us -> 60.5 us  [the longest x1 24.1 us: per_device(): lax.all_to_all(jnp.broadcast_to(flat, (tp, rows, half_width)), 'tp', 0, 0...]
    pallas_call x0 -> x4, Pallas kernels: none -> 29.5 us  [the longest x1 11.8 us: position_maps(): pl.pallas_call(maps_kernel, grid=(seqs,), out_shape=(jax.ShapeDtypeStruct...]
    mul x17 -> x0, other arithmetic: 24.7 us -> none  [the longest x16 24.7 us: advance(): key_risen * ending]
    reduce_sum x9 -> x2, other arithmetic: 18.4 us -> 1.42 us  [the longest x1 1.12 us: per_device(): jnp.sum(pieces.reshape(tp, seq_count // tp, tok_count, -1).astype(F32), a...]
    another operation x16 -> x0, other arithmetic: 14.9 us -> none  [advance(): cumulative = jnp.cumsum(decay_span, axis=2)]
  transfers between devices with their start and end apart: 5 -> 6, of which waited for: 5 -> 5; matrix products, arithmetic and copies ran while one was open for 22% -> 7% of each run, Pallas kernels for 0% -> 5%
where the time goes in v1:
time: 291 us; the launch traced here: 290 us
  waiting for transfers between devices  145 us (50%)
  starting transfers between devices  60.6 us (21%)
  Pallas kernels  29.5 us (10%)
  between operations  13.6 us (5%)
  matrix products  13.4 us (5%)
  blocking collectives  12.2 us (4%)
  local copies, waits for them, and re-layouts  8.08 us (3%)
  other arithmetic  7.55 us (3%)
    all_gather x2, waiting for transfers between devices, gathered(): lax.all_gather(jnp.concatenate(arrays, axis=1), axis, axis=0, tiled=True)  98.5 us
    all_to_all x1, waiting for transfers between devices, per_device(): fox = lax.all_to_all(fox, 'sp', 0, 0, tiled=True)  28.2 us
    all_to_all x1, starting transfers between devices, per_device(): lax.all_to_all(jnp.broadcast_to(flat, (tp, rows, half_width)), 'tp', 0, 0...  24.1 us
    all_to_all x1, waiting for transfers between devices, per_device(): lax.all_to_all(jnp.concatenate((fox_out, states), 1), 'sp', 0, 0, tiled=T...  17.1 us
    all_to_all x1, blocking collectives, per_device(): lax.all_to_all(partial.reshape(seq_count, tok_count, -1), 'tp', 0, 0, til...  12.2 us
    all_to_all x1, starting transfers between devices, per_device(): lax.all_to_all(jnp.concatenate((fox_out, states), 1), 'sp', 0, 0, tiled=T...  12.1 us
    all_to_all x1, starting transfers between devices, per_device(): maps = lax.all_to_all(maps, 'sp', 0, 0, tiled=True)  12.1 us
    all_to_all x1, starting transfers between devices, per_device(): fox = lax.all_to_all(fox, 'sp', 0, 0, tiled=True)  12.1 us
  transfers between devices with their start and end apart: 6, of which 5 were waited for; matrix products, arithmetic and copies ran while one was open for 7% of the time, Pallas kernels for 5%

profile of v1, /device:TPU:33, one launch (start us, length us, event | category | flops | bytes accessed | tf_op | source)
XLA Modules:
  0.0 290.0 jit_solution(16355397417969844618)
XLA Ops:
  6.6 2.8 pad_maximum_fusion.1
  9.6 1.3 pad_maximum_fusion
  10.9 0.2 copy.22
  11.2 1.0 broadcast_in_dim.4
  12.2 24.1 %all-to-all-start = ((bf16[2,256,1024]{1,2,0:T(8,128)(2,1)}), bf16[2,256,1024]{1,2,0:T(8,128)(2,1)S(1)}, u32[]{:S(2)}, u32[]{:S(2)}) async-start(bf16[2,256,1024]{1,2,0:T(8,128)(2,1)} %broadcast_in_dim.4), calls=%async_computation | async-start | bytes 2097152 | tf_op jit(solution)/shard_map/all_to_all | solution.py:429
  36.8 1.3 all-to-all-done
  38.1 0.3 multiply_reduce_fusion
  38.4 0.3 fusion.1
  38.8 1.5 fusion.6.rate_ref
  40.3 1.8 fusion.12.log_ref
  42.1 53.7 %all-gather.5.cloned.1.call-done = bf16[2048,1536]{1,0:T(8,128)(2,1)} async-done(((bf16[512,1536]{1,0:T(8,128)(2,1)}), bf16[2048,1536]{1,0:T(8,128)(2,1)}) %all-gather.5.cloned.1.call-update) | async-done | bytes 6291472 | tf_op jit(solution)/shard_map/all_gather | solution.py:391
  95.7 5.5 %convolution_convert_fusion.proj_ref = bf16[256,1536]{1,0:T(8,128)(2,1)} fusion(bf16[256,2048]{0,1:T(8,128)(2,1)S(1)} %fusion.1, bf16[2048,1536]{1,0:T(8,128)(2,1)} %all-gather.5.cloned.1.call-done), kind=kOutput, calls=%fused_computation | convolution fusion | flops 1611005952 | bytes 8126464 | tf_op jit(solution)/shard_map/dot_general | solution.py:437
  101.2 11.8 %position_maps.1 = (bf16[256,512]{1,0:T(8,128)(2,1)}, f32[256,512]{1,0:T(8,128)}, bf16[16,64,128]{2,1,0:T(8,128)(2,1)}) custom-call(bf16[256,1536]{1,0:T(8,128)(2,1)} %convolution_convert_fusion.proj_ref, f32[256,512]{1,0:T(8,128)} %fusion.12.log_ref, f32[256,512]{1,0:T(8,128)} %fusion.6.rate_ref), custom_call_target="tpu_custom_call" | custom-call | flops 1342177280 | bytes 2621440 | tf_op jit(solution)/shard_map/position_maps/pallas_call | solution.py:256
  113.1 12.1 %all-to-all-start.2 = ((bf16[16,64,128]{2,1,0:T(8,128)(2,1)}), bf16[16,64,128]{2,1,0:T(8,128)(2,1)S(1)}, u32[]{:S(2)}, u32[]{:S(2)}) async-start(bf16[16,64,128]{2,1,0:T(8,128)(2,1)} %get-tuple-element.8), calls=%async_computation.2 | async-start | bytes 524288 | tf_op jit(solution)/shard_map/all_to_all | solution.py:469
  125.2 44.8 %all-gather.3.cloned.1.call-done = bf16[2048,1536]{1,0:T(8,128)(2,1)} async-done(((bf16[512,1536]{1,0:T(8,128)(2,1)}), bf16[2048,1536]{1,0:T(8,128)(2,1)}) %all-gather.3.cloned.1.call-update) | async-done | bytes 6291472 | tf_op jit(solution)/shard_map/all_gather | solution.py:391
  170.0 4.6 %convolution_convert_fusion.1 = bf16[1536,256]{1,0:T(8,128)(2,1)S(1)} fusion(bf16[2048,1536]{1,0:T(8,128)(2,1)} %all-gather.3.cloned.1.call-done, bf16[256,2048]{0,1:T(8,128)(2,1)S(1)} %fusion.1), kind=kOutput, calls=%fused_computation.1 | convolution fusion | flops 1611005952 | bytes 8126464 | tf_op jit(solution)/shard_map/dot_general | solution.py:459
  174.8 1.1 copy.23
  175.9 12.1 %all-to-all-start.1 = ((bf16[16,192,128]{2,1,0:T(8,128)(2,1)}), bf16[16,192,128]{2,1,0:T(8,128)(2,1)S(1)}, u32[]{:S(2)}, u32[]{:S(2)}) async-start(bf16[16,192,128]{2,1,0:T(8,128)(2,1)} %bitcast.4), calls=%async_computation.1 | async-start | bytes 1572864 | tf_op jit(solution)/shard_map/all_to_all | solution.py:464
  188.0 1.4 dynamic-slice_bitcast_fusion.start_ref
  189.4 1.4 dynamic-slice_bitcast_fusion.1.gate_ref
  190.8 3.6 %states_ahead.1 = bf16[16,32,128]{2,1,0:T(8,128)(2,1)} custom-call(bf16[16,64,128]{2,1,0:T(8,128)(2,1)} %copy-done.2, f32[64,64]{1,0:T(8,128)} %dynamic-slice_bitcast_fusion.start_ref), custom_call_target="tpu_custom_call" | custom-call | flops 16777216 | bytes 524288 | tf_op jit(solution)/shard_map/states_ahead/pallas_call | solution.py:301
  194.4 28.2 %all-to-all-done.1.blocks_ref = bf16[16,192,128]{2,1,0:T(8,128)(2,1)S(1)} async-done(((bf16[16,192,128]{2,1,0:T(8,128)(2,1)}), bf16[16,192,128]{2,1,0:T(8,128)(2,1)S(1)}, u32[]{:S(2)}, u32[]{:S(2)}) %all-to-all-start.1) | async-done | bytes 786464 | tf_op jit(solution)/shard_map/all_to_all | solution.py:464
  222.6 0.9 copy-done.3
  223.5 7.1 %attention.1 = bf16[16,64,128]{2,1,0:T(8,128)(2,1)} custom-call(bf16[16,192,128]{2,1,0:T(8,128)(2,1)} %copy-done.3, f32[1,2048]{1,0:T(1,128)} %dynamic-slice_bitcast_fusion.1.gate_ref), custom_call_target="tpu_custom_call" | custom-call | flops 1073741824 | bytes 1572864 | tf_op jit(solution)/shard_map/attention/pallas_call | solution.py:86
  230.5 1.7 pad_maximum_fusion.2
  232.3 12.1 %all-to-all-start.3 = ((bf16[16,96,128]{2,1,0:T(8,128)(2,1)}), bf16[16,96,128]{2,1,0:T(8,128)(2,1)S(1)}, u32[]{:S(2)}, u32[]{:S(2)}) async-start(bf16[16,96,128]{2,1,0:T(8,128)(2,1)} %pad_maximum_fusion.2), calls=%async_computation.3 | async-start | bytes 786432 | tf_op jit(solution)/shard_map/all_to_all | solution.py:471
  244.5 0.6 reshape.50.gain_ref
  245.1 17.1 %all-to-all-done.3.back_ref = bf16[16,96,128]{2,1,0:T(8,128)(2,1)S(1)} async-done(((bf16[16,96,128]{2,1,0:T(8,128)(2,1)}), bf16[16,96,128]{2,1,0:T(8,128)(2,1)S(1)}, u32[]{:S(2)}, u32[]{:S(2)}) %all-to-all-start.3) | async-done | bytes 393248 | tf_op jit(solution)/shard_map/all_to_all | solution.py:471
  262.2 0.7 copy-done.1
  262.9 7.0 %closing.1 = bf16[256,2048]{1,0:T(8,128)(2,1)} custom-call(bf16[16,96,128]{2,1,0:T(8,128)(2,1)} %copy-done.1, bf16[256,512]{1,0:T(8,128)(2,1)} %get-tuple-element.9.q_ref, f32[256,512]{1,0:T(8,128)} %get-tuple-element.10.o_ref, bf16[1,512]{1,0:T(2,128)(2,1)} %reshape.50.gain_ref, bf16[2048,512]{1,0:T(8,128)(2,1)} %fox_w_ref.1, bf16[2048,512]{1,0:T(8,128)(2,1)} %lin_w_ref.1), custom_call_target="tpu_custom_call" | custom-call | flops 1073741824 | bytes 5242880 | tf_op jit(solution)/shard_map/closing/pallas_call | solution.py:366
  269.9 12.2 %all_to_all.25 = bf16[2,128,2048]{2,1,0:T(8,128)(2,1)S(1)} all-to-all(bf16[2,128,2048]{2,1,0:T(8,128)(2,1)} %bitcast.32), channel_id=1, replica_groups=mesh['grp'=2,'sp'=16,'fs'=4,'tp'=2] {'tp'}, dimensions={0} | all-to-all | bytes 2097152 | tf_op jit(solution)/shard_map/all_to_all | solution.py:474
  282.1 1.1 reduce_sum.24
  (45 shorter events, 1.0 us)
Async XLA Ops:
  6.5 32.2 %copy-start = (bf16[2048,128]{1,0:T(8,128)(2,1)S(1)}, bf16[2048,128]{1,0:T(8,128)(2,1)}, u32[]{:S(2)}) copy-start(bf16[2048,128]{1,0:T(8,128)(2,1)} %param.33) | copy-start | bytes 1572868
  6.6 3.0 %copy-start.6 = (bf16[512,512]{1,0:T(8,128)(2,1)S(1)}, bf16[512,512]{1,0:T(8,128)(2,1)}, u32[]{:S(2)}) copy-start(bf16[512,512]{1,0:T(8,128)(2,1)} %param.24) | copy-start | bytes 1572868
  6.6 3.0 %copy-start.7 = (bf16[512,512]{1,0:T(8,128)(2,1)S(1)}, bf16[512,512]{1,0:T(8,128)(2,1)}, u32[]{:S(2)}) copy-start(bf16[512,512]{1,0:T(8,128)(2,1)} %param.23) | copy-start | bytes 1572868
  6.6 3.0 %copy-start.8 = (bf16[512,512]{1,0:T(8,128)(2,1)S(1)}, bf16[512,512]{1,0:T(8,128)(2,1)}, u32[]{:S(2)}) copy-start(bf16[512,512]{1,0:T(8,128)(2,1)} %param.22) | copy-start | bytes 1572868
  6.6 89.2 %all-gather.5.cloned.1.call-start = ((), (), s32[]{:S(2)}) async-start(), calls=%async_computation.6 | async-start | bytes 7864320 | tf_op jit(solution)/shard_map/all_gather | solution.py:391
  9.5 1.5 copy-start.4
  9.5 160.5 %all-gather.3.cloned.1.call-start = ((), (), s32[]{:S(2)}) async-start(), calls=%async_computation.5 | async-start | bytes 7864320 | tf_op jit(solution)/shard_map/all_gather | solution.py:391
  11.1 25.2 %copy-start.10 = (bf16[2048]{0:T(1024)(128)(2,1)S(1)}, bf16[2048]{0:T(1024)(128)(2,1)}, u32[]{:S(2)}) copy-start(bf16[2048]{0:T(1024)(128)(2,1)} %param.21) | copy-start | bytes 12292
  11.1 25.2 %copy-start.9 = (f32[2,128,8]{1,2,0:T(8,128)S(1)}, f32[2,128,8]{1,2,0:T(8,128)}, u32[]{:S(2)}) copy-start(f32[2,128,8]{1,2,0:T(8,128)} %param.32) | copy-start | bytes 24580
  12.2 24.4 %copy-start.11 = (f32[1024]{0:T(1024)S(1)}, f32[1024]{0:T(1024)}, u32[]{:S(2)}) copy-start(f32[1024]{0:T(1024)} %param.31) | copy-start | bytes 12292
  12.2 24.5 %copy-start.12 = (f32[1024]{0:T(1024)S(1)}, f32[1024]{0:T(1024)}, u32[]{:S(2)}) copy-start(f32[1024]{0:T(1024)} %param.35) | copy-start | bytes 12292
  12.2 25.9 %all-to-all-start = ((bf16[2,256,1024]{1,2,0:T(8,128)(2,1)}), bf16[2,256,1024]{1,2,0:T(8,128)(2,1)S(1)}, u32[]{:S(2)}, u32[]{:S(2)}) async-start(bf16[2,256,1024]{1,2,0:T(8,128)(2,1)} %broadcast_in_dim.4), calls=%async_computation | async-start | bytes 2097152 | tf_op jit(solution)/shard_map/all_to_all | solution.py:429
  36.4 2.4 copy-start.15
  38.8 1.6 copy-start.14
  38.8 1.5 copy-start.16
  113.1 62.8 %all-to-all-start.2 = ((bf16[16,64,128]{2,1,0:T(8,128)(2,1)}), bf16[16,64,128]{2,1,0:T(8,128)(2,1)S(1)}, u32[]{:S(2)}, u32[]{:S(2)}) async-start(bf16[16,64,128]{2,1,0:T(8,128)(2,1)} %get-tuple-element.8), calls=%async_computation.2 | async-start | bytes 524288 | tf_op jit(solution)/shard_map/all_to_all | solution.py:469
  175.9 14.9 %copy-start.2 = (bf16[16,64,128]{2,1,0:T(8,128)(2,1)}, bf16[16,64,128]{2,1,0:T(8,128)(2,1)S(1)}, u32[]{:S(2)}) copy-start(bf16[16,64,128]{2,1,0:T(8,128)(2,1)S(1)} %all-to-all-done.2.maps_ref) | copy-start | bytes 786436
  175.9 46.7 %all-to-all-start.1 = ((bf16[16,192,128]{2,1,0:T(8,128)(2,1)}), bf16[16,192,128]{2,1,0:T(8,128)(2,1)S(1)}, u32[]{:S(2)}, u32[]{:S(2)}) async-start(bf16[16,192,128]{2,1,0:T(8,128)(2,1)} %bitcast.4), calls=%async_computation.1 | async-start | bytes 1572864 | tf_op jit(solution)/shard_map/all_to_all | solution.py:464
  194.4 36.1 %copy-start.5 = (bf16[16,32,128]{2,1,0:T(8,128)(2,1)S(1)}, bf16[16,32,128]{2,1,0:T(8,128)(2,1)}, u32[]{:S(2)}) copy-start(bf16[16,32,128]{2,1,0:T(8,128)(2,1)} %states_ahead.1) | copy-start | bytes 393220
  194.4 50.0 %copy-start.13 = (bf16[1024]{0:T(1024)(128)(2,1)S(1)}, bf16[1024]{0:T(1024)(128)(2,1)}, u32[]{:S(2)}) copy-start(bf16[1024]{0:T(1024)(128)(2,1)} %param.36) | copy-start | bytes 6148
  222.6 0.9 copy-start.3
  232.3 29.9 %all-to-all-start.3 = ((bf16[16,96,128]{2,1,0:T(8,128)(2,1)}), bf16[16,96,128]{2,1,0:T(8,128)(2,1)S(1)}, u32[]{:S(2)}, u32[]{:S(2)}) async-start(bf16[16,96,128]{2,1,0:T(8,128)(2,1)} %pad_maximum_fusion.2), calls=%async_computation.3 | async-start | bytes 786432 | tf_op jit(solution)/shard_map/all_to_all | solution.py:471
  262.2 0.7 copy-start.1
Sparse Core Ops, SparseCore 0:
  9.6 86.1 all-gather.4
  97.6 72.3 all-gather.2

commit v2 on v1

--- a/solution.py
+++ b/solution.py
@@ -32,7 +32,7 @@
     count, _, width = blocks_ref.shape
     channels = HEAD_CHANNELS
     for i in range(count):
-        gate = gate_ref[:, i * width : (i + 1) * width]
+        gate = gate_ref[i : i + 1, :]
         high = gate.astype(BF16).astype(F32)
         rest = gate - high
         middle = rest.astype(BF16).astype(F32)
@@ -108,11 +108,9 @@
     return row, col, same
 
 
-def maps_kernel(proj_ref, log_ref, rate_ref, q_ref, o_ref, maps_ref):
-    size = proj_ref.shape[0]
-    cols = log_ref.shape[1]
+def maps_kernel(proj_ref, log_ref, rate_ref, extra_ref, q_ref, o_ref, maps_ref):
+    seqs, _, size = extra_ref.shape
     lanes = 2 * HEAD_CHANNELS
-    pairs = cols // lanes
     row, col, same = chunk_masks(size)
     strict = same & (row > col)
     upto = same & (row >= col)
@@ -145,17 +143,20 @@
         )
 
     held = []
-    for p in range(pairs):
-        at = slice(p * lanes, (p + 1) * lanes)
-        rec = proj_ref[:, p * lanes : (p + 1) * lanes].astype(F32)
-        key = proj_ref[:, cols + p * lanes : cols + (p + 1) * lanes].astype(F32)
-        value = proj_ref[:, 2 * cols + p * lanes : 2 * cols + (p + 1) * lanes].astype(F32)
-        logged = log_ref[:, at]
+    for p in range(seqs):
+        at = slice(p * size, (p + 1) * size)
+        rec = proj_ref[at, :lanes].astype(F32)
+        key = proj_ref[at, lanes : 2 * lanes].astype(F32)
+        value = proj_ref[at, 2 * lanes :].astype(F32)
+        by_head = [
+            jnp.broadcast_to(extra_ref[p, k : k + 1, :], (HEAD_CHANNELS, size)) for k in range(2)
+        ]
+        logged = log_ref[at, :] + jnp.concatenate(by_head, 0).T
         squares = lax.dot_general(
             key * key, head_sum, MM, precision=lax.Precision.HIGHEST, preferred_element_type=F32
         )
         unit = key * lax.rsqrt(squares + 1e-06)
-        beta = unit * rate_ref[:, at]
+        beta = unit * rate_ref[at, :]
         total = lax.dot_general(
             running, logged, MM, precision=lax.Precision.HIGHEST, preferred_element_type=F32
         )
@@ -234,9 +235,9 @@
         later = mul(query[bottoms], jnp.concatenate(maps[0], 0), NT)
         query = jnp.concatenate((query[tops], later[:, :lanes]), 0)
         ready = jnp.concatenate((ready[tops], ready[bottoms] + later[:, lanes:]), 0)
-        at = slice(p * lanes, (p + 1) * lanes)
-        q_ref[:, at] = query.astype(BF16)
-        o_ref[:, at] = ready
+        at = slice(p * size, (p + 1) * size)
+        q_ref[at, :] = query.astype(BF16)
+        o_ref[at, :] = ready
         half = places((HEAD_CHANNELS, lanes), 1) < HEAD_CHANNELS
         turned_offset = pltpu.roll(offset, HEAD_CHANNELS, 1)
         turned_carry = pltpu.roll(carry, HEAD_CHANNELS, 1)
@@ -248,43 +249,43 @@
         ).astype(BF16)
 
 
-def position_maps(proj, logged, rate, tok_count):
-    rows, cols = logged.shape
-    seqs = rows // tok_count
-    heads = cols // HEAD_CHANNELS
-    lanes = 2 * HEAD_CHANNELS
+def position_maps(proj, logged, rate, extra):
+    seqs, heads, tok_count = extra.shape
+    rows, lanes = logged.shape
+    group = seqs // 2
     return pl.pallas_call(
         maps_kernel,
-        grid=(seqs,),
+        grid=(seqs // group,),
         out_shape=(
-            jax.ShapeDtypeStruct((rows, cols), BF16),
-            jax.ShapeDtypeStruct((rows, cols), F32),
+            jax.ShapeDtypeStruct((rows, lanes), BF16),
+            jax.ShapeDtypeStruct((rows, lanes), F32),
             jax.ShapeDtypeStruct((seqs * heads, HEAD_CHANNELS, lanes), BF16),
         ),
         in_specs=[
-            pl.BlockSpec((tok_count, 3 * cols), lambda s: (s, 0)),
-            pl.BlockSpec((tok_count, cols), lambda s: (s, 0)),
-            pl.BlockSpec((tok_count, cols), lambda s: (s, 0)),
+            pl.BlockSpec((group * tok_count, 3 * lanes), lambda s: (s, 0)),
+            pl.BlockSpec((group * tok_count, lanes), lambda s: (s, 0)),
+            pl.BlockSpec((group * tok_count, lanes), lambda s: (s, 0)),
+            pl.BlockSpec((group, heads, tok_count), lambda s: (s, 0, 0)),
         ],
         out_specs=(
-            pl.BlockSpec((tok_count, cols), lambda s: (s, 0)),
-            pl.BlockSpec((tok_count, cols), lambda s: (s, 0)),
-            pl.BlockSpec((heads, HEAD_CHANNELS, lanes), lambda s: (s, 0, 0)),
+            pl.BlockSpec((group * tok_count, lanes), lambda s: (s, 0)),
+            pl.BlockSpec((group * tok_count, lanes), lambda s: (s, 0)),
+            pl.BlockSpec((group * heads, HEAD_CHANNELS, lanes), lambda s: (s, 0, 0)),
         ),
         compiler_params=pltpu.CompilerParams(vmem_limit_bytes=VMEM_BYTES),
         cost_estimate=pl.CostEstimate(
-            flops=rows * cols * 2 * 256 * 20,
-            bytes_accessed=rows * cols * 20,
-            transcendentals=6 * rows * cols,
+            flops=rows * lanes * 2 * 256 * 20,
+            bytes_accessed=rows * lanes * 20,
+            transcendentals=6 * rows * lanes,
         ),
         name="position_maps",
-    )(proj, logged, rate)
+    )(proj, logged, rate, extra)
 
 
 def states_kernel(maps_ref, start_ref, out_ref):
     count = maps_ref.shape[0]
     n = HEAD_CHANNELS
-    state = start_ref[...]
+    state = jnp.concatenate((start_ref[:, :n], start_ref[:, n:]), 0)
     for i in range(count):
         out_ref[i] = jnp.concatenate((state[: n // 2], state[n // 2 :]), 1).astype(BF16)
         if i + 1 < count:
@@ -310,47 +311,157 @@
     )(maps, start)
 
 
-def closing_kernel(back_ref, q_ref, o_ref, gain_ref, fox_w_ref, lin_w_ref, out_ref, act_scr):
+def project_kernel(
+    both_ref,
+    gain_ref,
+    fox_w_ref,
+    lin_w_ref,
+    decay_low_ref,
+    rate_low_ref,
+    decay_up_ref,
+    rate_up_ref,
+    decay_base_ref,
+    rate_base_ref,
+    fox_ref,
+    lin_ref,
+    log_ref,
+    rate_ref,
+):
+    n = HEAD_CHANNELS
+    parts, rows, width = both_ref.shape
+    pairs, _, tok_count = fox_ref.shape
+    heads = pairs * tok_count // rows
+    lanes = heads * n
+    pieces = [both_ref[i].astype(F32) for i in range(parts)]
+    square = sum(jnp.sum(x * x, axis=1, keepdims=True) for x in pieces)
+    scaling = lax.rsqrt(square / (parts * width) + 1e-06)
+    normed = jnp.concatenate(
+        [
+            (x * scaling * gain_ref[:, i * width : (i + 1) * width].astype(F32)).astype(BF16)
+            for i, x in enumerate(pieces)
+        ],
+        1,
+    )
+
+    def project(weight_ref):
+        return lax.dot_general(normed, weight_ref[...], MM, preferred_element_type=F32)
+
+    fox = project(fox_w_ref)
+    for s in range(rows // tok_count):
+        here = slice(s * tok_count, (s + 1) * tok_count)
+        for k in range(3):
+            turned = fox[here, k * lanes : (k + 1) * lanes].T.astype(BF16)
+            for h in range(heads):
+                fox_ref[s * heads + h, k * n : (k + 1) * n, :] = turned[h * n : (h + 1) * n]
+    lin_ref[...] = project(lin_w_ref).astype(BF16)
+    decay_low = jnp.tanh(project(decay_low_ref))
+    decay = mul(decay_low, decay_up_ref[...]) + decay_base_ref[...]
+    log_ref[...] = jax.nn.sigmoid(decay) * -(2.718281828459045**-0.5)
+    rate = mul(project(rate_low_ref), rate_up_ref[...]) + rate_base_ref[...]
+    rate_ref[...] = jax.nn.sigmoid(rate)
+
+
+def projections(both, gain, fox_w, lin_w, lows, ups, bases, tok_count):
+    parts, rows, width = both.shape
+    lanes = fox_w.shape[1] // 3
+    heads = lanes // HEAD_CHANNELS
+    seqs = rows // tok_count
+    group = 2
+    whole = pl.BlockSpec(memory_space=pltpu.VMEM)
+    tall = group * tok_count
+    return pl.pallas_call(
+        project_kernel,
+        grid=(seqs // group,),
+        out_shape=(
+            jax.ShapeDtypeStruct((seqs * heads, 3 * HEAD_CHANNELS, tok_count), BF16),
+            jax.ShapeDtypeStruct((rows, 3 * lanes), BF16),
+            jax.ShapeDtypeStruct((rows, lanes), F32),
+            jax.ShapeDtypeStruct((rows, lanes), F32),
+        ),
+        in_specs=[pl.BlockSpec((parts, tall, width), lambda s: (0, s, 0))] + [whole] * 9,
+        out_specs=(
+            pl.BlockSpec((group * heads, 3 * HEAD_CHANNELS, tok_count), lambda s: (s, 0, 0)),
+            pl.BlockSpec((tall, 3 * lanes), lambda s: (s, 0)),
+            pl.BlockSpec((tall, lanes), lambda s: (s, 0)),
+            pl.BlockSpec((tall, lanes), lambda s: (s, 0)),
+        ),
+        compiler_params=pltpu.CompilerParams(vmem_limit_bytes=VMEM_BYTES),
+        cost_estimate=pl.CostEstimate(
+            flops=16 * rows * parts * width * lanes,
+            bytes_accessed=2 * (rows + 8 * lanes) * parts * width,
+            transcendentals=3 * rows * lanes,
+        ),
+        name="projections",
+    )(both, gain, fox_w, lin_w, *lows, *ups, *bases)
+
+
+def heads_kernel(back_ref, q_ref, o_ref, gain_ref, out_ref):
     n = HEAD_CHANNELS
     lanes = 2 * n
-    rows, cols = q_ref.shape
-    count, _, tok_count = back_ref.shape
-    heads = cols // n
-    seqs = rows // tok_count
+    pairs, _, tok_count = back_ref.shape
+    groups, rows, _ = out_ref.shape
+    head_block = (places((lanes, lanes), 0) < n) == (places((lanes, lanes), 1) < n)
+    average = jnp.where(head_block, 1.0 / n, 0.0).astype(BF16)
+    first = places((n // 2, lanes), 1) < n
+    gain = gain_ref[...].astype(F32)
+
+    def mean(values):
+        high = values.astype(BF16)
+        low = (values - high.astype(F32)).astype(BF16)
+        return mul(high, average) + mul(low, average)
+
+    raws = []
+    for s in range(pairs // 2):
+        here = slice(s * tok_count, (s + 1) * tok_count)
+        group, at = s * tok_count // rows, s * tok_count % rows
+        fox = jnp.concatenate((back_ref[2 * s, :n, :], back_ref[2 * s + 1, :n, :]), 0)
+        out_ref[group, at : at + tok_count, :lanes] = fox.astype(F32).T.astype(BF16)
+        packed = [back_ref[2 * s + k, n:, :].astype(F32) for k in range(2)]
+        turned = [pltpu.roll(x, n, 1) for x in packed]
+        state = jnp.concatenate(
+            (
+                jnp.where(first, packed[0], 0.0),
+                jnp.where(first, turned[0], 0.0),
+                jnp.where(first, 0.0, turned[1]),
+                jnp.where(first, 0.0, packed[1]),
+            ),
+            0,
+        )
+        raws.append(mul(q_ref[here, :], state, NT) + o_ref[here, :])
+    centred = [raw - mean(raw) for raw in raws]
+    spreads = [mean(x * x) for x in centred]
+    for s, (x, spread) in enumerate(zip(centred, spreads)):
+        group, at = s * tok_count // rows, s * tok_count % rows
+        lin = x * lax.rsqrt(spread + 0.00064) * gain
+        out_ref[group, at : at + tok_count, lanes:] = lin.astype(BF16)
+
+
+def heads_out(back, query, ready, gain, groups):
+    rows, lanes = query.shape
+    whole = pl.BlockSpec(memory_space=pltpu.VMEM)
+    return pl.pallas_call(
+        heads_kernel,
+        out_shape=jax.ShapeDtypeStruct((groups, rows // groups, 2 * lanes), BF16),
+        in_specs=[whole] * 4,
+        out_specs=whole,
+        compiler_params=pltpu.CompilerParams(vmem_limit_bytes=VMEM_BYTES),
+        cost_estimate=pl.CostEstimate(
+            flops=10 * rows * lanes * lanes, bytes_accessed=12 * rows * lanes, transcendentals=0
+        ),
+        name="heads_out",
+    )(back, query, ready, gain)
+
+
+def closing_kernel(acts_ref, fox_w_ref, lin_w_ref, out_ref, act_scr):
+    groups, rows, both = acts_ref.shape
+    lanes = both // 2
+    cols = groups * lanes
 
     @pl.when(pl.program_id(0) == 0)
     def _():
-        head_block = (places((lanes, lanes), 0) < n) == (places((lanes, lanes), 1) < n)
-        average = jnp.where(head_block, 1.0 / n, 0.0).astype(BF16)
-        first = places((n // 2, lanes), 1) < n
-
-        def mean(values):
-            high = values.astype(BF16)
-            low = (values - high.astype(F32)).astype(BF16)
-            return mul(high, average) + mul(low, average)
-
-        for s in range(seqs):
-            here = slice(s * tok_count, (s + 1) * tok_count)
-            for p in range(heads // 2):
-                at = slice(p * lanes, (p + 1) * lanes)
-                j = s * heads + 2 * p
-                fox = jnp.concatenate((back_ref[j, :n, :], back_ref[j + 1, :n, :]), 0)
-                act_scr[here, at] = fox.astype(F32).T.astype(BF16)
-                parts = []
-                for k in range(2):
-                    packed = back_ref[j + k, n:, :].astype(F32)
-                    turned = pltpu.roll(packed, n, 1)
-                    upper, lower = (packed, turned) if k == 0 else (turned, packed)
-                    if k == 0:
-                        parts += [jnp.where(first, packed, 0.0), jnp.where(first, turned, 0.0)]
-                    else:
-                        parts += [jnp.where(first, 0.0, turned), jnp.where(first, 0.0, packed)]
-                state = jnp.concatenate(parts, 0)
-                raw = mul(q_ref[here, at], state, NT) + o_ref[here, at]
-                centred = raw - mean(raw)
-                spread = mean(centred * centred)
-                lin = centred * lax.rsqrt(spread + 0.00064) * gain_ref[:, at].astype(F32)
-                act_scr[here, slice(cols + p * lanes, cols + (p + 1) * lanes)] = lin.astype(BF16)
+        for g in range(groups):
+            act_scr[:, g * lanes : (g + 1) * lanes] = acts_ref[g, :, :lanes]
+            act_scr[:, cols + g * lanes : cols + (g + 1) * lanes] = acts_ref[g, :, lanes:]
 
     out_ref[...] = (
         lax.dot_general(act_scr[:, :cols], fox_w_ref[...], NT, preferred_element_type=F32)
@@ -358,20 +469,16 @@
     ).astype(BF16)
 
 
-def closing(back, query, ready, gain, fox_w, lin_w):
-    rows, cols = query.shape
-    width = fox_w.shape[0]
+def closing(acts, fox_w, lin_w):
+    groups, rows, both = acts.shape
+    width, cols = fox_w.shape
     tile = 512
-    whole = pl.BlockSpec(memory_space=pltpu.VMEM)
     return pl.pallas_call(
         closing_kernel,
         grid=(width // tile,),
         out_shape=jax.ShapeDtypeStruct((rows, width), BF16),
         in_specs=[
-            whole,
-            whole,
-            whole,
-            whole,
+            pl.BlockSpec(memory_space=pltpu.VMEM),
             pl.BlockSpec((tile, cols), lambda i: (i, 0)),
             pl.BlockSpec((tile, cols), lambda i: (i, 0)),
         ],
@@ -384,11 +491,28 @@
             transcendentals=0,
         ),
         name="closing",
-    )(back, query, ready, gain, fox_w, lin_w)
-
-
-def gathered(arrays, axis):
-    return lax.all_gather(jnp.concatenate(arrays, axis=1), axis, axis=0, tiled=True)
+    )(acts, fox_w, lin_w)
+
+
+def exchange(x, axis):
+    return lax.all_to_all(x, axis, 0, 0, tiled=True)
+
+
+def from_everyone(x, axis):
+    return exchange(jnp.broadcast_to(x, (lax.axis_size(axis), *x.shape)), axis)
+
+
+def own_weights(arrays, axis):
+    groups = lax.axis_size(axis)
+    rows, cols = arrays[0].shape
+    lanes = cols // groups
+    sent = jnp.stack(
+        [
+            jnp.concatenate([a[:, g * lanes : (g + 1) * lanes] for a in arrays], 1)
+            for g in range(groups)
+        ]
+    )
+    return exchange(sent, axis).reshape(groups * rows, len(arrays) * lanes)
 
 
 def per_device(
@@ -417,63 +541,65 @@
     seq_count, tok_count, half_width = inputs.shape
     rows = seq_count * tok_count
     cols = softmax_query_matrix.shape[1]
-    heads = cols // n
+    groups, tp = lax.axis_size("fs"), lax.axis_size("tp")
+    lanes = cols // groups
+    heads = lanes // n
+    seqs = groups * seq_count
+    length = running_forget_gate.shape[1]
     place = lax.axis_index("sp")
-    col_start = lax.axis_index("tp") * cols
-
-    fox_w = gathered((softmax_query_matrix, softmax_key_matrix, softmax_value_matrix), "fs")
-    lin_w = gathered((receptance_weight, linear_key_weight, linear_value_weight), "fs")
-
-    flat = inputs.reshape(rows, half_width)
-    tp = lax.axis_size("tp")
-    both = lax.all_to_all(
-        jnp.broadcast_to(flat, (tp, rows, half_width)), "tp", 0, 0, tiled=True
-    )
-    whole = jnp.moveaxis(both, 0, 1).reshape(rows, tp * half_width).astype(F32)
-    scaling = lax.rsqrt(jnp.mean(whole * whole, axis=-1, keepdims=True) + 1e-06)
-    normed = (whole * scaling * input_norm_gain.astype(F32)).astype(BF16)
-
-    def project(weight):
-        return jnp.dot(normed, weight, preferred_element_type=F32)
+    col_start = lax.axis_index("tp") * cols + lax.axis_index("fs") * lanes
+
+    mine = from_everyone(inputs.reshape(rows, half_width), "fs")
+    fox_w = own_weights((softmax_query_matrix, softmax_key_matrix, softmax_value_matrix), "fs")
+    lin_w = own_weights((receptance_weight, linear_key_weight, linear_value_weight), "fs")
+
+    pair_seq, pair_head = place // heads, lax.rem(place, heads)
+    pair_group, pair_slot = pair_seq // seq_count, lax.rem(pair_seq, seq_count)
+
+    def of_pair(table, head_dim):
+        table = lax.dynamic_index_in_dim(table, pair_slot, 0, False)
+        shape = table.shape
+        table = table.reshape(*shape[:head_dim], groups, heads, *shape[head_dim + 1 :])
+        return lax.dynamic_index_in_dim(table, pair_head, head_dim + 1, False)
+
+    state = of_pair(starting_state, 0)
+    state = jnp.concatenate((state[:, : n // 2], state[:, n // 2 :]), 2)
+    gates = of_pair(running_forget_gate, 1).T.reshape(groups, length // tok_count, tok_count)
+    extra = decay_extra_log.reshape(seq_count, tok_count, groups, heads).transpose(2, 0, 3, 1)
+    extra = extra.reshape(groups, seq_count * heads, tok_count)
+    small = exchange(jnp.concatenate((state, gates, extra), 1), "fs")
+    half, after = n // 2, n // 2 + length // tok_count
+    extra = small[:, after:].reshape(seqs, heads, tok_count)
+    pair = lax.dynamic_index_in_dim(small, pair_group, 0, False)
+    start, gate = pair[:half], pair[half:after]
 
     def own_columns(table, axis):
-        return lax.dynamic_slice_in_dim(table, col_start, cols, axis)
-
-    decay_low = jnp.tanh(project(decay_lower_map)).astype(BF16)
-    decay_preact = own_columns(decay_offset_base, 0) + jnp.dot(
-        decay_low, own_columns(decay_upper_map, 1), preferred_element_type=F32
-    )
-    extra = jnp.repeat(decay_extra_log.reshape(rows, heads), n, axis=1)
-    decay_logged = -jnp.exp(-jax.nn.softplus(-decay_preact) - 0.5) + extra
-    rate_low = project(rate_lower_map).astype(BF16)
-    rate = jax.nn.sigmoid(
-        own_columns(rate_offset_base, 0)
-        + jnp.dot(rate_low, own_columns(rate_upper_map, 1), preferred_element_type=F32)
-    )
-    gate_rows = running_forget_gate.transpose(0, 2, 1).reshape(seq_count * heads, 1, -1)
-    gate = lax.dynamic_index_in_dim(gate_rows, place, 0, False)
-    start = lax.dynamic_index_in_dim(
-        starting_state.reshape(seq_count * heads, n, n), place, 0, False
-    )
-
-    fox = lax.dot_general(
-        fox_w, normed, (((0,), (1,)), ((), ())), preferred_element_type=F32
-    ).astype(BF16)
-    fox = fox.reshape(3, heads, n, seq_count, tok_count).transpose(3, 1, 0, 2, 4)
-    fox = fox.reshape(seq_count * heads, 3 * n, tok_count)
-    fox = lax.all_to_all(fox, "sp", 0, 0, tiled=True)
+        return lax.dynamic_slice_in_dim(table, col_start, lanes, axis)
+
+    both = from_everyone(mine.reshape(seqs * tok_count, half_width), "tp")
+    fox, lin, logged, rate = projections(
+        both,
+        input_norm_gain.reshape(1, -1),
+        fox_w,
+        lin_w,
+        (decay_lower_map, rate_lower_map),
+        (own_columns(decay_upper_map, 1), own_columns(rate_upper_map, 1)),
+        (
+            own_columns(decay_offset_base, 0).reshape(1, lanes),
+            own_columns(rate_offset_base, 0).reshape(1, lanes),
+        ),
+        tok_count,
+    )
+    fox = exchange(fox, "sp")
+    query, ready, maps = position_maps(lin, logged, rate, extra)
+    maps = exchange(maps, "sp")
     fox_out = attention(fox, gate)
-
-    lin = project(lin_w).astype(BF16)
-    query, ready, maps = position_maps(lin, decay_logged, rate, tok_count)
-    maps = lax.all_to_all(maps, "sp", 0, 0, tiled=True)
     states = states_ahead(maps, start)
-    back = lax.all_to_all(jnp.concatenate((fox_out, states), 1), "sp", 0, 0, tiled=True)
-    gain = own_columns(linear_head_gain, 0).reshape(1, cols)
-    partial = closing(back, query, ready, gain, softmax_output_weight, linear_output_weight)
-    pieces = lax.all_to_all(
-        partial.reshape(seq_count, tok_count, -1), "tp", 0, 0, tiled=True
-    )
+    back = exchange(jnp.concatenate((fox_out, states), 1), "sp")
+    gain = own_columns(linear_head_gain, 0).reshape(1, lanes)
+    acts = exchange(heads_out(back, query, ready, gain, groups), "fs")
+    partial = closing(acts, softmax_output_weight, linear_output_weight)
+    pieces = exchange(partial.reshape(seq_count, tok_count, -1), "tp")
     mixed = jnp.sum(
         pieces.reshape(tp, seq_count // tp, tok_count, -1).astype(F32), axis=0
     )

time: 291 us -> 280 us (0.962)
  blocking collectives: 12.2 us -> 101 us
  waiting for transfers between devices: 145 us -> 78.6 us
  starting transfers between devices: 60.6 us -> 36.2 us
  Pallas kernels: 29.5 us -> 43 us
  matrix products: 13.4 us -> 0 us
  between operations: 13.6 us -> 0.33 us
  local copies, waits for them, and re-layouts: 8.08 us -> 13.4 us
    all_gather x2 -> x0, waiting for transfers between devices: 98.5 us -> none  [gathered(): lax.all_gather(jnp.concatenate(arrays, axis=1), axis, axis=0, tiled=True)]
    all_to_all x1 -> x5, blocking collectives: 12.2 us -> 101 us  [exchange(): return lax.all_to_all(x, axis, 0, 0, tiled=True)]
    all_to_all x4 -> x5, waiting for transfers between devices: 46.6 us -> 78.6 us  [exchange(): return lax.all_to_all(x, axis, 0, 0, tiled=True)]
    all_to_all x4 -> x5, starting transfers between devices: 60.5 us -> 36.2 us  [exchange(): return lax.all_to_all(x, axis, 0, 0, tiled=True)]
    pallas_call x1 -> x3, Pallas kernels: 11.8 us -> 27.1 us  [the longest x1 12.4 us: projections(): pl.pallas_call(project_kernel, grid=(seqs // group,), out_shape=(jax.Shap...]
    dot_general x4 -> x0, matrix products: 13.4 us -> none  [the longest x1 5.49 us: project(): return jnp.dot(normed, weight, preferred_element_type=F32)]
    concatenate x3 -> x2, other arithmetic: 5.78 us -> 2.46 us  [the longest x1 1.72 us: per_device(): back = exchange(jnp.concatenate((fox_out, states), 1), 'sp')]
  transfers between devices with their start and end apart: 6 -> 5, of which waited for: 5 -> 5; matrix products, arithmetic and copies ran while one was open for 7% -> 3% of each run, Pallas kernels for 5% -> 1%
where the time goes in v2:
time: 280 us; the launch traced here: 279 us
  blocking collectives  101 us (36%)
  waiting for transfers between devices  78.6 us (28%)
  Pallas kernels  43 us (15%)
  starting transfers between devices  36.2 us (13%)
  local copies, waits for them, and re-layouts  13.4 us (5%)
  other arithmetic  5.67 us (2%)
    all_to_all x5, blocking collectives, exchange(): return lax.all_to_all(x, axis, 0, 0, tiled=True)  101 us
    all_to_all x5, waiting for transfers between devices, exchange(): return lax.all_to_all(x, axis, 0, 0, tiled=True)  78.6 us
    all_to_all x5, starting transfers between devices, exchange(): return lax.all_to_all(x, axis, 0, 0, tiled=True)  36.2 us
    pallas_call x1, Pallas kernels, projections(): pl.pallas_call(project_kernel, grid=(seqs // group,), out_shape=(jax.Shap...  12.4 us
    pallas_call x1, Pallas kernels, position_maps(): pl.pallas_call(maps_kernel, grid=(seqs // group,), out_shape=(jax.ShapeDt...  11.9 us
    pallas_call x1, Pallas kernels, attention(): pl.pallas_call(attention_kernel, out_shape=jax.ShapeDtypeStruct((count, H...  7.08 us
  transfers between devices with their start and end apart: 5, of which 5 were waited for; matrix products, arithmetic and copies ran while one was open for 3% of the time, Pallas kernels for 1%

profile of v2, /device:TPU:33, one launch (start us, length us, event | category | flops | bytes accessed | tf_op | source)
XLA Modules:
  0.0 278.6 jit_solution(13075316629114135256)
XLA Ops:
  0.0 0.8 copy.22
  0.8 0.8 constant_dynamic-slice_fusion.1
  2.7 5.1 %all-to-all-start.5 = ((f32[4,52,128]{2,1,0:T(8,128)}), f32[4,52,128]{2,1,0:T(8,128)S(1)}, u32[]{:S(2)}, u32[]{:S(2)}) async-start(f32[4,52,128]{2,1,0:T(8,128)} %pad_maximum_fusion.3), calls=%async_computation.5 | async-start | bytes 229376 | tf_op jit(solution)/shard_map/all_to_all | solution.py:498
  8.3 1.4 pad_maximum_fusion
  9.8 2.8 all-to-all-done.5
  12.5 4.4 %all-to-all-start.2 = ((bf16[4,512,384]{2,1,0:T(8,128)(2,1)}), bf16[4,512,384]{2,1,0:T(8,128)(2,1)}, u32[]{:S(2)}, u32[]{:S(2)}) async-start(bf16[4,512,384]{2,1,0:T(8,128)(2,1)} %pad_maximum_fusion), calls=%async_computation.2 | async-start | bytes 3145728 | tf_op jit(solution)/shard_map/all_to_all | solution.py:498
  17.2 0.8 copy-done.9
  18.6 10.9 %all-to-all-done.2 = bf16[4,512,384]{2,1,0:T(8,128)(2,1)} async-done(((bf16[4,512,384]{2,1,0:T(8,128)(2,1)}), bf16[4,512,384]{2,1,0:T(8,128)(2,1)}, u32[]{:S(2)}, u32[]{:S(2)}) %all-to-all-start.2) | async-done | bytes 1572896 | tf_op jit(solution)/shard_map/all_to_all | solution.py:498
  29.5 19.7 %all_to_all.50 = bf16[4,512,384]{2,1,0:T(8,128)(2,1)} all-to-all(bf16[4,512,384]{2,1,0:T(8,128)(2,1)S(1)} %pad_maximum_fusion.1), channel_id=1, replica_groups=mesh['grp'=2,'sp'=16,'fs'=4,'tp'=2] {'fs'}, dimensions={0} | all-to-all | bytes 3145728 | tf_op jit(solution)/shard_map/all_to_all | solution.py:498
  49.3 1.6 broadcast_in_dim.6
  50.9 3.8 %all-to-all-start = ((bf16[4,256,1024]{2,1,0:T(8,128)(2,1)}), bf16[4,256,1024]{2,1,0:T(8,128)(2,1)S(1)}, u32[]{:S(2)}, u32[]{:S(2)}) async-start(bf16[4,256,1024]{2,1,0:T(8,128)(2,1)} %broadcast_in_dim.6), calls=%async_computation | async-start | bytes 4194304 | tf_op jit(solution)/shard_map/all_to_all | solution.py:498
  55.3 1.3 dynamic-slice_bitcast_fusion.4
  56.6 1.4 constant_dynamic-slice_fusion.3
  58.6 19.3 %all-to-all-done = bf16[4,256,1024]{2,1,0:T(8,128)(2,1)S(1)} async-done(((bf16[4,256,1024]{2,1,0:T(8,128)(2,1)}), bf16[4,256,1024]{2,1,0:T(8,128)(2,1)S(1)}, u32[]{:S(2)}, u32[]{:S(2)}) %all-to-all-start) | async-done | bytes 2097184 | tf_op jit(solution)/shard_map/all_to_all | solution.py:498
  78.5 31.0 %all_to_all.51.both_ref = bf16[2,1024,1024]{2,1,0:T(8,128)(2,1)} all-to-all(bf16[2,1024,1024]{2,1,0:T(8,128)(2,1)S(1)} %broadcast_in_dim.7), channel_id=1, replica_groups=mesh['grp'=2,'sp'=16,'fs'=4,'tp'=2] {'tp'}, dimensions={0} | all-to-all | bytes 8388608 | tf_op jit(solution)/shard_map/all_to_all | solution.py:498
  109.4 12.4 %projections.1 = (bf16[16,192,128]{2,1,0:T(8,128)(2,1)}, bf16[1024,384]{1,0:T(8,128)(2,1)}, f32[1024,128]{1,0:T(8,128)}, f32[1024,128]{1,0:T(8,128)}) custom-call(bf16[2,1024,1024]{2,1,0:T(8,128)(2,1)} %all_to_all.51.both_ref, bf16[1,2048]{1,0:T(2,128)(2,1)} %reshape.53.gain_ref, bf16[2048,384]{1,0:T(8,128)(2,1)} %bitcast.6.fox_w_ref, ...), custom_call_target="tpu_custom_call" | custom-call | flops 4294967296 | bytes 8388608 | tf_op jit(solution)/shard_map/projections/pallas_call | solution.py:372
  121.8 11.9 %position_maps.1 = (bf16[1024,128]{1,0:T(8,128)(2,1)}, f32[1024,128]{1,0:T(8,128)}, bf16[16,64,128]{2,1,0:T(8,128)(2,1)}) custom-call(bf16[1024,384]{1,0:T(8,128)(2,1)} %get-tuple-element.13.proj_ref, f32[1024,128]{1,0:T(8,128)} %get-tuple-element.14.log_ref, f32[1024,128]{1,0:T(8,128)} %get-tuple-element.15.rate_ref, f32[8,2,128]{2,1,0:T(2,128)} %bitcast.60), custom_call_target="tpu_custom_call" | custom-call | flops 1342177280 | bytes 2621440 | tf_op jit(solution)/shard_map/position_maps/pallas_call | solution.py:256
  133.7 25.8 %all_to_all.52.maps_ref = bf16[16,64,128]{2,1,0:T(8,128)(2,1)} all-to-all(bf16[16,64,128]{2,1,0:T(8,128)(2,1)} %get-tuple-element.16), channel_id=1, replica_groups=mesh['grp'=2,'sp'=16,'fs'=4,'tp'=2] {'sp'}, dimensions={0} | all-to-all | bytes 524288 | tf_op jit(solution)/shard_map/all_to_all | solution.py:498
  159.5 10.4 %all-to-all-start.4 = ((bf16[16,192,128]{2,1,0:T(8,128)(2,1)}), bf16[16,192,128]{2,1,0:T(8,128)(2,1)S(1)}, u32[]{:S(2)}, u32[]{:S(2)}) async-start(bf16[16,192,128]{2,1,0:T(8,128)(2,1)} %get-tuple-element.12), calls=%async_computation.4 | async-start | bytes 1572864 | tf_op jit(solution)/shard_map/all_to_all | solution.py:498
  171.2 3.7 %states_ahead.1 = bf16[16,32,128]{2,1,0:T(8,128)(2,1)} custom-call(bf16[16,64,128]{2,1,0:T(8,128)(2,1)} %all_to_all.52.maps_ref, f32[32,128]{1,0:T(8,128)} %dynamic-slice_bitcast_fusion.1.start_ref), custom_call_target="tpu_custom_call" | custom-call | flops 16777216 | bytes 524288 | tf_op jit(solution)/shard_map/states_ahead/pallas_call | solution.py:302
  174.8 29.5 %all-to-all-done.4.blocks_ref = bf16[16,192,128]{2,1,0:T(8,128)(2,1)S(1)} async-done(((bf16[16,192,128]{2,1,0:T(8,128)(2,1)}), bf16[16,192,128]{2,1,0:T(8,128)(2,1)S(1)}, u32[]{:S(2)}, u32[]{:S(2)}) %all-to-all-start.4) | async-done | bytes 786464 | tf_op jit(solution)/shard_map/all_to_all | solution.py:498
  204.4 0.9 copy-done.2
  205.3 7.1 %attention.1 = bf16[16,64,128]{2,1,0:T(8,128)(2,1)} custom-call(bf16[16,192,128]{2,1,0:T(8,128)(2,1)} %copy-done.2, f32[16,128]{1,0:T(8,128)} %dynamic-slice_bitcast_fusion.2.gate_ref), custom_call_target="tpu_custom_call" | custom-call | flops 1073741824 | bytes 1572864 | tf_op jit(solution)/shard_map/attention/pallas_call | solution.py:86
  212.3 1.7 pad_maximum_fusion.2
  214.1 12.4 %all-to-all-start.7 = ((bf16[16,96,128]{2,1,0:T(8,128)(2,1)}), bf16[16,96,128]{2,1,0:T(8,128)(2,1)S(1)}, u32[]{:S(2)}, u32[]{:S(2)}) async-start(bf16[16,96,128]{2,1,0:T(8,128)(2,1)} %pad_maximum_fusion.2), calls=%async_computation.7 | async-start | bytes 786432 | tf_op jit(solution)/shard_map/all_to_all | solution.py:498
  226.5 1.3 dynamic-slice_bitcast_fusion.3.gain_ref
  227.8 16.1 %all-to-all-done.7.back_ref = bf16[16,96,128]{2,1,0:T(8,128)(2,1)S(1)} async-done(((bf16[16,96,128]{2,1,0:T(8,128)(2,1)}), bf16[16,96,128]{2,1,0:T(8,128)(2,1)S(1)}, u32[]{:S(2)}, u32[]{:S(2)}) %all-to-all-start.7) | async-done | bytes 393248 | tf_op jit(solution)/shard_map/all_to_all | solution.py:498
  244.7 2.7 heads_out.1
  247.4 11.2 %all_to_all.53.acts_ref = bf16[4,256,256]{2,1,0:T(8,128)(2,1)} all-to-all(bf16[4,256,256]{2,1,0:T(8,128)(2,1)} %heads_out.1), channel_id=1, replica_groups=mesh['grp'=2,'sp'=16,'fs'=4,'tp'=2] {'fs'}, dimensions={0} | all-to-all | bytes 1048576 | tf_op jit(solution)/shard_map/all_to_all | solution.py:498
  258.6 5.2 %closing.1 = bf16[256,2048]{1,0:T(8,128)(2,1)} custom-call(bf16[4,256,256]{2,1,0:T(8,128)(2,1)} %all_to_all.53.acts_ref, bf16[2048,512]{1,0:T(8,128)(2,1)} %fox_w_ref.1, bf16[2048,512]{1,0:T(8,128)(2,1)} %lin_w_ref.1), custom_call_target="tpu_custom_call" | custom-call | flops 1073741824 | bytes 5242880 | tf_op jit(solution)/shard_map/closing/pallas_call | solution.py:476
  263.7 13.7 %all_to_all.54 = bf16[2,128,2048]{2,1,0:T(8,128)(2,1)S(1)} all-to-all(bf16[2,128,2048]{2,1,0:T(8,128)(2,1)} %bitcast.52), channel_id=1, replica_groups=mesh['grp'=2,'sp'=16,'fs'=4,'tp'=2] {'tp'}, dimensions={0} | all-to-all | bytes 2097152 | tf_op jit(solution)/shard_map/all_to_all | solution.py:498
  277.5 1.1 reduce_sum.14
  (46 shorter events, 5.8 us)
Async XLA Ops:
  0.0 1.8 copy-start
  0.0 7.8 %copy-start.4 = (bf16[512,512]{1,0:T(8,128)(2,1)S(1)}, bf16[512,512]{1,0:T(8,128)(2,1)}, u32[]{:S(2)}) copy-start(bf16[512,512]{1,0:T(8,128)(2,1)} %param.24) | copy-start | bytes 1572868
  0.0 7.9 %copy-start.5 = (bf16[512,512]{1,0:T(8,128)(2,1)S(1)}, bf16[512,512]{1,0:T(8,128)(2,1)}, u32[]{:S(2)}) copy-start(bf16[512,512]{1,0:T(8,128)(2,1)} %param.23) | copy-start | bytes 1572868
  1.9 6.1 %copy-start.6 = (bf16[512,512]{1,0:T(8,128)(2,1)S(1)}, bf16[512,512]{1,0:T(8,128)(2,1)}, u32[]{:S(2)}) copy-start(bf16[512,512]{1,0:T(8,128)(2,1)} %param.22) | copy-start | bytes 1572868
  2.7 9.9 %all-to-all-start.5 = ((f32[4,52,128]{2,1,0:T(8,128)}), f32[4,52,128]{2,1,0:T(8,128)S(1)}, u32[]{:S(2)}, u32[]{:S(2)}) async-start(f32[4,52,128]{2,1,0:T(8,128)} %pad_maximum_fusion.3), calls=%async_computation.5 | async-start | bytes 229376 | tf_op jit(solution)/shard_map/all_to_all | solution.py:498
  9.7 7.2 %copy-start.7 = (bf16[512,512]{1,0:T(8,128)(2,1)S(1)}, bf16[512,512]{1,0:T(8,128)(2,1)}, u32[]{:S(2)}) copy-start(bf16[512,512]{1,0:T(8,128)(2,1)} %param.28) | copy-start | bytes 1572868
  9.7 7.3 %copy-start.8 = (bf16[512,512]{1,0:T(8,128)(2,1)S(1)}, bf16[512,512]{1,0:T(8,128)(2,1)}, u32[]{:S(2)}) copy-start(bf16[512,512]{1,0:T(8,128)(2,1)} %param.27) | copy-start | bytes 1572868
  12.5 17.0 %all-to-all-start.2 = ((bf16[4,512,384]{2,1,0:T(8,128)(2,1)}), bf16[4,512,384]{2,1,0:T(8,128)(2,1)}, u32[]{:S(2)}, u32[]{:S(2)}) async-start(bf16[4,512,384]{2,1,0:T(8,128)(2,1)} %pad_maximum_fusion), calls=%async_computation.2 | async-start | bytes 3145728 | tf_op jit(solution)/shard_map/all_to_all | solution.py:498
  17.0 1.0 copy-start.9
  18.6 30.7 %copy-start.3 = (bf16[2,128,1024]{2,1,0:T(8,128)(2,1)S(1)}, bf16[2,128,1024]{2,1,0:T(8,128)(2,1)}, u32[]{:S(2)}) copy-start(bf16[2,128,1024]{2,1,0:T(8,128)(2,1)} %param.20) | copy-start | bytes 1572868
  50.9 3.8 %copy-start.11 = (bf16[2048]{0:T(1024)(128)(2,1)S(1)}, bf16[2048]{0:T(1024)(128)(2,1)}, u32[]{:S(2)}) copy-start(bf16[2048]{0:T(1024)(128)(2,1)} %param.21) | copy-start | bytes 12292
  50.9 27.0 %all-to-all-start = ((bf16[4,256,1024]{2,1,0:T(8,128)(2,1)}), bf16[4,256,1024]{2,1,0:T(8,128)(2,1)S(1)}, u32[]{:S(2)}, u32[]{:S(2)}) async-start(bf16[4,256,1024]{2,1,0:T(8,128)(2,1)} %broadcast_in_dim.6), calls=%async_computation | async-start | bytes 4194304 | tf_op jit(solution)/shard_map/all_to_all | solution.py:498
  159.5 44.8 %all-to-all-start.4 = ((bf16[16,192,128]{2,1,0:T(8,128)(2,1)}), bf16[16,192,128]{2,1,0:T(8,128)(2,1)S(1)}, u32[]{:S(2)}, u32[]{:S(2)}) async-start(bf16[16,192,128]{2,1,0:T(8,128)(2,1)} %get-tuple-element.12), calls=%async_computation.4 | async-start | bytes 1572864 | tf_op jit(solution)/shard_map/all_to_all | solution.py:498
  174.8 37.5 %copy-start.10 = (bf16[16,32,128]{2,1,0:T(8,128)(2,1)S(1)}, bf16[16,32,128]{2,1,0:T(8,128)(2,1)}, u32[]{:S(2)}) copy-start(bf16[16,32,128]{2,1,0:T(8,128)(2,1)} %states_ahead.1) | copy-start | bytes 393220
  204.4 0.9 copy-start.2
  214.1 29.9 %all-to-all-start.7 = ((bf16[16,96,128]{2,1,0:T(8,128)(2,1)}), bf16[16,96,128]{2,1,0:T(8,128)(2,1)S(1)}, u32[]{:S(2)}, u32[]{:S(2)}) async-start(bf16[16,96,128]{2,1,0:T(8,128)(2,1)} %pad_maximum_fusion.2), calls=%async_computation.7 | async-start | bytes 786432 | tf_op jit(solution)/shard_map/all_to_all | solution.py:498
  243.9 0.7 copy-start.1

commit v3 on v2

--- a/solution.py
+++ b/solution.py
@@ -311,30 +311,59 @@
     )(maps, start)
 
 
-def project_kernel(
-    both_ref,
-    gain_ref,
-    fox_w_ref,
-    lin_w_ref,
-    decay_low_ref,
-    rate_low_ref,
-    decay_up_ref,
-    rate_up_ref,
-    decay_base_ref,
-    rate_base_ref,
-    fox_ref,
-    lin_ref,
-    log_ref,
-    rate_ref,
-):
+def halves(weights):
+    rows = weights[0].shape[0] // 2
+    return [w[k * rows : (k + 1) * rows, :] for k in range(2) for w in weights]
+
+
+def pack_kernel(*refs):
+    out_ref = refs[-1]
+    at = 0
+    for piece in [r[...] for r in refs[:-4]] + halves([r[...] for r in refs[-4:-1]]):
+        out_ref[0, :, at : at + piece.shape[1]] = piece
+        at += piece.shape[1]
+
+
+def packed(leading, weights, groups):
+    rows, cols = weights[0].shape
+    lanes = cols // groups
+    width = sum(x.shape[1] for x in leading) + 6 * lanes
+    whole = pl.BlockSpec(memory_space=pltpu.VMEM)
+    return pl.pallas_call(
+        pack_kernel,
+        grid=(groups,),
+        out_shape=jax.ShapeDtypeStruct((groups, rows // 2, width), BF16),
+        in_specs=[whole] * len(leading) + [pl.BlockSpec((rows, lanes), lambda g: (0, g))] * 3,
+        out_specs=pl.BlockSpec((1, rows // 2, width), lambda g: (g, 0, 0)),
+        compiler_params=pltpu.CompilerParams(vmem_limit_bytes=VMEM_BYTES),
+        cost_estimate=pl.CostEstimate(
+            flops=1 << 20, bytes_accessed=4 * groups * rows * width, transcendentals=0
+        ),
+        name="packed",
+    )(*leading, *weights)
+
+
+def fox_kernel(at_ref, mine_ref, other_ref, gain_ref, fox_ref, normed_ref, weight_scr):
     n = HEAD_CHANNELS
-    parts, rows, width = both_ref.shape
+    groups, rows, width = other_ref.shape
     pairs, _, tok_count = fox_ref.shape
     heads = pairs * tok_count // rows
     lanes = heads * n
-    pieces = [both_ref[i].astype(F32) for i in range(parts)]
+    step = pl.program_id(0)
+
+    @pl.when(step == 0)
+    def _():
+        for i in range(groups):
+            source = lax.rem(i + at_ref[0] * (groups // 2), groups)
+            for k in range(2):
+                at = width + 3 * k * lanes
+                weight_scr[(2 * i + k) * rows : (2 * i + k + 1) * rows, :] = mine_ref[
+                    source, :, at : at + 3 * lanes
+                ]
+
+    pieces = [mine_ref[step, :, :width].astype(F32), other_ref[step].astype(F32)]
     square = sum(jnp.sum(x * x, axis=1, keepdims=True) for x in pieces)
-    scaling = lax.rsqrt(square / (parts * width) + 1e-06)
+    scaling = lax.rsqrt(square / (2 * width) + 1e-06)
     normed = jnp.concatenate(
         [
             (x * scaling * gain_ref[:, i * width : (i + 1) * width].astype(F32)).astype(BF16)
@@ -342,57 +371,104 @@
         ],
         1,
     )
-
-    def project(weight_ref):
-        return lax.dot_general(normed, weight_ref[...], MM, preferred_element_type=F32)
-
-    fox = project(fox_w_ref)
+    normed_ref[...] = normed
+    fox = lax.dot_general(normed, weight_scr[...], MM, preferred_element_type=F32)
     for s in range(rows // tok_count):
         here = slice(s * tok_count, (s + 1) * tok_count)
         for k in range(3):
             turned = fox[here, k * lanes : (k + 1) * lanes].T.astype(BF16)
             for h in range(heads):
                 fox_ref[s * heads + h, k * n : (k + 1) * n, :] = turned[h * n : (h + 1) * n]
-    lin_ref[...] = project(lin_w_ref).astype(BF16)
-    decay_low = jnp.tanh(project(decay_low_ref))
-    decay = mul(decay_low, decay_up_ref[...]) + decay_base_ref[...]
+
+
+def fox_projections(at, mine, other, gain, tok_count):
+    groups, rows, width = other.shape
+    lanes = (mine.shape[2] - width) // 6
+    heads = lanes // HEAD_CHANNELS
+    pairs = rows // tok_count * heads
+    whole = pl.BlockSpec(memory_space=pltpu.VMEM)
+    return pl.pallas_call(
+        fox_kernel,
+        grid=(groups,),
+        out_shape=(
+            jax.ShapeDtypeStruct((groups * pairs, 3 * HEAD_CHANNELS, tok_count), BF16),
+            jax.ShapeDtypeStruct((groups * rows, 2 * width), BF16),
+        ),
+        in_specs=[pl.BlockSpec(memory_space=pltpu.SMEM), whole, whole, whole],
+        out_specs=(
+            pl.BlockSpec((pairs, 3 * HEAD_CHANNELS, tok_count), lambda g: (g, 0, 0)),
+            pl.BlockSpec((rows, 2 * width), lambda g: (g, 0)),
+        ),
+        scratch_shapes=[pltpu.VMEM((2 * width, 3 * lanes), BF16)],
+        compiler_params=pltpu.CompilerParams(vmem_limit_bytes=VMEM_BYTES),
+        cost_estimate=pl.CostEstimate(
+            flops=12 * groups * rows * width * lanes,
+            bytes_accessed=8 * groups * rows * width,
+            transcendentals=0,
+        ),
+        name="fox_projections",
+    )(at, mine, other, gain)
+
+
+def lin_kernel(at_ref, normed_ref, low_ref, decay_up_ref, rate_up_ref, base_ref, *rest):
+    sent_refs, (lin_ref, log_ref, rate_ref, weight_scr) = rest[:-4], rest[-4:]
+    groups = len(sent_refs)
+    rows, both = sent_refs[0].shape
+    lanes = both // 6
+
+    @pl.when(pl.program_id(0) == 0)
+    def _():
+        for d, ref in enumerate(sent_refs):
+            source = lax.rem(at_ref[1] + (groups - d), groups)
+            place = lax.rem(source + at_ref[0] * (groups // 2), groups)
+            for k in range(2):
+                start = pl.multiple_of((2 * place + k) * rows, rows)
+                weight_scr[pl.ds(start, rows), :] = ref[:, 3 * k * lanes : 3 * (k + 1) * lanes]
+
+    normed = normed_ref[...]
+    lin_ref[...] = lax.dot_general(
+        normed, weight_scr[...], MM, preferred_element_type=F32
+    ).astype(BF16)
+    low = lax.dot_general(normed, low_ref[...], MM, preferred_element_type=F32)
+    inner = low.shape[1] // 2
+    decay = mul(jnp.tanh(low[:, :inner]), decay_up_ref[...]) + base_ref[0:1, :]
     log_ref[...] = jax.nn.sigmoid(decay) * -(2.718281828459045**-0.5)
-    rate = mul(project(rate_low_ref), rate_up_ref[...]) + rate_base_ref[...]
+    rate = mul(low[:, inner:], rate_up_ref[...]) + base_ref[1:2, :]
     rate_ref[...] = jax.nn.sigmoid(rate)
 
 
-def projections(both, gain, fox_w, lin_w, lows, ups, bases, tok_count):
-    parts, rows, width = both.shape
-    lanes = fox_w.shape[1] // 3
-    heads = lanes // HEAD_CHANNELS
-    seqs = rows // tok_count
-    group = 2
+def lin_projections(at, normed, low, decay_up, rate_up, bases, sent):
+    rows, width = normed.shape
+    lanes = sent[0].shape[1] // 6
+    tall = rows // 4
     whole = pl.BlockSpec(memory_space=pltpu.VMEM)
-    tall = group * tok_count
     return pl.pallas_call(
-        project_kernel,
-        grid=(seqs // group,),
+        lin_kernel,
+        grid=(rows // tall,),
         out_shape=(
-            jax.ShapeDtypeStruct((seqs * heads, 3 * HEAD_CHANNELS, tok_count), BF16),
             jax.ShapeDtypeStruct((rows, 3 * lanes), BF16),
             jax.ShapeDtypeStruct((rows, lanes), F32),
             jax.ShapeDtypeStruct((rows, lanes), F32),
         ),
-        in_specs=[pl.BlockSpec((parts, tall, width), lambda s: (0, s, 0))] + [whole] * 9,
+        in_specs=[
+            pl.BlockSpec(memory_space=pltpu.SMEM),
+            pl.BlockSpec((tall, width), lambda s: (s, 0)),
+        ]
+        + [whole] * (4 + len(sent)),
         out_specs=(
-            pl.BlockSpec((group * heads, 3 * HEAD_CHANNELS, tok_count), lambda s: (s, 0, 0)),
             pl.BlockSpec((tall, 3 * lanes), lambda s: (s, 0)),
             pl.BlockSpec((tall, lanes), lambda s: (s, 0)),
             pl.BlockSpec((tall, lanes), lambda s: (s, 0)),
         ),
+        scratch_shapes=[pltpu.VMEM((width, 3 * lanes), BF16)],
         compiler_params=pltpu.CompilerParams(vmem_limit_bytes=VMEM_BYTES),
         cost_estimate=pl.CostEstimate(
-            flops=16 * rows * parts * width * lanes,
-            bytes_accessed=2 * (rows + 8 * lanes) * parts * width,
+            flops=10 * rows * width * lanes,
+            bytes_accessed=2 * rows * width,
             transcendentals=3 * rows * lanes,
         ),
-        name="projections",
-    )(both, gain, fox_w, lin_w, *lows, *ups, *bases)
+        name="lin_projections",
+    )(at, normed, low, decay_up, rate_up, bases, *sent)
 
 
 def heads_kernel(back_ref, q_ref, o_ref, gain_ref, out_ref):
@@ -498,21 +574,14 @@
     return lax.all_to_all(x, axis, 0, 0, tiled=True)
 
 
-def from_everyone(x, axis):
-    return exchange(jnp.broadcast_to(x, (lax.axis_size(axis), *x.shape)), axis)
-
-
-def own_weights(arrays, axis):
-    groups = lax.axis_size(axis)
-    rows, cols = arrays[0].shape
-    lanes = cols // groups
-    sent = jnp.stack(
-        [
-            jnp.concatenate([a[:, g * lanes : (g + 1) * lanes] for a in arrays], 1)
-            for g in range(groups)
-        ]
-    )
-    return exchange(sent, axis).reshape(groups * rows, len(arrays) * lanes)
+def by_permutes(x, axis):
+    size = lax.axis_size(axis)
+    here = lax.axis_index(axis)
+    return [
+        lax.ppermute(block, axis, [(i, (i + d) % size) for i in range(size)]) if d else block
+        for d in range(size)
+        for block in [lax.dynamic_index_in_dim(x, lax.rem(here + d, size), 0, False)]
+    ]
 
 
 def per_device(
@@ -549,9 +618,19 @@
     place = lax.axis_index("sp")
     col_start = lax.axis_index("tp") * cols + lax.axis_index("fs") * lanes
 
-    mine = from_everyone(inputs.reshape(rows, half_width), "fs")
-    fox_w = own_weights((softmax_query_matrix, softmax_key_matrix, softmax_value_matrix), "fs")
-    lin_w = own_weights((receptance_weight, linear_key_weight, linear_value_weight), "fs")
+    here, side = lax.axis_index("fs"), lax.axis_index("tp")
+    at = jnp.stack((side, here)).astype(jnp.int32)
+    mine = exchange(
+        packed(
+            (inputs.reshape(rows, half_width),),
+            (softmax_query_matrix, softmax_key_matrix, softmax_value_matrix),
+            groups,
+        ),
+        "fs",
+    )
+    lin_sent = packed((), (receptance_weight, linear_key_weight, linear_value_weight), groups)
+    mine, lin_sent = lax.optimization_barrier((mine, lin_sent))
+    lin_sent = by_permutes(lin_sent, "fs")
 
     pair_seq, pair_head = place // heads, lax.rem(place, heads)
     pair_group, pair_slot = pair_seq // seq_count, lax.rem(pair_seq, seq_count)
@@ -567,31 +646,40 @@
     gates = of_pair(running_forget_gate, 1).T.reshape(groups, length // tok_count, tok_count)
     extra = decay_extra_log.reshape(seq_count, tok_count, groups, heads).transpose(2, 0, 3, 1)
     extra = extra.reshape(groups, seq_count * heads, tok_count)
-    small = exchange(jnp.concatenate((state, gates, extra), 1), "fs")
+    small = jnp.stack(by_permutes(jnp.concatenate((state, gates, extra), 1), "fs"))
     half, after = n // 2, n // 2 + length // tok_count
-    extra = small[:, after:].reshape(seqs, heads, tok_count)
-    pair = lax.dynamic_index_in_dim(small, pair_group, 0, False)
+
+    def small_from(group):
+        return lax.dynamic_index_in_dim(small, lax.rem(here + groups - group, groups), 0, False)
+
+    extra = jnp.concatenate([small_from(g)[after:] for g in range(groups)], 0)
+    extra = extra.reshape(seqs, heads, tok_count)
+    pair = small_from(pair_group)
     start, gate = pair[:half], pair[half:after]
 
     def own_columns(table, axis):
         return lax.dynamic_slice_in_dim(table, col_start, lanes, axis)
 
-    both = from_everyone(mine.reshape(seqs * tok_count, half_width), "tp")
-    fox, lin, logged, rate = projections(
-        both,
-        input_norm_gain.reshape(1, -1),
-        fox_w,
-        lin_w,
-        (decay_lower_map, rate_lower_map),
-        (own_columns(decay_upper_map, 1), own_columns(rate_upper_map, 1)),
-        (
-            own_columns(decay_offset_base, 0).reshape(1, lanes),
-            own_columns(rate_offset_base, 0).reshape(1, lanes),
-        ),
-        tok_count,
+    def own_first(table, axis):
+        return jnp.where(side == 0, table, jnp.roll(table, half_width, axis))
+
+    swap = [(i, tp - 1 - i) for i in range(tp)]
+    other = lax.ppermute(mine[:, :, :half_width], "tp", swap)
+    fox, normed = fox_projections(
+        at, mine, other, own_first(input_norm_gain.reshape(1, -1), 1), tok_count
     )
     fox = exchange(fox, "sp")
+    lin, logged, rate = lin_projections(
+        at,
+        normed,
+        own_first(jnp.concatenate((decay_lower_map, rate_lower_map), 1), 0),
+        own_columns(decay_upper_map, 1),
+        own_columns(rate_upper_map, 1),
+        jnp.stack((own_columns(decay_offset_base, 0), own_columns(rate_offset_base, 0))),
+        lin_sent,
+    )
     query, ready, maps = position_maps(lin, logged, rate, extra)
+    maps, fox = lax.optimization_barrier((maps, fox))
     maps = exchange(maps, "sp")
     fox_out = attention(fox, gate)
     states = states_ahead(maps, start)

time: 280 us -> 235 us (0.84)
  blocking collectives: 101 us -> 26.9 us
  starting transfers between devices: 36.2 us -> 78.8 us
  waiting for transfers between devices: 78.6 us -> 55.9 us
  Pallas kernels: 43 us -> 54.4 us
    all_to_all x5 -> x2, blocking collectives: 101 us -> 26.9 us  [exchange(): return lax.all_to_all(x, axis, 0, 0, tiled=True)]
    all_to_all x5 -> x4, waiting for transfers between devices: 78.6 us -> 40.1 us  [exchange(): return lax.all_to_all(x, axis, 0, 0, tiled=True)]
    ppermute x0 -> x7, starting transfers between devices: none -> 28 us  [the longest x1 20.8 us: per_device(): other = lax.ppermute(mine[:, :, :half_width], 'tp', swap)]
    ppermute x0 -> x7, waiting for transfers between devices: none -> 15.9 us  [the longest x6 14.1 us: by_permutes(): lax.ppermute(block, axis, [(i, (i + d) % size) for i in range(size)])]
    all_to_all x5 -> x4, starting transfers between devices: 36.2 us -> 50.8 us  [exchange(): return lax.all_to_all(x, axis, 0, 0, tiled=True)]
    pallas_call x1 -> x4, Pallas kernels: 12.4 us -> 23.8 us  [the longest x2 8.29 us: packed(): pl.pallas_call(pack_kernel, grid=(groups,), out_shape=jax.ShapeDtypeStruc...]
  transfers between devices with their start and end apart: 5 -> 11, of which waited for: 5 -> 7; matrix products, arithmetic and copies ran while one was open for 3% -> 5% of each run, Pallas kernels for 1% -> 13%
where the time goes in v3:
time: 235 us; the launch traced here: 234 us
  starting transfers between devices  78.8 us (34%)
  waiting for transfers between devices  55.9 us (24%)
  Pallas kernels  54.4 us (23%)
  blocking collectives  26.9 us (11%)
  local copies, waits for them, and re-layouts  11.7 us (5%)
  other arithmetic  6.17 us (3%)
    all_to_all x4, starting transfers between devices, exchange(): return lax.all_to_all(x, axis, 0, 0, tiled=True)  50.8 us
    all_to_all x4, waiting for transfers between devices, exchange(): return lax.all_to_all(x, axis, 0, 0, tiled=True)  40.1 us
    all_to_all x2, blocking collectives, exchange(): return lax.all_to_all(x, axis, 0, 0, tiled=True)  26.9 us
    ppermute x1, starting transfers between devices, per_device(): other = lax.ppermute(mine[:, :, :half_width], 'tp', swap)  20.8 us
    ppermute x6, waiting for transfers between devices, by_permutes(): lax.ppermute(block, axis, [(i, (i + d) % size) for i in range(size)])  14.1 us
    pallas_call x1, Pallas kernels, position_maps(): pl.pallas_call(maps_kernel, grid=(seqs // group,), out_shape=(jax.ShapeDt...  12 us
    pallas_call x2, Pallas kernels, packed(): pl.pallas_call(pack_kernel, grid=(groups,), out_shape=jax.ShapeDtypeStruc...  8.29 us
    pallas_call x1, Pallas kernels, lin_projections(): pl.pallas_call(lin_kernel, grid=(rows // tall,), out_shape=(jax.ShapeDtyp...  7.75 us
  transfers between devices with their start and end apart: 11, of which 7 were waited for; matrix products, arithmetic and copies ran while one was open for 5% of the time, Pallas kernels for 13%

profile of v3, /device:TPU:33, one launch (start us, length us, event | category | flops | bytes accessed | tf_op | source)
XLA Modules:
  0.0 234.2 jit_solution(10869394625910933132)
XLA Ops:
  0.0 4.5 %packed.2 = bf16[4,256,1792]{2,1,0:T(8,128)(2,1)} custom-call(bf16[256,1024]{1,0:T(8,128)(2,1)} %bitcast.61, bf16[512,512]{1,0:T(8,128)(2,1)} %refs_1_.2, bf16[512,512]{1,0:T(8,128)(2,1)} %refs_2_.2, bf16[512,512]{1,0:T(8,128)(2,1)} %refs_3_.1), custom_call_target="tpu_custom_call" | custom-call | flops 1048576 | bytes 14680064 | tf_op jit(solution)/shard_map/packed/pallas_call | solution.py:332
  4.5 5.1 %all-to-all-start = ((bf16[4,256,1792]{2,1,0:T(8,128)(2,1)}), bf16[4,256,1792]{2,1,0:T(8,128)(2,1)}, u32[]{:S(2)}, u32[]{:S(2)}) async-start(bf16[4,256,1792]{2,1,0:T(8,128)(2,1)} %packed.2), calls=%async_computation | async-start | bytes 7340032 | tf_op jit(solution)/shard_map/all_to_all | solution.py:574
  9.7 3.8 %packed.3 = bf16[4,256,768]{2,1,0:T(8,128)(2,1)} custom-call(bf16[512,512]{1,0:T(8,128)(2,1)} %refs_0_.1, bf16[512,512]{1,0:T(8,128)(2,1)} %refs_1_.3, bf16[512,512]{1,0:T(8,128)(2,1)} %refs_2_.3), custom_call_target="tpu_custom_call" | custom-call | flops 1048576 | bytes 6291456 | tf_op jit(solution)/shard_map/packed/pallas_call | solution.py:332
  13.4 20.6 %all-to-all-done.mine_ref = bf16[4,256,1792]{2,1,0:T(8,128)(2,1)} async-done(((bf16[4,256,1792]{2,1,0:T(8,128)(2,1)}), bf16[4,256,1792]{2,1,0:T(8,128)(2,1)}, u32[]{:S(2)}, u32[]{:S(2)}) %all-to-all-start) | async-done | bytes 3670048 | tf_op jit(solution)/shard_map/all_to_all | solution.py:574
  34.0 1.8 slice.61
  35.8 20.8 %collective-permute-start = (bf16[4,256,1024]{2,1,0:T(8,128)(2,1)S(1)}, bf16[4,256,1024]{2,1,0:T(8,128)(2,1)}, u32[]{:S(2)}, u32[]{:S(2)}) collective-permute-start(bf16[4,256,1024]{2,1,0:T(8,128)(2,1)S(1)} %slice.61), channel_id=1, source_target_pairs={{0,1},{1,0},{2,3},{3,2},{4,5},{5,4},{6,7},{7,6},{8,9},{9,8},{10,11... | collective-permute-start | bytes 6291464 | tf_op jit(solution)/shard_map/ppermute | solution.py:667
  58.8 1.7 collective-permute-done.other_ref
  60.5 7.7 %fox_projections.1 = (bf16[16,192,128]{2,1,0:T(8,128)(2,1)}, bf16[1024,2048]{1,0:T(8,128)(2,1)}) custom-call(s32[2]{0:T(128)} %pad_add_fusion.at_ref, bf16[4,256,1792]{2,1,0:T(8,128)(2,1)} %all-to-all-done.mine_ref, bf16[4,256,1024]{2,1,0:T(8,128)(2,1)} %collective-permute-done.other_ref, bf16[1,2048]{1,0:T(2,128)(2,1)} %select_n.74.gain_ref), custom_call_target="tpu_custom_call" | custom-call | flops 1610612736 | bytes 8388608 | tf_op jit(solution)/shard_map/fox_projections/pallas_call | solution.py:390
  68.3 23.5 %all-to-all-start.1 = ((bf16[16,192,128]{2,1,0:T(8,128)(2,1)}), bf16[16,192,128]{2,1,0:T(8,128)(2,1)S(1)}, u32[]{:S(2)}, u32[]{:S(2)}) async-start(bf16[16,192,128]{2,1,0:T(8,128)(2,1)} %get-tuple-element.24), calls=%async_computation.1 | async-start | bytes 1572864 | tf_op jit(solution)/shard_map/all_to_all | solution.py:574
  93.0 1.4 collective-permute-start.5
  95.2 1.4 constant_dynamic-slice_fusion.8
  96.9 1.3 maximum_select_fusion.low_ref
  99.6 1.2 collective-permute-start.1
  100.8 2.6 %collective-permute-start.2 = (bf16[256,768]{1,0:T(8,128)(2,1)S(1)}, bf16[256,768]{1,0:T(8,128)(2,1)S(1)}, u32[]{:S(2)}, u32[]{:S(2)}) collective-permute-start(bf16[256,768]{1,0:T(8,128)(2,1)S(1)} %get-tuple-element.32), channel_id=1, source_target_pairs={{0,4},{2,6},{4,0},{6,2},{1,5},{3,7},{5,1},{7,3},{8,12},{10,14},{12... | collective-permute-start | bytes 1179656 | tf_op jit(solution)/shard_map/ppermute | solution.py:581
  103.4 1.0 collective-permute-start.3
  105.7 4.6 %collective-permute-done.1.rest_1_ = bf16[256,768]{1,0:T(8,128)(2,1)S(1)} collective-permute-done((bf16[256,768]{1,0:T(8,128)(2,1)S(1)}, bf16[256,768]{1,0:T(8,128)(2,1)S(1)}, u32[]{:S(2)}, u32[]{:S(2)}) %collective-permute-start.1) | collective-permute-done | bytes 393248 | tf_op jit(solution)/shard_map/ppermute | solution.py:581
  110.2 9.3 %collective-permute-done.2.rest_2_ = bf16[256,768]{1,0:T(8,128)(2,1)S(1)} collective-permute-done((bf16[256,768]{1,0:T(8,128)(2,1)S(1)}, bf16[256,768]{1,0:T(8,128)(2,1)S(1)}, u32[]{:S(2)}, u32[]{:S(2)}) %collective-permute-start.2) | collective-permute-done | bytes 393248 | tf_op jit(solution)/shard_map/ppermute | solution.py:581
  120.3 7.7 %lin_projections.1 = (bf16[1024,384]{1,0:T(8,128)(2,1)}, f32[1024,128]{1,0:T(8,128)}, f32[1024,128]{1,0:T(8,128)}) custom-call(s32[2]{0:T(128)} %pad_add_fusion.at_ref, bf16[1024,2048]{1,0:T(8,128)(2,1)} %get-tuple-element.18.normed_ref, bf16[2048,256]{1,0:T(8,128)(2,1)} %maximum_select_fusion.low_ref, bf16[128,128]{1,0:T(8,128)(2,1)} %get-tuple-element.48.decay_up_ref, ...), custom_call_target="tpu_custom_call" | custom-call | flops 2684354560 | bytes 4194304 | tf_op jit(solution)/shard_map/lin_projections/pallas_call | solution.py:445
  128.1 12.0 %position_maps.1 = (bf16[1024,128]{1,0:T(8,128)(2,1)}, f32[1024,128]{1,0:T(8,128)}, bf16[16,64,128]{2,1,0:T(8,128)(2,1)}) custom-call(bf16[1024,384]{1,0:T(8,128)(2,1)} %get-tuple-element.20.proj_ref, f32[1024,128]{1,0:T(8,128)} %get-tuple-element.21.log_ref, f32[1024,128]{1,0:T(8,128)} %get-tuple-element.22.rate_ref, f32[8,2,128]{2,1,0:T(2,128)} %bitcast.69), custom_call_target="tpu_custom_call" | custom-call | flops 1342177280 | bytes 2621440 | tf_op jit(solution)/shard_map/position_maps/pallas_call | solution.py:256
  140.1 11.2 %all-to-all-start.2 = ((bf16[16,64,128]{2,1,0:T(8,128)(2,1)}), bf16[16,64,128]{2,1,0:T(8,128)(2,1)S(1)}, u32[]{:S(2)}, u32[]{:S(2)}) async-start(bf16[16,64,128]{2,1,0:T(8,128)(2,1)} %get-tuple-element.26), calls=%async_computation.2 | async-start | bytes 524288 | tf_op jit(solution)/shard_map/all_to_all | solution.py:574
  152.6 7.1 %attention.1 = bf16[16,64,128]{2,1,0:T(8,128)(2,1)} custom-call(bf16[16,192,128]{2,1,0:T(8,128)(2,1)} %copy-done.4, f32[16,128]{1,0:T(8,128)} %dynamic-slice_bitcast_fusion.9.gate_ref), custom_call_target="tpu_custom_call" | custom-call | flops 1073741824 | bytes 1572864 | tf_op jit(solution)/shard_map/attention/pallas_call | solution.py:86
  159.6 4.2 %all-to-all-done.2.maps_ref = bf16[16,64,128]{2,1,0:T(8,128)(2,1)S(1)} async-done(((bf16[16,64,128]{2,1,0:T(8,128)(2,1)}), bf16[16,64,128]{2,1,0:T(8,128)(2,1)S(1)}, u32[]{:S(2)}, u32[]{:S(2)}) %all-to-all-start.2) | async-done | bytes 262176 | tf_op jit(solution)/shard_map/all_to_all | solution.py:574
  164.5 3.7 %states_ahead.1 = bf16[16,32,128]{2,1,0:T(8,128)(2,1)} custom-call(bf16[16,64,128]{2,1,0:T(8,128)(2,1)} %copy-done.3, f32[32,128]{1,0:T(8,128)} %dynamic-slice_bitcast_fusion.8.start_ref), custom_call_target="tpu_custom_call" | custom-call | flops 16777216 | bytes 524288 | tf_op jit(solution)/shard_map/states_ahead/pallas_call | solution.py:302
  168.2 1.8 pad_maximum_fusion
  170.0 10.9 %all-to-all-start.3 = ((bf16[16,96,128]{2,1,0:T(8,128)(2,1)}), bf16[16,96,128]{2,1,0:T(8,128)(2,1)S(1)}, u32[]{:S(2)}, u32[]{:S(2)}) async-start(bf16[16,96,128]{2,1,0:T(8,128)(2,1)} %pad_maximum_fusion), calls=%async_computation.3 | async-start | bytes 786432 | tf_op jit(solution)/shard_map/all_to_all | solution.py:574
  180.9 1.3 dynamic-slice_bitcast_fusion.10.gain_ref
  182.2 15.3 %all-to-all-done.3.back_ref = bf16[16,96,128]{2,1,0:T(8,128)(2,1)S(1)} async-done(((bf16[16,96,128]{2,1,0:T(8,128)(2,1)}), bf16[16,96,128]{2,1,0:T(8,128)(2,1)S(1)}, u32[]{:S(2)}, u32[]{:S(2)}) %all-to-all-start.3) | async-done | bytes 393248 | tf_op jit(solution)/shard_map/all_to_all | solution.py:574
  198.3 2.7 %heads_out.1 = bf16[4,256,256]{2,1,0:T(8,128)(2,1)} custom-call(bf16[16,96,128]{2,1,0:T(8,128)(2,1)} %copy-done.2, bf16[1024,128]{1,0:T(8,128)(2,1)} %get-tuple-element.27.q_ref, f32[1024,128]{1,0:T(8,128)} %get-tuple-element.28.o_ref, bf16[1,128]{1,0:T(2,128)(2,1)} %dynamic-slice_bitcast_fusion.10.gain_ref), custom_call_target="tpu_custom_call" | custom-call | flops 167772160 | bytes 1572864 | tf_op jit(solution)/shard_map/heads_out/pallas_call | solution.py:518
  201.0 13.6 %all_to_all.30.acts_ref = bf16[4,256,256]{2,1,0:T(8,128)(2,1)} all-to-all(bf16[4,256,256]{2,1,0:T(8,128)(2,1)} %heads_out.1), channel_id=1, replica_groups=mesh['grp'=2,'sp'=16,'fs'=4,'tp'=2] {'fs'}, dimensions={0} | all-to-all | bytes 1048576 | tf_op jit(solution)/shard_map/all_to_all | solution.py:574
  214.6 5.2 %closing.1 = bf16[256,2048]{1,0:T(8,128)(2,1)} custom-call(bf16[4,256,256]{2,1,0:T(8,128)(2,1)} %all_to_all.30.acts_ref, bf16[2048,512]{1,0:T(8,128)(2,1)} %fox_w_ref.1, bf16[2048,512]{1,0:T(8,128)(2,1)} %lin_w_ref.1), custom_call_target="tpu_custom_call" | custom-call | flops 1073741824 | bytes 5242880 | tf_op jit(solution)/shard_map/closing/pallas_call | solution.py:552
  219.7 13.3 %all_to_all.31 = bf16[2,128,2048]{2,1,0:T(8,128)(2,1)S(1)} all-to-all(bf16[2,128,2048]{2,1,0:T(8,128)(2,1)} %bitcast.59), channel_id=1, replica_groups=mesh['grp'=2,'sp'=16,'fs'=4,'tp'=2] {'tp'}, dimensions={0} | all-to-all | bytes 2097152 | tf_op jit(solution)/shard_map/all_to_all | solution.py:574
  233.1 1.1 reduce_sum.14
  (60 shorter events, 10.4 us)
Async XLA Ops:
  0.0 58.0 %copy-start = (f32[2,8,64,64]{3,2,1,0:T(8,128)S(1)}, f32[2,8,64,64]{3,2,1,0:T(8,128)}, u32[]{:S(2)}) copy-start(f32[2,8,64,64]{3,2,1,0:T(8,128)} %param.37) | copy-start | bytes 786436
  4.5 29.5 %all-to-all-start = ((bf16[4,256,1792]{2,1,0:T(8,128)(2,1)}), bf16[4,256,1792]{2,1,0:T(8,128)(2,1)}, u32[]{:S(2)}, u32[]{:S(2)}) async-start(bf16[4,256,1792]{2,1,0:T(8,128)(2,1)} %packed.2), calls=%async_computation | async-start | bytes 7340032 | tf_op jit(solution)/shard_map/all_to_all | solution.py:574
  13.4 43.2 %copy-start.9 = (bf16[2048]{0:T(1024)(128)(2,1)S(1)}, bf16[2048]{0:T(1024)(128)(2,1)}, u32[]{:S(2)}) copy-start(bf16[2048]{0:T(1024)(128)(2,1)} %param.21) | copy-start | bytes 12292
  13.4 43.9 %copy-start.8 = (f32[2,2048,8]{1,2,0:T(8,128)S(1)}, f32[2,2048,8]{1,2,0:T(8,128)}, u32[]{:S(2)}) copy-start(f32[2,2048,8]{1,2,0:T(8,128)} %param.25) | copy-start | bytes 393220
  35.8 24.7 %collective-permute-start = (bf16[4,256,1024]{2,1,0:T(8,128)(2,1)S(1)}, bf16[4,256,1024]{2,1,0:T(8,128)(2,1)}, u32[]{:S(2)}, u32[]{:S(2)}) collective-permute-start(bf16[4,256,1024]{2,1,0:T(8,128)(2,1)S(1)} %slice.61), channel_id=1, source_target_pairs={{0,1},{1,0},{2,3},{3,2},{4,5},{5,4},{6,7},{7,6},{8,9},{9,8},{10,11... | collective-permute-start | bytes 6291464 | tf_op jit(solution)/shard_map/ppermute | solution.py:667
  58.8 33.1 %copy-start.10 = (f32[2,128,8]{1,2,0:T(8,128)S(1)}, f32[2,128,8]{1,2,0:T(8,128)}, u32[]{:S(2)}) copy-start(f32[2,128,8]{1,2,0:T(8,128)} %param.32) | copy-start | bytes 24580
  60.5 31.3 %copy-start.5 = (f32[1,8,64,64]{3,2,1,0:T(8,128)S(1)}, f32[1,8,64,64]{3,2,1,0:T(8,128)}, u32[]{:S(2)}) copy-start(f32[1,8,64,64]{3,2,1,0:T(8,128)} %constant_dynamic-slice_fusion.7) | copy-start | bytes 393220
  68.3 28.3 %copy-start.6 = (bf16[2048,128]{1,0:T(8,128)(2,1)S(1)}, bf16[2048,128]{1,0:T(8,128)(2,1)}, u32[]{:S(2)}) copy-start(bf16[2048,128]{1,0:T(8,128)(2,1)} %param.29) | copy-start | bytes 1572868
  68.3 28.4 %copy-start.7 = (bf16[2048,128]{1,0:T(8,128)(2,1)S(1)}, bf16[2048,128]{1,0:T(8,128)(2,1)}, u32[]{:S(2)}) copy-start(bf16[2048,128]{1,0:T(8,128)(2,1)} %param.33) | copy-start | bytes 1572868
  68.3 71.8 %all-to-all-start.1 = ((bf16[16,192,128]{2,1,0:T(8,128)(2,1)}), bf16[16,192,128]{2,1,0:T(8,128)(2,1)S(1)}, u32[]{:S(2)}, u32[]{:S(2)}) async-start(bf16[16,192,128]{2,1,0:T(8,128)(2,1)} %get-tuple-element.24), calls=%async_computation.1 | async-start | bytes 1572864 | tf_op jit(solution)/shard_map/all_to_all | solution.py:574
  92.1 11.4 %collective-permute-start.6 = (f32[52,128]{1,0:T(8,128)S(1)}, f32[52,128]{1,0:T(8,128)S(1)}, u32[]{:S(2)}, u32[]{:S(2)}) collective-permute-start(f32[52,128]{1,0:T(8,128)S(1)} %get-tuple-element.44), channel_id=1, source_target_pairs={{0,6},{2,0},{4,2},{6,4},{1,7},{3,1},{5,3},{7,5},{8,14},{10,8},{12,... | collective-permute-start | bytes 79880 | tf_op jit(solution)/shard_map/ppermute | solution.py:581
  93.0 12.0 %collective-permute-start.5 = (f32[52,128]{1,0:T(8,128)S(1)}, f32[52,128]{1,0:T(8,128)S(1)}, u32[]{:S(2)}, u32[]{:S(2)}) collective-permute-start(f32[52,128]{1,0:T(8,128)S(1)} %get-tuple-element.45), channel_id=1, source_target_pairs={{0,4},{2,6},{4,0},{6,2},{1,5},{3,7},{5,1},{7,3},{8,12},{10,14},{12... | collective-permute-start | bytes 79880 | tf_op jit(solution)/shard_map/ppermute | solution.py:581
  94.4 10.6 %collective-permute-start.4 = (f32[52,128]{1,0:T(8,128)S(1)}, f32[52,128]{1,0:T(8,128)S(1)}, u32[]{:S(2)}, u32[]{:S(2)}) collective-permute-start(f32[52,128]{1,0:T(8,128)S(1)} %get-tuple-element.46), channel_id=1, source_target_pairs={{0,2},{2,4},{4,6},{6,0},{1,3},{3,5},{5,7},{7,1},{8,10},{10,12},{12... | collective-permute-start | bytes 79880 | tf_op jit(solution)/shard_map/ppermute | solution.py:581
  96.9 1.8 copy-start.1
  99.6 10.7 %collective-permute-start.1 = (bf16[256,768]{1,0:T(8,128)(2,1)S(1)}, bf16[256,768]{1,0:T(8,128)(2,1)S(1)}, u32[]{:S(2)}, u32[]{:S(2)}) collective-permute-start(bf16[256,768]{1,0:T(8,128)(2,1)S(1)} %get-tuple-element.33), channel_id=1, source_target_pairs={{0,2},{2,4},{4,6},{6,0},{1,3},{3,5},{5,7},{7,1},{8,10},{10,12},{12... | collective-permute-start | bytes 1179656 | tf_op jit(solution)/shard_map/ppermute | solution.py:581
  100.8 18.8 %collective-permute-start.2 = (bf16[256,768]{1,0:T(8,128)(2,1)S(1)}, bf16[256,768]{1,0:T(8,128)(2,1)S(1)}, u32[]{:S(2)}, u32[]{:S(2)}) collective-permute-start(bf16[256,768]{1,0:T(8,128)(2,1)S(1)} %get-tuple-element.32), channel_id=1, source_target_pairs={{0,4},{2,6},{4,0},{6,2},{1,5},{3,7},{5,1},{7,3},{8,12},{10,14},{12... | collective-permute-start | bytes 1179656 | tf_op jit(solution)/shard_map/ppermute | solution.py:581
  103.4 16.4 %collective-permute-start.3 = (bf16[256,768]{1,0:T(8,128)(2,1)S(1)}, bf16[256,768]{1,0:T(8,128)(2,1)}, u32[]{:S(2)}, u32[]{:S(2)}) collective-permute-start(bf16[256,768]{1,0:T(8,128)(2,1)S(1)} %get-tuple-element.31), channel_id=1, source_target_pairs={{0,6},{2,0},{4,2},{6,4},{1,7},{3,1},{5,3},{7,5},{8,14},{10,8},{12,... | collective-permute-start | bytes 1179656 | tf_op jit(solution)/shard_map/ppermute | solution.py:581
  110.2 9.6 %copy-start.11 = (bf16[256,768]{1,0:T(8,128)(2,1)}, bf16[256,768]{1,0:T(8,128)(2,1)S(1)}, u32[]{:S(2)}) copy-start(bf16[256,768]{1,0:T(8,128)(2,1)S(1)} %collective-permute-done.1.rest_1_) | copy-start | bytes 1179652
  119.6 0.8 copy-start.12
  140.1 12.5 %copy-start.4 = (bf16[16,192,128]{2,1,0:T(8,128)(2,1)}, bf16[16,192,128]{2,1,0:T(8,128)(2,1)S(1)}, u32[]{:S(2)}) copy-start(bf16[16,192,128]{2,1,0:T(8,128)(2,1)S(1)} %all-to-all-done.1.blocks_ref) | copy-start | bytes 2359300
  140.1 23.7 %all-to-all-start.2 = ((bf16[16,64,128]{2,1,0:T(8,128)(2,1)}), bf16[16,64,128]{2,1,0:T(8,128)(2,1)S(1)}, u32[]{:S(2)}, u32[]{:S(2)}) async-start(bf16[16,64,128]{2,1,0:T(8,128)(2,1)} %get-tuple-element.26), calls=%async_computation.2 | async-start | bytes 524288 | tf_op jit(solution)/shard_map/all_to_all | solution.py:574
  163.8 0.7 copy-start.3
  170.0 27.5 %all-to-all-start.3 = ((bf16[16,96,128]{2,1,0:T(8,128)(2,1)}), bf16[16,96,128]{2,1,0:T(8,128)(2,1)S(1)}, u32[]{:S(2)}, u32[]{:S(2)}) async-start(bf16[16,96,128]{2,1,0:T(8,128)(2,1)} %pad_maximum_fusion), calls=%async_computation.3 | async-start | bytes 786432 | tf_op jit(solution)/shard_map/all_to_all | solution.py:574
  197.5 0.8 copy-start.2

commit v4 on v3

--- a/solution.py
+++ b/solution.py
@@ -1,5 +1,3 @@
-import functools
-
 import jax
 import jax.numpy as jnp
 from jax import lax
@@ -282,12 +280,13 @@
     )(proj, logged, rate, extra)
 
 
-def states_kernel(maps_ref, start_ref, out_ref):
+def states_kernel(maps_ref, start_ref, fox_ref, out_ref):
     count = maps_ref.shape[0]
     n = HEAD_CHANNELS
+    out_ref[:, :n, :] = fox_ref[...]
     state = jnp.concatenate((start_ref[:, :n], start_ref[:, n:]), 0)
     for i in range(count):
-        out_ref[i] = jnp.concatenate((state[: n // 2], state[n // 2 :]), 1).astype(BF16)
+        out_ref[i, n:, :] = jnp.concatenate((state[: n // 2], state[n // 2 :]), 1).astype(BF16)
         if i + 1 < count:
             pair = maps_ref[i]
             high = state.astype(BF16)
@@ -296,19 +295,19 @@
             state = moved[:n] + moved[n:] + pair[:, n:].astype(F32)
 
 
-def states_ahead(maps, start):
+def states_ahead(maps, start, fox):
     count = maps.shape[0]
     whole = pl.BlockSpec(memory_space=pltpu.VMEM)
     return pl.pallas_call(
         states_kernel,
-        out_shape=jax.ShapeDtypeStruct((count, HEAD_CHANNELS // 2, 2 * HEAD_CHANNELS), BF16),
-        in_specs=[whole, whole],
+        out_shape=jax.ShapeDtypeStruct((count, 3 * HEAD_CHANNELS // 2, 2 * HEAD_CHANNELS), BF16),
+        in_specs=[whole, whole, whole],
         out_specs=whole,
         cost_estimate=pl.CostEstimate(
             flops=count * 4 * HEAD_CHANNELS**3, bytes_accessed=1 << 19, transcendentals=0
         ),
         name="states_ahead",
-    )(maps, start)
+    )(maps, start, fox)
 
 
 def halves(weights):
@@ -475,7 +474,7 @@
     n = HEAD_CHANNELS
     lanes = 2 * n
     pairs, _, tok_count = back_ref.shape
-    groups, rows, _ = out_ref.shape
+    _, rows, _ = out_ref.shape
     head_block = (places((lanes, lanes), 0) < n) == (places((lanes, lanes), 1) < n)
     average = jnp.where(head_block, 1.0 / n, 0.0).astype(BF16)
     first = places((n // 2, lanes), 1) < n
@@ -528,16 +527,18 @@
     )(back, query, ready, gain)
 
 
-def closing_kernel(acts_ref, fox_w_ref, lin_w_ref, out_ref, act_scr):
-    groups, rows, both = acts_ref.shape
+def closing_kernel(seq_ref, acts_ref, fox_w_ref, lin_w_ref, out_ref, act_scr):
+    groups, _, both = acts_ref.shape
+    rows = act_scr.shape[0]
     lanes = both // 2
     cols = groups * lanes
 
     @pl.when(pl.program_id(0) == 0)
     def _():
+        here = pl.ds(pl.multiple_of(seq_ref[0] * rows, rows), rows)
         for g in range(groups):
-            act_scr[:, g * lanes : (g + 1) * lanes] = acts_ref[g, :, :lanes]
-            act_scr[:, cols + g * lanes : cols + (g + 1) * lanes] = acts_ref[g, :, lanes:]
+            act_scr[:, g * lanes : (g + 1) * lanes] = acts_ref[g, here, :lanes]
+            act_scr[:, cols + g * lanes : cols + (g + 1) * lanes] = acts_ref[g, here, lanes:]
 
     out_ref[...] = (
         lax.dot_general(act_scr[:, :cols], fox_w_ref[...], NT, preferred_element_type=F32)
@@ -545,8 +546,9 @@
     ).astype(BF16)
 
 
-def closing(acts, fox_w, lin_w):
-    groups, rows, both = acts.shape
+def closing(part, parts, acts, fox_w, lin_w):
+    _, rows, _ = acts.shape
+    rows = rows // parts
     width, cols = fox_w.shape
     tile = 512
     return pl.pallas_call(
@@ -554,6 +556,7 @@
         grid=(width // tile,),
         out_shape=jax.ShapeDtypeStruct((rows, width), BF16),
         in_specs=[
+            pl.BlockSpec(memory_space=pltpu.SMEM),
             pl.BlockSpec(memory_space=pltpu.VMEM),
             pl.BlockSpec((tile, cols), lambda i: (i, 0)),
             pl.BlockSpec((tile, cols), lambda i: (i, 0)),
@@ -567,20 +570,24 @@
             transcendentals=0,
         ),
         name="closing",
-    )(acts, fox_w, lin_w)
+    )(part, acts, fox_w, lin_w)
 
 
 def exchange(x, axis):
     return lax.all_to_all(x, axis, 0, 0, tiled=True)
 
 
-def by_permutes(x, axis):
+def in_turn(x, axis):
     size = lax.axis_size(axis)
     here = lax.axis_index(axis)
+    return [lax.dynamic_index_in_dim(x, lax.rem(here + d, size), 0, False) for d in range(size)]
+
+
+def by_permutes(blocks, axis):
+    size = lax.axis_size(axis)
     return [
         lax.ppermute(block, axis, [(i, (i + d) % size) for i in range(size)]) if d else block
-        for d in range(size)
-        for block in [lax.dynamic_index_in_dim(x, lax.rem(here + d, size), 0, False)]
+        for d, block in enumerate(blocks)
     ]
 
 
@@ -618,7 +625,7 @@
     place = lax.axis_index("sp")
     col_start = lax.axis_index("tp") * cols + lax.axis_index("fs") * lanes
 
-    here, side = lax.axis_index("fs"), lax.axis_index("tp")
+    here, side = lax.axis_index("fs"), lax.axis_index("tp").astype(jnp.int32)
     at = jnp.stack((side, here)).astype(jnp.int32)
     mine = exchange(
         packed(
@@ -629,7 +636,7 @@
         "fs",
     )
     lin_sent = packed((), (receptance_weight, linear_key_weight, linear_value_weight), groups)
-    mine, lin_sent = lax.optimization_barrier((mine, lin_sent))
+    mine, lin_sent = lax.optimization_barrier((mine, in_turn(lin_sent, "fs")))
     lin_sent = by_permutes(lin_sent, "fs")
 
     pair_seq, pair_head = place // heads, lax.rem(place, heads)
@@ -646,7 +653,8 @@
     gates = of_pair(running_forget_gate, 1).T.reshape(groups, length // tok_count, tok_count)
     extra = decay_extra_log.reshape(seq_count, tok_count, groups, heads).transpose(2, 0, 3, 1)
     extra = extra.reshape(groups, seq_count * heads, tok_count)
-    small = jnp.stack(by_permutes(jnp.concatenate((state, gates, extra), 1), "fs"))
+    small = in_turn(jnp.concatenate((state, gates, extra), 1), "fs")
+    small = jnp.stack(by_permutes(small, "fs"))
     half, after = n // 2, n // 2 + length // tok_count
 
     def small_from(group):
@@ -682,15 +690,14 @@
     maps, fox = lax.optimization_barrier((maps, fox))
     maps = exchange(maps, "sp")
     fox_out = attention(fox, gate)
-    states = states_ahead(maps, start)
-    back = exchange(jnp.concatenate((fox_out, states), 1), "sp")
+    back = exchange(states_ahead(maps, start, fox_out), "sp")
     gain = own_columns(linear_head_gain, 0).reshape(1, lanes)
     acts = exchange(heads_out(back, query, ready, gain, groups), "fs")
-    partial = closing(acts, softmax_output_weight, linear_output_weight)
-    pieces = exchange(partial.reshape(seq_count, tok_count, -1), "tp")
-    mixed = jnp.sum(
-        pieces.reshape(tp, seq_count // tp, tok_count, -1).astype(F32), axis=0
-    )
+    weights = (softmax_output_weight, linear_output_weight)
+    theirs = closing((tp - 1 - side).reshape(1), tp, acts, *weights)
+    theirs = lax.ppermute(theirs, "tp", swap)
+    own = closing(side.reshape(1), tp, acts, *weights)
+    mixed = (own.astype(F32) + theirs.astype(F32)).reshape(seq_count // tp, tok_count, -1)
     return mixed.astype(BF16)
 
 
@@ -717,6 +724,7 @@
         P(None, "tp"),
         P(None, "tp"),
     )
+
     return jax.shard_map(
         per_device,
         mesh=mesh,

time: 235 us -> 234 us (level)
  blocking collectives: 26.9 us -> 0 us
  starting transfers between devices: 78.8 us -> 92.6 us
  waiting for transfers between devices: 55.9 us -> 61.9 us
  Pallas kernels: 54.4 us -> 59.4 us
    all_to_all x2 -> x0, blocking collectives: 26.9 us -> none  [exchange(): return lax.all_to_all(x, axis, 0, 0, tiled=True)]
    ppermute x0 -> x1, starting transfers between devices: none -> 8.02 us  [per_device(): theirs = lax.ppermute(theirs, 'tp', swap)]
    all_to_all x4 -> x5, waiting for transfers between devices: 40.1 us -> 45.9 us  [exchange(): return lax.all_to_all(x, axis, 0, 0, tiled=True)]
    all_to_all x4 -> x5, starting transfers between devices: 50.8 us -> 56.5 us  [exchange(): return lax.all_to_all(x, axis, 0, 0, tiled=True)]
    pallas_call x1 -> x2, Pallas kernels: 5.15 us -> 9.97 us  [closing(): pl.pallas_call(closing_kernel, grid=(width // tile,), out_shape=jax.Shape...]
  transfers between devices with their start and end apart: 11 -> 13, of which waited for: 7 -> 8; matrix products, arithmetic and copies ran while one was open for 5% -> 5% of each run, Pallas kernels for 13% -> 15%
where the time goes in v4:
time: 234 us; the launch traced here: 232 us
  starting transfers between devices  92.6 us (40%)
  waiting for transfers between devices  61.9 us (26%)
  Pallas kernels  59.4 us (25%)
  local copies, waits for them, and re-layouts  13.1 us (6%)
  other arithmetic  5.24 us (2%)
    all_to_all x5, starting transfers between devices, exchange(): return lax.all_to_all(x, axis, 0, 0, tiled=True)  56.5 us
    all_to_all x5, waiting for transfers between devices, exchange(): return lax.all_to_all(x, axis, 0, 0, tiled=True)  45.9 us
    ppermute x1, starting transfers between devices, per_device(): other = lax.ppermute(mine[:, :, :half_width], 'tp', swap)  20.8 us
    ppermute x6, waiting for transfers between devices, by_permutes(): lax.ppermute(block, axis, [(i, (i + d) % size) for i in range(size)])  14.3 us
    pallas_call x1, Pallas kernels, position_maps(): pl.pallas_call(maps_kernel, grid=(seqs // group,), out_shape=(jax.ShapeDt...  12 us
    pallas_call x2, Pallas kernels, closing(): pl.pallas_call(closing_kernel, grid=(width // tile,), out_shape=jax.Shape...  9.97 us
    pallas_call x2, Pallas kernels, packed(): pl.pallas_call(pack_kernel, grid=(groups,), out_shape=jax.ShapeDtypeStruc...  8.3 us
    ppermute x1, starting transfers between devices, per_device(): theirs = lax.ppermute(theirs, 'tp', swap)  8.02 us
  transfers between devices with their start and end apart: 13, of which 8 were waited for; matrix products, arithmetic and copies ran while one was open for 5% of the time, Pallas kernels for 15%

profile of v4, /device:TPU:33, one launch (start us, length us, event | category | flops | bytes accessed | tf_op | source)
XLA Modules:
  0.0 232.4 jit_solution(14420534126397465960)
XLA Ops:
  0.0 4.5 %packed.2 = bf16[4,256,1792]{2,1,0:T(8,128)(2,1)} custom-call(bf16[256,1024]{1,0:T(8,128)(2,1)} %bitcast.61, bf16[512,512]{1,0:T(8,128)(2,1)} %refs_1_.2, bf16[512,512]{1,0:T(8,128)(2,1)} %refs_2_.2, bf16[512,512]{1,0:T(8,128)(2,1)} %refs_3_.1), custom_call_target="tpu_custom_call" | custom-call | flops 1048576 | bytes 14680064 | tf_op jit(solution)/shard_map/packed/pallas_call | solution.py:331
  4.5 5.1 %all-to-all-start = ((bf16[4,256,1792]{2,1,0:T(8,128)(2,1)}), bf16[4,256,1792]{2,1,0:T(8,128)(2,1)}, u32[]{:S(2)}, u32[]{:S(2)}) async-start(bf16[4,256,1792]{2,1,0:T(8,128)(2,1)} %packed.2), calls=%async_computation | async-start | bytes 7340032 | tf_op jit(solution)/shard_map/all_to_all | solution.py:577
  9.6 3.8 %packed.3 = bf16[4,256,768]{2,1,0:T(8,128)(2,1)} custom-call(bf16[512,512]{1,0:T(8,128)(2,1)} %refs_0_.1, bf16[512,512]{1,0:T(8,128)(2,1)} %refs_1_.3, bf16[512,512]{1,0:T(8,128)(2,1)} %refs_2_.3), custom_call_target="tpu_custom_call" | custom-call | flops 1048576 | bytes 6291456 | tf_op jit(solution)/shard_map/packed/pallas_call | solution.py:331
  13.4 2.3 dynamic-slice_bitcast_fusion
  15.7 18.3 %all-to-all-done.mine_ref = bf16[4,256,1792]{2,1,0:T(8,128)(2,1)} async-done(((bf16[4,256,1792]{2,1,0:T(8,128)(2,1)}), bf16[4,256,1792]{2,1,0:T(8,128)(2,1)}, u32[]{:S(2)}, u32[]{:S(2)}) %all-to-all-start) | async-done | bytes 3670048 | tf_op jit(solution)/shard_map/all_to_all | solution.py:577
  34.0 1.8 slice.61
  35.8 20.8 %collective-permute-start = (bf16[4,256,1024]{2,1,0:T(8,128)(2,1)S(1)}, bf16[4,256,1024]{2,1,0:T(8,128)(2,1)}, u32[]{:S(2)}, u32[]{:S(2)}) collective-permute-start(bf16[4,256,1024]{2,1,0:T(8,128)(2,1)S(1)} %slice.61), channel_id=1, source_target_pairs={{0,1},{1,0},{2,3},{3,2},{4,5},{5,4},{6,7},{7,6},{8,9},{9,8},{10,11... | collective-permute-start | bytes 6291464 | tf_op jit(solution)/shard_map/ppermute | solution.py:675
  58.9 1.6 collective-permute-done.other_ref
  60.6 7.7 %fox_projections.1 = (bf16[16,192,128]{2,1,0:T(8,128)(2,1)}, bf16[1024,2048]{1,0:T(8,128)(2,1)}) custom-call(s32[2]{0:T(128)} %pad_add_fusion.at_ref, bf16[4,256,1792]{2,1,0:T(8,128)(2,1)} %all-to-all-done.mine_ref, bf16[4,256,1024]{2,1,0:T(8,128)(2,1)} %collective-permute-done.other_ref, bf16[1,2048]{1,0:T(2,128)(2,1)} %select_n.78.gain_ref), custom_call_target="tpu_custom_call" | custom-call | flops 1610612736 | bytes 8388608 | tf_op jit(solution)/shard_map/fox_projections/pallas_call | solution.py:389
  68.3 23.5 %all-to-all-start.1 = ((bf16[16,192,128]{2,1,0:T(8,128)(2,1)}), bf16[16,192,128]{2,1,0:T(8,128)(2,1)S(1)}, u32[]{:S(2)}, u32[]{:S(2)}) async-start(bf16[16,192,128]{2,1,0:T(8,128)(2,1)} %get-tuple-element.30), calls=%async_computation.1 | async-start | bytes 1572864 | tf_op jit(solution)/shard_map/all_to_all | solution.py:577
  92.9 1.4 collective-permute-start.5
  94.4 1.4 constant_dynamic-slice_fusion.8
  96.1 1.3 maximum_select_fusion.low_ref
  99.5 2.6 %collective-permute-start.2 = (bf16[256,768]{1,0:T(8,128)(2,1)S(1)}, bf16[256,768]{1,0:T(8,128)(2,1)}, u32[]{:S(2)}, u32[]{:S(2)}) collective-permute-start(bf16[256,768]{1,0:T(8,128)(2,1)S(1)} %get-tuple-element.24), channel_id=1, source_target_pairs={{0,4},{2,6},{4,0},{6,2},{1,5},{3,7},{5,1},{7,3},{8,12},{10,14},{12... | collective-permute-start | bytes 1179656 | tf_op jit(solution)/shard_map/ppermute | solution.py:589
  104.4 4.6 %collective-permute-done.1.rest_1_ = bf16[256,768]{1,0:T(8,128)(2,1)S(1)} collective-permute-done((bf16[256,768]{1,0:T(8,128)(2,1)S(1)}, bf16[256,768]{1,0:T(8,128)(2,1)S(1)}, u32[]{:S(2)}, u32[]{:S(2)}) %collective-permute-start.1) | collective-permute-done | bytes 393248 | tf_op jit(solution)/shard_map/ppermute | solution.py:589
  108.9 9.4 %collective-permute-done.2.rest_2_ = bf16[256,768]{1,0:T(8,128)(2,1)} collective-permute-done((bf16[256,768]{1,0:T(8,128)(2,1)S(1)}, bf16[256,768]{1,0:T(8,128)(2,1)}, u32[]{:S(2)}, u32[]{:S(2)}) %collective-permute-start.2) | collective-permute-done | bytes 393248 | tf_op jit(solution)/shard_map/ppermute | solution.py:589
  118.6 7.8 %lin_projections.1 = (bf16[1024,384]{1,0:T(8,128)(2,1)}, f32[1024,128]{1,0:T(8,128)}, f32[1024,128]{1,0:T(8,128)}) custom-call(s32[2]{0:T(128)} %pad_add_fusion.at_ref, bf16[1024,2048]{1,0:T(8,128)(2,1)} %get-tuple-element.21.normed_ref, bf16[2048,256]{1,0:T(8,128)(2,1)} %maximum_select_fusion.low_ref, bf16[128,128]{1,0:T(8,128)(2,1)} %get-tuple-element.54.decay_up_ref, ...), custom_call_target="tpu_custom_call" | custom-call | flops 2684354560 | bytes 4194304 | tf_op jit(solution)/shard_map/lin_projections/pallas_call | solution.py:444
  126.4 12.0 %position_maps.1 = (bf16[1024,128]{1,0:T(8,128)(2,1)}, f32[1024,128]{1,0:T(8,128)}, bf16[16,64,128]{2,1,0:T(8,128)(2,1)}) custom-call(bf16[1024,384]{1,0:T(8,128)(2,1)} %get-tuple-element.26.proj_ref, f32[1024,128]{1,0:T(8,128)} %get-tuple-element.27.log_ref, f32[1024,128]{1,0:T(8,128)} %get-tuple-element.28.rate_ref, f32[8,2,128]{2,1,0:T(2,128)} %bitcast.69), custom_call_target="tpu_custom_call" | custom-call | flops 1342177280 | bytes 2621440 | tf_op jit(solution)/shard_map/position_maps/pallas_call | solution.py:254
  138.4 11.5 %all-to-all-start.2 = ((bf16[16,64,128]{2,1,0:T(8,128)(2,1)}), bf16[16,64,128]{2,1,0:T(8,128)(2,1)S(1)}, u32[]{:S(2)}, u32[]{:S(2)}) async-start(bf16[16,64,128]{2,1,0:T(8,128)(2,1)} %get-tuple-element.31), calls=%async_computation.2 | async-start | bytes 524288 | tf_op jit(solution)/shard_map/all_to_all | solution.py:577
  151.1 7.1 %attention.1.fox_ref = bf16[16,64,128]{2,1,0:T(8,128)(2,1)} custom-call(bf16[16,192,128]{2,1,0:T(8,128)(2,1)} %copy-done.4, f32[16,128]{1,0:T(8,128)} %dynamic-slice_bitcast_fusion.9.gate_ref), custom_call_target="tpu_custom_call" | custom-call | flops 1073741824 | bytes 1572864 | tf_op jit(solution)/shard_map/attention/pallas_call | solution.py:84
  158.2 4.2 %all-to-all-done.2.maps_ref = bf16[16,64,128]{2,1,0:T(8,128)(2,1)S(1)} async-done(((bf16[16,64,128]{2,1,0:T(8,128)(2,1)}), bf16[16,64,128]{2,1,0:T(8,128)(2,1)S(1)}, u32[]{:S(2)}, u32[]{:S(2)}) %all-to-all-start.2) | async-done | bytes 262176 | tf_op jit(solution)/shard_map/all_to_all | solution.py:577
  163.1 3.8 %states_ahead.1 = bf16[16,96,128]{2,1,0:T(8,128)(2,1)} custom-call(bf16[16,64,128]{2,1,0:T(8,128)(2,1)} %copy-done.3, f32[32,128]{1,0:T(8,128)} %dynamic-slice_bitcast_fusion.8.start_ref, bf16[16,64,128]{2,1,0:T(8,128)(2,1)} %attention.1.fox_ref), custom_call_target="tpu_custom_call" | custom-call | flops 16777216 | bytes 524288 | tf_op jit(solution)/shard_map/states_ahead/pallas_call | solution.py:301
  166.9 10.1 %all-to-all-start.3 = ((bf16[16,96,128]{2,1,0:T(8,128)(2,1)}), bf16[16,96,128]{2,1,0:T(8,128)(2,1)S(1)}, u32[]{:S(2)}, u32[]{:S(2)}) async-start(bf16[16,96,128]{2,1,0:T(8,128)(2,1)} %states_ahead.1), calls=%async_computation.3 | async-start | bytes 786432 | tf_op jit(solution)/shard_map/all_to_all | solution.py:577
  177.1 1.4 dynamic-slice_bitcast_fusion.10.gain_ref
  178.4 16.5 %all-to-all-done.3.back_ref = bf16[16,96,128]{2,1,0:T(8,128)(2,1)S(1)} async-done(((bf16[16,96,128]{2,1,0:T(8,128)(2,1)}), bf16[16,96,128]{2,1,0:T(8,128)(2,1)S(1)}, u32[]{:S(2)}, u32[]{:S(2)}) %all-to-all-start.3) | async-done | bytes 393248 | tf_op jit(solution)/shard_map/all_to_all | solution.py:577
  195.7 2.7 %heads_out.1 = bf16[4,256,256]{2,1,0:T(8,128)(2,1)} custom-call(bf16[16,96,128]{2,1,0:T(8,128)(2,1)} %copy-done.2, bf16[1024,128]{1,0:T(8,128)(2,1)} %get-tuple-element.33.q_ref, f32[1024,128]{1,0:T(8,128)} %get-tuple-element.34.o_ref, bf16[1,128]{1,0:T(2,128)(2,1)} %dynamic-slice_bitcast_fusion.10.gain_ref), custom_call_target="tpu_custom_call" | custom-call | flops 167772160 | bytes 1572864 | tf_op jit(solution)/shard_map/heads_out/pallas_call | solution.py:517
  198.4 6.3 %all-to-all-start.4 = ((bf16[4,256,256]{2,1,0:T(8,128)(2,1)}), bf16[4,256,256]{2,1,0:T(8,128)(2,1)S(1)}, u32[]{:S(2)}, u32[]{:S(2)}) async-start(bf16[4,256,256]{2,1,0:T(8,128)(2,1)} %heads_out.1), calls=%async_computation.4 | async-start | bytes 1048576 | tf_op jit(solution)/shard_map/all_to_all | solution.py:577
  204.7 6.9 %all-to-all-done.4.acts_ref = bf16[4,256,256]{2,1,0:T(8,128)(2,1)S(1)} async-done(((bf16[4,256,256]{2,1,0:T(8,128)(2,1)}), bf16[4,256,256]{2,1,0:T(8,128)(2,1)S(1)}, u32[]{:S(2)}, u32[]{:S(2)}) %all-to-all-start.4) | async-done | bytes 524320 | tf_op jit(solution)/shard_map/all_to_all | solution.py:577
  212.4 5.0 %closing.3 = bf16[128,2048]{1,0:T(8,128)(2,1)} custom-call(s32[1]{0:T(128)} %bitcast.29.seq_ref, bf16[4,256,256]{2,1,0:T(8,128)(2,1)} %copy-done.1, bf16[2048,512]{1,0:T(8,128)(2,1)} %fox_w_ref.3, bf16[2048,512]{1,0:T(8,128)(2,1)} %lin_w_ref.3), custom_call_target="tpu_custom_call" | custom-call | flops 536870912 | bytes 4718592 | tf_op jit(solution)/shard_map/closing/pallas_call | solution.py:554
  217.4 8.0 %collective-permute-start.7 = (bf16[128,2048]{1,0:T(8,128)(2,1)}, bf16[128,2048]{1,0:T(8,128)(2,1)S(1)}, u32[]{:S(2)}, u32[]{:S(2)}) collective-permute-start(bf16[128,2048]{1,0:T(8,128)(2,1)} %closing.3), channel_id=1, source_target_pairs={{0,1},{1,0},{2,3},{3,2},{4,5},{5,4},{6,7},{7,6},{8,9},{9,8},{10,11... | collective-permute-start | bytes 1572872 | tf_op jit(solution)/shard_map/ppermute | solution.py:698
  225.4 5.0 %closing.2 = bf16[128,2048]{1,0:T(8,128)(2,1)} custom-call(s32[1]{0:T(128)} %bitcast.seq_ref, bf16[4,256,256]{2,1,0:T(8,128)(2,1)} %copy-done.1, bf16[2048,512]{1,0:T(8,128)(2,1)} %fox_w_ref.3, bf16[2048,512]{1,0:T(8,128)(2,1)} %lin_w_ref.3), custom_call_target="tpu_custom_call" | custom-call | flops 536870912 | bytes 4718592 | tf_op jit(solution)/shard_map/closing/pallas_call | solution.py:554
  230.4 2.0 fusion
  (58 shorter events, 11.7 us)
Async XLA Ops:
  0.0 91.8 %copy-start = (f32[2,8,64,64]{3,2,1,0:T(8,128)S(1)}, f32[2,8,64,64]{3,2,1,0:T(8,128)}, u32[]{:S(2)}) copy-start(f32[2,8,64,64]{3,2,1,0:T(8,128)} %param.37) | copy-start | bytes 786436
  4.5 29.5 %all-to-all-start = ((bf16[4,256,1792]{2,1,0:T(8,128)(2,1)}), bf16[4,256,1792]{2,1,0:T(8,128)(2,1)}, u32[]{:S(2)}, u32[]{:S(2)}) async-start(bf16[4,256,1792]{2,1,0:T(8,128)(2,1)} %packed.2), calls=%async_computation | async-start | bytes 7340032 | tf_op jit(solution)/shard_map/all_to_all | solution.py:577
  34.0 22.6 %copy-start.8 = (bf16[2048]{0:T(1024)(128)(2,1)S(1)}, bf16[2048]{0:T(1024)(128)(2,1)}, u32[]{:S(2)}) copy-start(bf16[2048]{0:T(1024)(128)(2,1)} %param.21) | copy-start | bytes 12292
  34.0 23.3 %copy-start.9 = (f32[2,128,8]{1,2,0:T(8,128)S(1)}, f32[2,128,8]{1,2,0:T(8,128)}, u32[]{:S(2)}) copy-start(f32[2,128,8]{1,2,0:T(8,128)} %param.32) | copy-start | bytes 24580
  35.8 24.7 %collective-permute-start = (bf16[4,256,1024]{2,1,0:T(8,128)(2,1)S(1)}, bf16[4,256,1024]{2,1,0:T(8,128)(2,1)}, u32[]{:S(2)}, u32[]{:S(2)}) collective-permute-start(bf16[4,256,1024]{2,1,0:T(8,128)(2,1)S(1)} %slice.61), channel_id=1, source_target_pairs={{0,1},{1,0},{2,3},{3,2},{4,5},{5,4},{6,7},{7,6},{8,9},{9,8},{10,11... | collective-permute-start | bytes 6291464 | tf_op jit(solution)/shard_map/ppermute | solution.py:675
  68.3 27.5 %copy-start.5 = (bf16[2048,128]{1,0:T(8,128)(2,1)S(1)}, bf16[2048,128]{1,0:T(8,128)(2,1)}, u32[]{:S(2)}) copy-start(bf16[2048,128]{1,0:T(8,128)(2,1)} %param.29) | copy-start | bytes 1572868
  68.3 27.6 %copy-start.6 = (bf16[2048,128]{1,0:T(8,128)(2,1)S(1)}, bf16[2048,128]{1,0:T(8,128)(2,1)}, u32[]{:S(2)}) copy-start(bf16[2048,128]{1,0:T(8,128)(2,1)} %param.33) | copy-start | bytes 1572868
  68.3 70.1 %all-to-all-start.1 = ((bf16[16,192,128]{2,1,0:T(8,128)(2,1)}), bf16[16,192,128]{2,1,0:T(8,128)(2,1)S(1)}, u32[]{:S(2)}, u32[]{:S(2)}) async-start(bf16[16,192,128]{2,1,0:T(8,128)(2,1)} %get-tuple-element.30), calls=%async_computation.1 | async-start | bytes 1572864 | tf_op jit(solution)/shard_map/all_to_all | solution.py:577
  92.0 10.1 %collective-permute-start.6 = (f32[52,128]{1,0:T(8,128)S(1)}, f32[52,128]{1,0:T(8,128)S(1)}, u32[]{:S(2)}, u32[]{:S(2)}) collective-permute-start(f32[52,128]{1,0:T(8,128)S(1)} %get-tuple-element.50), channel_id=1, source_target_pairs={{0,6},{2,0},{4,2},{6,4},{1,7},{3,1},{5,3},{7,5},{8,14},{10,8},{12,... | collective-permute-start | bytes 79880 | tf_op jit(solution)/shard_map/ppermute | solution.py:589
  92.9 10.8 %collective-permute-start.5 = (f32[52,128]{1,0:T(8,128)S(1)}, f32[52,128]{1,0:T(8,128)S(1)}, u32[]{:S(2)}, u32[]{:S(2)}) collective-permute-start(f32[52,128]{1,0:T(8,128)S(1)} %get-tuple-element.51), channel_id=1, source_target_pairs={{0,4},{2,6},{4,0},{6,2},{1,5},{3,7},{5,1},{7,3},{8,12},{10,14},{12... | collective-permute-start | bytes 79880 | tf_op jit(solution)/shard_map/ppermute | solution.py:589
  94.4 9.3 %collective-permute-start.4 = (f32[52,128]{1,0:T(8,128)S(1)}, f32[52,128]{1,0:T(8,128)S(1)}, u32[]{:S(2)}, u32[]{:S(2)}) collective-permute-start(f32[52,128]{1,0:T(8,128)S(1)} %get-tuple-element.52), channel_id=1, source_target_pairs={{0,2},{2,4},{4,6},{6,0},{1,3},{3,5},{5,7},{7,1},{8,10},{10,12},{12... | collective-permute-start | bytes 79880 | tf_op jit(solution)/shard_map/ppermute | solution.py:589
  96.1 2.1 copy-start.7
  98.2 10.7 %collective-permute-start.1 = (bf16[256,768]{1,0:T(8,128)(2,1)S(1)}, bf16[256,768]{1,0:T(8,128)(2,1)S(1)}, u32[]{:S(2)}, u32[]{:S(2)}) collective-permute-start(bf16[256,768]{1,0:T(8,128)(2,1)S(1)} %copy-done.7), channel_id=1, source_target_pairs={{0,2},{2,4},{4,6},{6,0},{1,3},{3,5},{5,7},{7,1},{8,10},{10,12},{12... | collective-permute-start | bytes 1179656 | tf_op jit(solution)/shard_map/ppermute | solution.py:589
  99.5 18.9 %collective-permute-start.2 = (bf16[256,768]{1,0:T(8,128)(2,1)S(1)}, bf16[256,768]{1,0:T(8,128)(2,1)}, u32[]{:S(2)}, u32[]{:S(2)}) collective-permute-start(bf16[256,768]{1,0:T(8,128)(2,1)S(1)} %get-tuple-element.24), channel_id=1, source_target_pairs={{0,4},{2,6},{4,0},{6,2},{1,5},{3,7},{5,1},{7,3},{8,12},{10,14},{12... | collective-permute-start | bytes 1179656 | tf_op jit(solution)/shard_map/ppermute | solution.py:589
  102.1 16.5 %collective-permute-start.3 = (bf16[256,768]{1,0:T(8,128)(2,1)S(1)}, bf16[256,768]{1,0:T(8,128)(2,1)}, u32[]{:S(2)}, u32[]{:S(2)}) collective-permute-start(bf16[256,768]{1,0:T(8,128)(2,1)S(1)} %get-tuple-element.25), channel_id=1, source_target_pairs={{0,6},{2,0},{4,2},{6,4},{1,7},{3,1},{5,3},{7,5},{8,14},{10,8},{12,... | collective-permute-start | bytes 1179656 | tf_op jit(solution)/shard_map/ppermute | solution.py:589
  108.9 9.7 %copy-start.10 = (bf16[256,768]{1,0:T(8,128)(2,1)}, bf16[256,768]{1,0:T(8,128)(2,1)S(1)}, u32[]{:S(2)}) copy-start(bf16[256,768]{1,0:T(8,128)(2,1)S(1)} %collective-permute-done.1.rest_1_) | copy-start | bytes 1179652
  138.4 12.7 %copy-start.4 = (bf16[16,192,128]{2,1,0:T(8,128)(2,1)}, bf16[16,192,128]{2,1,0:T(8,128)(2,1)S(1)}, u32[]{:S(2)}) copy-start(bf16[16,192,128]{2,1,0:T(8,128)(2,1)S(1)} %all-to-all-done.1.blocks_ref) | copy-start | bytes 2359300
  138.4 24.0 %all-to-all-start.2 = ((bf16[16,64,128]{2,1,0:T(8,128)(2,1)}), bf16[16,64,128]{2,1,0:T(8,128)(2,1)S(1)}, u32[]{:S(2)}, u32[]{:S(2)}) async-start(bf16[16,64,128]{2,1,0:T(8,128)(2,1)} %get-tuple-element.31), calls=%async_computation.2 | async-start | bytes 524288 | tf_op jit(solution)/shard_map/all_to_all | solution.py:577
  162.4 0.7 copy-start.3
  166.9 28.0 %all-to-all-start.3 = ((bf16[16,96,128]{2,1,0:T(8,128)(2,1)}), bf16[16,96,128]{2,1,0:T(8,128)(2,1)S(1)}, u32[]{:S(2)}, u32[]{:S(2)}) async-start(bf16[16,96,128]{2,1,0:T(8,128)(2,1)} %states_ahead.1), calls=%async_computation.3 | async-start | bytes 786432 | tf_op jit(solution)/shard_map/all_to_all | solution.py:577
  195.0 0.7 copy-start.2
  198.4 13.2 %all-to-all-start.4 = ((bf16[4,256,256]{2,1,0:T(8,128)(2,1)}), bf16[4,256,256]{2,1,0:T(8,128)(2,1)S(1)}, u32[]{:S(2)}, u32[]{:S(2)}) async-start(bf16[4,256,256]{2,1,0:T(8,128)(2,1)} %heads_out.1), calls=%async_computation.4 | async-start | bytes 1048576 | tf_op jit(solution)/shard_map/all_to_all | solution.py:577
  211.6 0.8 copy-start.1
  217.4 13.0 %collective-permute-start.7 = (bf16[128,2048]{1,0:T(8,128)(2,1)}, bf16[128,2048]{1,0:T(8,128)(2,1)S(1)}, u32[]{:S(2)}, u32[]{:S(2)}) collective-permute-start(bf16[128,2048]{1,0:T(8,128)(2,1)} %closing.3), channel_id=1, source_target_pairs={{0,1},{1,0},{2,3},{3,2},{4,5},{5,4},{6,7},{7,6},{8,9},{9,8},{10,11... | collective-permute-start | bytes 1572872 | tf_op jit(solution)/shard_map/ppermute | solution.py:698

commit v5 on v4

--- a/solution.py
+++ b/solution.py
@@ -1,3 +1,5 @@
+import functools
+
 import jax
 import jax.numpy as jnp
 from jax import lax
@@ -9,7 +11,8 @@
 CHUNK = 64
 F32 = jnp.float32
 BF16 = jnp.bfloat16
-VMEM_BYTES = 56 * 1024 * 1024
+MIB = 1024 * 1024
+VMEM_BYTES = 56 * MIB
 
 MM = (((1,), (0,)), ((), ()))
 NT = (((1,), (1,)), ((), ()))
@@ -90,7 +93,7 @@
             pltpu.VMEM((count * width, 2 * HEAD_CHANNELS), BF16),
             pltpu.VMEM((HEAD_CHANNELS, count * width), BF16),
         ],
-        compiler_params=pltpu.CompilerParams(vmem_limit_bytes=VMEM_BYTES),
+        compiler_params=pltpu.CompilerParams(vmem_limit_bytes=16 * MIB),
         cost_estimate=pl.CostEstimate(
             flops=4 * HEAD_CHANNELS * (count * width) ** 2,
             bytes_accessed=4 * count * rows * width,
@@ -270,7 +273,7 @@
             pl.BlockSpec((group * tok_count, lanes), lambda s: (s, 0)),
             pl.BlockSpec((group * heads, HEAD_CHANNELS, lanes), lambda s: (s, 0, 0)),
         ),
-        compiler_params=pltpu.CompilerParams(vmem_limit_bytes=VMEM_BYTES),
+        compiler_params=pltpu.CompilerParams(vmem_limit_bytes=24 * MIB),
         cost_estimate=pl.CostEstimate(
             flops=rows * lanes * 2 * 256 * 20,
             bytes_accessed=rows * lanes * 20,
@@ -303,6 +306,7 @@
         out_shape=jax.ShapeDtypeStruct((count, 3 * HEAD_CHANNELS // 2, 2 * HEAD_CHANNELS), BF16),
         in_specs=[whole, whole, whole],
         out_specs=whole,
+        compiler_params=pltpu.CompilerParams(vmem_limit_bytes=16 * MIB),
         cost_estimate=pl.CostEstimate(
             flops=count * 4 * HEAD_CHANNELS**3, bytes_accessed=1 << 19, transcendentals=0
         ),
@@ -310,30 +314,46 @@
     )(maps, start, fox)
 
 
-def halves(weights):
-    rows = weights[0].shape[0] // 2
-    return [w[k * rows : (k + 1) * rows, :] for k in range(2) for w in weights]
-
-
-def pack_kernel(*refs):
-    out_ref = refs[-1]
-    at = 0
-    for piece in [r[...] for r in refs[:-4]] + halves([r[...] for r in refs[-4:-1]]):
-        out_ref[0, :, at : at + piece.shape[1]] = piece
-        at += piece.shape[1]
+def pack_kernel(groups, *refs):
+    *piece_refs, out_ref, sems = refs
+    leading, weights = piece_refs[:-3], piece_refs[-3:]
+    rows = out_ref.shape[1]
+    lanes = weights[0].shape[1] // groups
+    copies = []
+
+    def send(source, group, at, width):
+        copies.append(
+            pltpu.make_async_copy(
+                source, out_ref.at[group, :, at : at + width], sems.at[len(copies)]
+            )
+        )
+
+    for g in range(groups):
+        at = 0
+        for ref in leading:
+            send(ref, g, at, ref.shape[1])
+            at += ref.shape[1]
+        for k in range(2):
+            for ref in weights:
+                block = ref.at[k * rows : (k + 1) * rows, g * lanes : (g + 1) * lanes]
+                send(block, g, at, lanes)
+                at += lanes
+    for copy in copies:
+        copy.start()
+    for copy in copies:
+        copy.wait()
 
 
 def packed(leading, weights, groups):
     rows, cols = weights[0].shape
-    lanes = cols // groups
-    width = sum(x.shape[1] for x in leading) + 6 * lanes
+    width = sum(x.shape[1] for x in leading) + 6 * cols // groups
     whole = pl.BlockSpec(memory_space=pltpu.VMEM)
     return pl.pallas_call(
-        pack_kernel,
-        grid=(groups,),
+        functools.partial(pack_kernel, groups),
         out_shape=jax.ShapeDtypeStruct((groups, rows // 2, width), BF16),
-        in_specs=[whole] * len(leading) + [pl.BlockSpec((rows, lanes), lambda g: (0, g))] * 3,
-        out_specs=pl.BlockSpec((1, rows // 2, width), lambda g: (g, 0, 0)),
+        in_specs=[whole] * (len(leading) + 3),
+        out_specs=pl.BlockSpec(memory_space=pl.ANY),
+        scratch_shapes=[pltpu.SemaphoreType.DMA((groups * (len(leading) + 6),))],
         compiler_params=pltpu.CompilerParams(vmem_limit_bytes=VMEM_BYTES),
         cost_estimate=pl.CostEstimate(
             flops=1 << 20, bytes_accessed=4 * groups * rows * width, transcendentals=0
@@ -342,25 +362,37 @@
     )(*leading, *weights)
 
 
-def fox_kernel(at_ref, mine_ref, other_ref, gain_ref, fox_ref, normed_ref, weight_scr):
+def fox_kernel(
+    at_ref,
+    mine_ref,
+    other_ref,
+    first_ref,
+    second_ref,
+    third_ref,
+    gain_ref,
+    fox_ref,
+    normed_ref,
+    weight_scr,
+):
     n = HEAD_CHANNELS
-    groups, rows, width = other_ref.shape
+    groups = first_ref.shape[0]
+    _, rows, width = other_ref.shape
     pairs, _, tok_count = fox_ref.shape
     heads = pairs * tok_count // rows
     lanes = heads * n
-    step = pl.program_id(0)
-
-    @pl.when(step == 0)
+
+    @pl.when(pl.program_id(0) == 0)
     def _():
         for i in range(groups):
             source = lax.rem(i + at_ref[0] * (groups // 2), groups)
-            for k in range(2):
-                at = width + 3 * k * lanes
-                weight_scr[(2 * i + k) * rows : (2 * i + k + 1) * rows, :] = mine_ref[
-                    source, :, at : at + 3 * lanes
-                ]
-
-    pieces = [mine_ref[step, :, :width].astype(F32), other_ref[step].astype(F32)]
+            upper = slice(2 * i * rows, (2 * i + 1) * rows)
+            lower = slice((2 * i + 1) * rows, (2 * i + 2) * rows)
+            weight_scr[upper, : 2 * lanes] = first_ref[source]
+            weight_scr[upper, 2 * lanes :] = second_ref[source, :, :lanes]
+            weight_scr[lower, :lanes] = second_ref[source, :, lanes:]
+            weight_scr[lower, lanes:] = third_ref[source]
+
+    pieces = [mine_ref[0].astype(F32), other_ref[0].astype(F32)]
     square = sum(jnp.sum(x * x, axis=1, keepdims=True) for x in pieces)
     scaling = lax.rsqrt(square / (2 * width) + 1e-06)
     normed = jnp.concatenate(
@@ -393,20 +425,29 @@
             jax.ShapeDtypeStruct((groups * pairs, 3 * HEAD_CHANNELS, tok_count), BF16),
             jax.ShapeDtypeStruct((groups * rows, 2 * width), BF16),
         ),
-        in_specs=[pl.BlockSpec(memory_space=pltpu.SMEM), whole, whole, whole],
+        in_specs=[
+            pl.BlockSpec(memory_space=pltpu.SMEM),
+            pl.BlockSpec((1, rows, width), lambda g: (g, 0, 0)),
+            pl.BlockSpec((1, rows, width), lambda g: (g, 0, 0)),
+            *(
+                pl.BlockSpec((groups, rows, 2 * lanes), lambda g, at=at: (0, 0, at))
+                for at in range(width // (2 * lanes), width // (2 * lanes) + 3)
+            ),
+            whole,
+        ],
         out_specs=(
             pl.BlockSpec((pairs, 3 * HEAD_CHANNELS, tok_count), lambda g: (g, 0, 0)),
             pl.BlockSpec((rows, 2 * width), lambda g: (g, 0)),
         ),
         scratch_shapes=[pltpu.VMEM((2 * width, 3 * lanes), BF16)],
-        compiler_params=pltpu.CompilerParams(vmem_limit_bytes=VMEM_BYTES),
+        compiler_params=pltpu.CompilerParams(vmem_limit_bytes=24 * MIB),
         cost_estimate=pl.CostEstimate(
             flops=12 * groups * rows * width * lanes,
             bytes_accessed=8 * groups * rows * width,
             transcendentals=0,
         ),
         name="fox_projections",
-    )(at, mine, other, gain)
+    )(at, mine, other, mine, mine, mine, gain)
 
 
 def lin_kernel(at_ref, normed_ref, low_ref, decay_up_ref, rate_up_ref, base_ref, *rest):
@@ -460,7 +501,7 @@
             pl.BlockSpec((tall, lanes), lambda s: (s, 0)),
         ),
         scratch_shapes=[pltpu.VMEM((width, 3 * lanes), BF16)],
-        compiler_params=pltpu.CompilerParams(vmem_limit_bytes=VMEM_BYTES),
+        compiler_params=pltpu.CompilerParams(vmem_limit_bytes=24 * MIB),
         cost_estimate=pl.CostEstimate(
             flops=10 * rows * width * lanes,
             bytes_accessed=2 * rows * width,
@@ -519,7 +560,7 @@
         out_shape=jax.ShapeDtypeStruct((groups, rows // groups, 2 * lanes), BF16),
         in_specs=[whole] * 4,
         out_specs=whole,
-        compiler_params=pltpu.CompilerParams(vmem_limit_bytes=VMEM_BYTES),
+        compiler_params=pltpu.CompilerParams(vmem_limit_bytes=16 * MIB),
         cost_estimate=pl.CostEstimate(
             flops=10 * rows * lanes * lanes, bytes_accessed=12 * rows * lanes, transcendentals=0
         ),
@@ -540,10 +581,10 @@
             act_scr[:, g * lanes : (g + 1) * lanes] = acts_ref[g, here, :lanes]
             act_scr[:, cols + g * lanes : cols + (g + 1) * lanes] = acts_ref[g, here, lanes:]
 
-    out_ref[...] = (
-        lax.dot_general(act_scr[:, :cols], fox_w_ref[...], NT, preferred_element_type=F32)
-        + lax.dot_general(act_scr[:, cols:], lin_w_ref[...], NT, preferred_element_type=F32)
-    ).astype(BF16)
+    turned = lax.dot_general(
+        fox_w_ref[...], act_scr[:, :cols], NT, preferred_element_type=F32
+    ) + lax.dot_general(lin_w_ref[...], act_scr[:, cols:], NT, preferred_element_type=F32)
+    out_ref[...] = turned.T.astype(BF16)
 
 
 def closing(part, parts, acts, fox_w, lin_w):
@@ -563,7 +604,7 @@
         ],
         out_specs=pl.BlockSpec((rows, tile), lambda i: (0, i)),
         scratch_shapes=[pltpu.VMEM((rows, 2 * cols), BF16)],
-        compiler_params=pltpu.CompilerParams(vmem_limit_bytes=VMEM_BYTES),
+        compiler_params=pltpu.CompilerParams(vmem_limit_bytes=16 * MIB),
         cost_estimate=pl.CostEstimate(
             flops=4 * rows * cols * width,
             bytes_accessed=4 * cols * width + 2 * rows * width,

time: 234 us -> 225 us (0.962)
  Pallas kernels: 59.4 us -> 42.9 us
  local copies, waits for them, and re-layouts: 13.1 us -> 19 us
  waiting for transfers between devices: 61.9 us -> 67.4 us
  other arithmetic: 5.24 us -> 1.39 us
    unnamed x25 -> x35, local copies, waits for them, and re-layouts: 2.38 us -> 9.28 us
    pallas_call x2, Pallas kernels: 9.97 us -> 4.39 us  [closing(): pl.pallas_call(closing_kernel, grid=(width // tile,), out_shape=jax.Shape...]
  transfers between devices with their start and end apart: 13 -> 13, of which waited for: 8 -> 8; matrix products, arithmetic and copies ran while one was open for 5% -> 3% of each run, Pallas kernels for 15% -> 12%
where the time goes in v5:
time: 225 us; the launch traced here: 224 us
  starting transfers between devices  92.8 us (41%)
  waiting for transfers between devices  67.4 us (30%)
  Pallas kernels  42.9 us (19%)
  local copies, waits for them, and re-layouts  19 us (8%)
    all_to_all x5, starting transfers between devices, exchange(): return lax.all_to_all(x, axis, 0, 0, tiled=True)  56.7 us
    all_to_all x5, waiting for transfers between devices, exchange(): return lax.all_to_all(x, axis, 0, 0, tiled=True)  48 us
    ppermute x1, starting transfers between devices, per_device(): other = lax.ppermute(mine[:, :, :half_width], 'tp', swap)  20.7 us
    ppermute x6, waiting for transfers between devices, by_permutes(): lax.ppermute(block, axis, [(i, (i + d) % size) for i in range(size)])  15.8 us
    pallas_call x1, Pallas kernels, position_maps(): pl.pallas_call(maps_kernel, grid=(seqs // group,), out_shape=(jax.ShapeDt...  10.7 us
    unnamed x35, local copies, waits for them, and re-layouts  9.28 us
    ppermute x1, starting transfers between devices, per_device(): theirs = lax.ppermute(theirs, 'tp', swap)  8.14 us
    ppermute x6, starting transfers between devices, by_permutes(): lax.ppermute(block, axis, [(i, (i + d) % size) for i in range(size)])  7.25 us
  transfers between devices with their start and end apart: 13, of which 8 were waited for; matrix products, arithmetic and copies ran while one was open for 3% of the time, Pallas kernels for 12%

profile of v5, /device:TPU:33, one launch (start us, length us, event | category | flops | bytes accessed | tf_op | source)
XLA Modules:
  0.0 223.9 jit_solution(14441529130718693252)
XLA Ops:
  0.0 3.6 %packed.2 = bf16[4,256,1792]{2,1,0:T(8,128)(2,1)} custom-call(bf16[256,1024]{1,0:T(8,128)(2,1)} %bitcast.62, bf16[512,512]{1,0:T(8,128)(2,1)} %refs_1_.2, bf16[512,512]{1,0:T(8,128)(2,1)} %refs_2_.2, bf16[512,512]{1,0:T(8,128)(2,1)} %refs_3_.1), custom_call_target="tpu_custom_call" | custom-call | flops 1048576 | bytes 14680064 | tf_op jit(solution)/shard_map/packed/pallas_call | solution.py:351
  3.6 5.1 %all-to-all-start = ((bf16[4,256,1792]{2,1,0:T(8,128)(2,1)}), bf16[4,256,1792]{2,1,0:T(8,128)(2,1)}, u32[]{:S(2)}, u32[]{:S(2)}) async-start(bf16[4,256,1792]{2,1,0:T(8,128)(2,1)} %packed.2), calls=%async_computation | async-start | bytes 7340032 | tf_op jit(solution)/shard_map/all_to_all | solution.py:618
  8.8 2.8 %packed.3 = bf16[4,256,768]{2,1,0:T(8,128)(2,1)} custom-call(bf16[512,512]{1,0:T(8,128)(2,1)} %refs_0_.1, bf16[512,512]{1,0:T(8,128)(2,1)} %refs_1_.3, bf16[512,512]{1,0:T(8,128)(2,1)} %refs_2_.3), custom_call_target="tpu_custom_call" | custom-call | flops 1048576 | bytes 6291456 | tf_op jit(solution)/shard_map/packed/pallas_call | solution.py:351
  11.6 2.4 %dynamic-slice_bitcast_fusion = (bf16[256,768]{1,0:T(8,128)(2,1)}, bf16[256,768]{1,0:T(8,128)(2,1)}, bf16[256,768]{1,0:T(8,128)(2,1)}, bf16[256,768]{1,0:T(8,128)(2,1)S(1)}) fusion(bf16[4,256,768]{2,1,0:T(8,128)(2,1)} %packed.3, s32[]{:T(128)S(6)} %select_n.75, s32[]{:T(128)S(6)} %select_n.74, s32[]{:T(128)S(6)} %select_n.73, s32[]{:T(128)S(6)} %select_n.72), kind=kLoop, calls=%fused_computation.3 | loop fusion | bytes 3145744 | tf_op jit(solution)/shard_map/jit(dynamic_index_in_dim)/squeeze | solution.py:624
  14.0 19.2 %all-to-all-done.mine_ref.first_ref.second_ref.third_ref = bf16[4,256,1792]{2,1,0:T(8,128)(2,1)} async-done(((bf16[4,256,1792]{2,1,0:T(8,128)(2,1)}), bf16[4,256,1792]{2,1,0:T(8,128)(2,1)}, u32[]{:S(2)}, u32[]{:S(2)}) %all-to-all-start) | async-done | bytes 3670048 | tf_op jit(solution)/shard_map/all_to_all | solution.py:618
  33.2 3.1 %slice.61 = bf16[4,256,1024]{2,1,0:T(8,128)(2,1)} slice(bf16[4,256,1792]{2,1,0:T(8,128)(2,1)} %all-to-all-done.mine_ref.first_ref.second_ref.third_ref), slice={[0:4], [0:256], [0:1024]} | slice | bytes 4194304 | tf_op jit(solution)/shard_map/slice | solution.py:716
  36.3 20.7 %collective-permute-start = (bf16[4,256,1024]{2,1,0:T(8,128)(2,1)}, bf16[4,256,1024]{2,1,0:T(8,128)(2,1)S(1)}, u32[]{:S(2)}, u32[]{:S(2)}) collective-permute-start(bf16[4,256,1024]{2,1,0:T(8,128)(2,1)} %slice.61), channel_id=1, source_target_pairs={{0,1},{1,0},{2,3},{3,2},{4,5},{5,4},{6,7},{7,6},{8,9},{9,8},{10,11... | collective-permute-start | bytes 6291464 | tf_op jit(solution)/shard_map/ppermute | solution.py:716
  57.3 3.6 %collective-permute-done.other_ref = bf16[4,256,1024]{2,1,0:T(8,128)(2,1)S(1)} collective-permute-done((bf16[4,256,1024]{2,1,0:T(8,128)(2,1)}, bf16[4,256,1024]{2,1,0:T(8,128)(2,1)S(1)}, u32[]{:S(2)}, u32[]{:S(2)}) %collective-permute-start) | collective-permute-done | bytes 2097184 | tf_op jit(solution)/shard_map/ppermute | solution.py:716
  61.0 6.7 %fox_projections.1 = (bf16[16,192,128]{2,1,0:T(8,128)(2,1)}, bf16[1024,2048]{1,0:T(8,128)(2,1)S(1)}) custom-call(s32[2]{0:T(128)S(1)} %pad_add_fusion.at_ref, bf16[4,256,1792]{2,1,0:T(8,128)(2,1)} %all-to-all-done.mine_ref.first_ref.second_ref.third_ref, bf16[4,256,1024]{2,1,0:T(8,128)(2,1)S(1)} %collective-permute-done.other_ref, ...), custom_call_target="tpu_custom_call" | custom-call | flops 1610612736 | bytes 8388608 | tf_op jit(solution)/shard_map/fox_projections/pallas_call | solution.py:421
  67.6 2.0 copy-done.8
  69.6 23.5 %all-to-all-start.1 = ((bf16[16,192,128]{2,1,0:T(8,128)(2,1)}), bf16[16,192,128]{2,1,0:T(8,128)(2,1)S(1)}, u32[]{:S(2)}, u32[]{:S(2)}) async-start(bf16[16,192,128]{2,1,0:T(8,128)(2,1)} %get-tuple-element.30), calls=%async_computation.1 | async-start | bytes 1572864 | tf_op jit(solution)/shard_map/all_to_all | solution.py:618
  94.3 1.4 collective-permute-start.5
  97.9 1.2 collective-permute-start.1
  99.1 2.6 %collective-permute-start.2 = (bf16[256,768]{1,0:T(8,128)(2,1)}, bf16[256,768]{1,0:T(8,128)(2,1)}, u32[]{:S(2)}, u32[]{:S(2)}) collective-permute-start(bf16[256,768]{1,0:T(8,128)(2,1)} %get-tuple-element.24), channel_id=1, source_target_pairs={{0,4},{2,6},{4,0},{6,2},{1,5},{3,7},{5,1},{7,3},{8,12},{10,14},{12... | collective-permute-start | bytes 1179656 | tf_op jit(solution)/shard_map/ppermute | solution.py:630
  101.8 1.0 collective-permute-start.3
  102.8 5.9 %collective-permute-done.1.rest_1_ = bf16[256,768]{1,0:T(8,128)(2,1)S(1)} collective-permute-done((bf16[256,768]{1,0:T(8,128)(2,1)}, bf16[256,768]{1,0:T(8,128)(2,1)S(1)}, u32[]{:S(2)}, u32[]{:S(2)}) %collective-permute-start.1) | collective-permute-done | bytes 393248 | tf_op jit(solution)/shard_map/ppermute | solution.py:630
  108.8 9.4 %collective-permute-done.2.rest_2_ = bf16[256,768]{1,0:T(8,128)(2,1)} collective-permute-done((bf16[256,768]{1,0:T(8,128)(2,1)}, bf16[256,768]{1,0:T(8,128)(2,1)}, u32[]{:S(2)}, u32[]{:S(2)}) %collective-permute-start.2) | collective-permute-done | bytes 393248 | tf_op jit(solution)/shard_map/ppermute | solution.py:630
  118.6 2.2 copy-done.9
  120.8 6.1 %lin_projections.1 = (bf16[1024,384]{1,0:T(8,128)(2,1)S(1)}, f32[1024,128]{1,0:T(8,128)S(1)}, f32[1024,128]{1,0:T(8,128)S(1)}) custom-call(s32[2]{0:T(128)S(1)} %pad_add_fusion.at_ref, bf16[1024,2048]{1,0:T(8,128)(2,1)S(1)} %copy-done.9, bf16[2048,256]{1,0:T(8,128)(2,1)S(1)} %maximum_select_fusion.low_ref, ...), custom_call_target="tpu_custom_call" | custom-call | flops 2684354560 | bytes 4194304 | tf_op jit(solution)/shard_map/lin_projections/pallas_call | solution.py:485
  126.8 10.7 %position_maps.1 = (bf16[1024,128]{1,0:T(8,128)(2,1)S(1)}, f32[1024,128]{1,0:T(8,128)S(1)}, bf16[16,64,128]{2,1,0:T(8,128)(2,1)}) custom-call(bf16[1024,384]{1,0:T(8,128)(2,1)S(1)} %get-tuple-element.26.proj_ref, f32[1024,128]{1,0:T(8,128)S(1)} %get-tuple-element.27.log_ref, f32[1024,128]{1,0:T(8,128)S(1)} %get-tuple-element.28.rate_ref, ...), custom_call_target="tpu_custom_call" | custom-call | flops 1342177280 | bytes 2621440 | tf_op jit(solution)/shard_map/position_maps/pallas_call | solution.py:257
  137.6 11.5 %all-to-all-start.2 = ((bf16[16,64,128]{2,1,0:T(8,128)(2,1)}), bf16[16,64,128]{2,1,0:T(8,128)(2,1)S(1)}, u32[]{:S(2)}, u32[]{:S(2)}) async-start(bf16[16,64,128]{2,1,0:T(8,128)(2,1)} %get-tuple-element.31), calls=%async_computation.2 | async-start | bytes 524288 | tf_op jit(solution)/shard_map/all_to_all | solution.py:618
  150.5 5.2 %attention.1.fox_ref = bf16[16,64,128]{2,1,0:T(8,128)(2,1)S(1)} custom-call(bf16[16,192,128]{2,1,0:T(8,128)(2,1)S(1)} %all-to-all-done.1.blocks_ref, f32[16,128]{1,0:T(8,128)S(1)} %dynamic-slice_bitcast_fusion.9.gate_ref), custom_call_target="tpu_custom_call" | custom-call | flops 1073741824 | bytes 1572864 | tf_op jit(solution)/shard_map/attention/pallas_call | solution.py:87
  156.4 5.1 %all-to-all-done.2.maps_ref = bf16[16,64,128]{2,1,0:T(8,128)(2,1)S(1)} async-done(((bf16[16,64,128]{2,1,0:T(8,128)(2,1)}), bf16[16,64,128]{2,1,0:T(8,128)(2,1)S(1)}, u32[]{:S(2)}, u32[]{:S(2)}) %all-to-all-start.2) | async-done | bytes 262176 | tf_op jit(solution)/shard_map/all_to_all | solution.py:618
  162.5 2.8 %states_ahead.1 = bf16[16,96,128]{2,1,0:T(8,128)(2,1)} custom-call(bf16[16,64,128]{2,1,0:T(8,128)(2,1)S(1)} %all-to-all-done.2.maps_ref, f32[32,128]{1,0:T(8,128)S(1)} %dynamic-slice_bitcast_fusion.8.start_ref, bf16[16,64,128]{2,1,0:T(8,128)(2,1)S(1)} %copy-done.7), custom_call_target="tpu_custom_call" | custom-call | flops 16777216 | bytes 524288 | tf_op jit(solution)/shard_map/states_ahead/pallas_call | solution.py:304
  165.3 10.0 %all-to-all-start.3 = ((bf16[16,96,128]{2,1,0:T(8,128)(2,1)}), bf16[16,96,128]{2,1,0:T(8,128)(2,1)S(1)}, u32[]{:S(2)}, u32[]{:S(2)}) async-start(bf16[16,96,128]{2,1,0:T(8,128)(2,1)} %states_ahead.1), calls=%async_computation.3 | async-start | bytes 786432 | tf_op jit(solution)/shard_map/all_to_all | solution.py:618
  176.1 16.8 %all-to-all-done.3.back_ref = bf16[16,96,128]{2,1,0:T(8,128)(2,1)S(1)} async-done(((bf16[16,96,128]{2,1,0:T(8,128)(2,1)}), bf16[16,96,128]{2,1,0:T(8,128)(2,1)S(1)}, u32[]{:S(2)}, u32[]{:S(2)}) %all-to-all-start.3) | async-done | bytes 393248 | tf_op jit(solution)/shard_map/all_to_all | solution.py:618
  195.3 6.6 %all-to-all-start.4 = ((bf16[4,256,256]{2,1,0:T(8,128)(2,1)}), bf16[4,256,256]{2,1,0:T(8,128)(2,1)S(1)}, u32[]{:S(2)}, u32[]{:S(2)}) async-start(bf16[4,256,256]{2,1,0:T(8,128)(2,1)} %copy-done.3), calls=%async_computation.4 | async-start | bytes 1048576 | tf_op jit(solution)/shard_map/all_to_all | solution.py:618
  201.9 6.9 %all-to-all-done.4.acts_ref = bf16[4,256,256]{2,1,0:T(8,128)(2,1)S(1)} async-done(((bf16[4,256,256]{2,1,0:T(8,128)(2,1)}), bf16[4,256,256]{2,1,0:T(8,128)(2,1)S(1)}, u32[]{:S(2)}, u32[]{:S(2)}) %all-to-all-start.4) | async-done | bytes 524320 | tf_op jit(solution)/shard_map/all_to_all | solution.py:618
  208.9 1.6 copy-done.2
  210.5 2.2 closing.3
  212.7 8.1 %collective-permute-start.7 = (bf16[128,2048]{1,0:T(8,128)(2,1)S(1)}, bf16[128,2048]{1,0:T(8,128)(2,1)S(1)}, u32[]{:S(2)}, u32[]{:S(2)}) collective-permute-start(bf16[128,2048]{1,0:T(8,128)(2,1)S(1)} %closing.3), channel_id=1, source_target_pairs={{0,1},{1,0},{2,3},{3,2},{4,5},{5,4},{6,7},{7,6},{8,9},{9,8},{10,11... | collective-permute-start | bytes 1572872 | tf_op jit(solution)/shard_map/ppermute | solution.py:739
  220.8 2.2 closing.2
  (68 shorter events, 11.2 us)
Async XLA Ops:
  0.0 93.1 %copy-start = (f32[2,8,64,64]{3,2,1,0:T(8,128)S(1)}, f32[2,8,64,64]{3,2,1,0:T(8,128)}, u32[]{:S(2)}) copy-start(f32[2,8,64,64]{3,2,1,0:T(8,128)} %param.37) | copy-start | bytes 786436
  3.6 29.5 %all-to-all-start = ((bf16[4,256,1792]{2,1,0:T(8,128)(2,1)}), bf16[4,256,1792]{2,1,0:T(8,128)(2,1)}, u32[]{:S(2)}, u32[]{:S(2)}) async-start(bf16[4,256,1792]{2,1,0:T(8,128)(2,1)} %packed.2), calls=%async_computation | async-start | bytes 7340032 | tf_op jit(solution)/shard_map/all_to_all | solution.py:618
  33.1 23.8 %copy-start.14 = (bf16[2048]{0:T(1024)(128)(2,1)S(1)}, bf16[2048]{0:T(1024)(128)(2,1)}, u32[]{:S(2)}) copy-start(bf16[2048]{0:T(1024)(128)(2,1)} %param.21) | copy-start | bytes 12292
  33.1 23.9 %copy-start.15 = (f32[2,128,8]{1,2,0:T(8,128)S(1)}, f32[2,128,8]{1,2,0:T(8,128)}, u32[]{:S(2)}) copy-start(f32[2,128,8]{1,2,0:T(8,128)} %param.32) | copy-start | bytes 24580
  33.2 24.0 %copy-start.13 = (f32[2,2048,8]{1,2,0:T(8,128)S(1)}, f32[2,2048,8]{1,2,0:T(8,128)}, u32[]{:S(2)}) copy-start(f32[2,2048,8]{1,2,0:T(8,128)} %param.25) | copy-start | bytes 393220
  36.3 24.7 %collective-permute-start = (bf16[4,256,1024]{2,1,0:T(8,128)(2,1)}, bf16[4,256,1024]{2,1,0:T(8,128)(2,1)S(1)}, u32[]{:S(2)}, u32[]{:S(2)}) collective-permute-start(bf16[4,256,1024]{2,1,0:T(8,128)(2,1)} %slice.61), channel_id=1, source_target_pairs={{0,1},{1,0},{2,3},{3,2},{4,5},{5,4},{6,7},{7,6},{8,9},{9,8},{10,11... | collective-permute-start | bytes 6291464 | tf_op jit(solution)/shard_map/ppermute | solution.py:716
  67.6 2.0 copy-start.8
  69.6 26.9 %copy-start.10 = (bf16[2048,128]{1,0:T(8,128)(2,1)S(1)}, bf16[2048,128]{1,0:T(8,128)(2,1)}, u32[]{:S(2)}) copy-start(bf16[2048,128]{1,0:T(8,128)(2,1)} %param.29) | copy-start | bytes 1572868
  69.6 27.0 %copy-start.11 = (bf16[2048,128]{1,0:T(8,128)(2,1)S(1)}, bf16[2048,128]{1,0:T(8,128)(2,1)}, u32[]{:S(2)}) copy-start(bf16[2048,128]{1,0:T(8,128)(2,1)} %param.33) | copy-start | bytes 1572868
  69.6 67.9 %all-to-all-start.1 = ((bf16[16,192,128]{2,1,0:T(8,128)(2,1)}), bf16[16,192,128]{2,1,0:T(8,128)(2,1)S(1)}, u32[]{:S(2)}, u32[]{:S(2)}) async-start(bf16[16,192,128]{2,1,0:T(8,128)(2,1)} %get-tuple-element.30), calls=%async_computation.1 | async-start | bytes 1572864 | tf_op jit(solution)/shard_map/all_to_all | solution.py:618
  93.3 8.4 %collective-permute-start.6 = (f32[52,128]{1,0:T(8,128)S(1)}, f32[52,128]{1,0:T(8,128)S(1)}, u32[]{:S(2)}, u32[]{:S(2)}) collective-permute-start(f32[52,128]{1,0:T(8,128)S(1)} %get-tuple-element.50), channel_id=1, source_target_pairs={{0,6},{2,0},{4,2},{6,4},{1,7},{3,1},{5,3},{7,5},{8,14},{10,8},{12,... | collective-permute-start | bytes 79880 | tf_op jit(solution)/shard_map/ppermute | solution.py:630
  94.3 8.5 %collective-permute-start.5 = (f32[52,128]{1,0:T(8,128)S(1)}, f32[52,128]{1,0:T(8,128)S(1)}, u32[]{:S(2)}, u32[]{:S(2)}) collective-permute-start(f32[52,128]{1,0:T(8,128)S(1)} %get-tuple-element.51), channel_id=1, source_target_pairs={{0,4},{2,6},{4,0},{6,2},{1,5},{3,7},{5,1},{7,3},{8,12},{10,14},{12... | collective-permute-start | bytes 79880 | tf_op jit(solution)/shard_map/ppermute | solution.py:630
  95.7 7.0 %collective-permute-start.4 = (f32[52,128]{1,0:T(8,128)S(1)}, f32[52,128]{1,0:T(8,128)S(1)}, u32[]{:S(2)}, u32[]{:S(2)}) collective-permute-start(f32[52,128]{1,0:T(8,128)S(1)} %get-tuple-element.52), channel_id=1, source_target_pairs={{0,2},{2,4},{4,6},{6,0},{1,3},{3,5},{5,7},{7,1},{8,10},{10,12},{12... | collective-permute-start | bytes 79880 | tf_op jit(solution)/shard_map/ppermute | solution.py:630
  97.9 10.9 %collective-permute-start.1 = (bf16[256,768]{1,0:T(8,128)(2,1)}, bf16[256,768]{1,0:T(8,128)(2,1)S(1)}, u32[]{:S(2)}, u32[]{:S(2)}) collective-permute-start(bf16[256,768]{1,0:T(8,128)(2,1)} %get-tuple-element.23), channel_id=1, source_target_pairs={{0,2},{2,4},{4,6},{6,0},{1,3},{3,5},{5,7},{7,1},{8,10},{10,12},{12... | collective-permute-start | bytes 1179656 | tf_op jit(solution)/shard_map/ppermute | solution.py:630
  99.1 19.1 %collective-permute-start.2 = (bf16[256,768]{1,0:T(8,128)(2,1)}, bf16[256,768]{1,0:T(8,128)(2,1)}, u32[]{:S(2)}, u32[]{:S(2)}) collective-permute-start(bf16[256,768]{1,0:T(8,128)(2,1)} %get-tuple-element.24), channel_id=1, source_target_pairs={{0,4},{2,6},{4,0},{6,2},{1,5},{3,7},{5,1},{7,3},{8,12},{10,14},{12... | collective-permute-start | bytes 1179656 | tf_op jit(solution)/shard_map/ppermute | solution.py:630
  101.8 16.8 %collective-permute-start.3 = (bf16[256,768]{1,0:T(8,128)(2,1)}, bf16[256,768]{1,0:T(8,128)(2,1)}, u32[]{:S(2)}, u32[]{:S(2)}) collective-permute-start(bf16[256,768]{1,0:T(8,128)(2,1)} %get-tuple-element.25), channel_id=1, source_target_pairs={{0,6},{2,0},{4,2},{6,4},{1,7},{3,1},{5,3},{7,5},{8,14},{10,8},{12,... | collective-permute-start | bytes 1179656 | tf_op jit(solution)/shard_map/ppermute | solution.py:630
  102.8 24.1 %copy-start.12 = (f32[4,52,128]{2,1,0:T(8,128)}, f32[4,52,128]{2,1,0:T(8,128)S(1)}, u32[]{:S(2)}) copy-start(f32[4,52,128]{2,1,0:T(8,128)S(1)} %pad_maximum_fusion.1) | copy-start | bytes 319492
  118.6 2.2 copy-start.9
  137.5 13.0 %copy-start.4 = (bf16[1024,128]{1,0:T(8,128)(2,1)}, bf16[1024,128]{1,0:T(8,128)(2,1)S(1)}, u32[]{:S(2)}) copy-start(bf16[1024,128]{1,0:T(8,128)(2,1)S(1)} %get-tuple-element.33.q_ref) | copy-start | bytes 786436
  137.6 24.0 %all-to-all-start.2 = ((bf16[16,64,128]{2,1,0:T(8,128)(2,1)}), bf16[16,64,128]{2,1,0:T(8,128)(2,1)S(1)}, u32[]{:S(2)}, u32[]{:S(2)}) async-start(bf16[16,64,128]{2,1,0:T(8,128)(2,1)} %get-tuple-element.31), calls=%async_computation.2 | async-start | bytes 524288 | tf_op jit(solution)/shard_map/all_to_all | solution.py:618
  155.7 0.7 copy-start.6
  156.4 52.4 %copy-start.1 = (bf16[2048,512]{1,0:T(8,128)(2,1)S(1)}, bf16[2048,512]{1,0:T(8,128)(2,1)}, u32[]{:S(2)}) copy-start(bf16[2048,512]{1,0:T(8,128)(2,1)} %fox_w_ref.3) | copy-start | bytes 6291460
  161.6 1.0 copy-start.7
  165.3 27.5 %all-to-all-start.3 = ((bf16[16,96,128]{2,1,0:T(8,128)(2,1)}), bf16[16,96,128]{2,1,0:T(8,128)(2,1)S(1)}, u32[]{:S(2)}, u32[]{:S(2)}) async-start(bf16[16,96,128]{2,1,0:T(8,128)(2,1)} %states_ahead.1), calls=%async_computation.3 | async-start | bytes 786432 | tf_op jit(solution)/shard_map/all_to_all | solution.py:618
  192.9 1.0 copy-start.5
  194.5 0.8 copy-start.3
  195.3 13.6 %all-to-all-start.4 = ((bf16[4,256,256]{2,1,0:T(8,128)(2,1)}), bf16[4,256,256]{2,1,0:T(8,128)(2,1)S(1)}, u32[]{:S(2)}, u32[]{:S(2)}) async-start(bf16[4,256,256]{2,1,0:T(8,128)(2,1)} %copy-done.3), calls=%async_computation.4 | async-start | bytes 1048576 | tf_op jit(solution)/shard_map/all_to_all | solution.py:618
  208.9 1.6 copy-start.2
  212.7 10.3 %collective-permute-start.7 = (bf16[128,2048]{1,0:T(8,128)(2,1)S(1)}, bf16[128,2048]{1,0:T(8,128)(2,1)S(1)}, u32[]{:S(2)}, u32[]{:S(2)}) collective-permute-start(bf16[128,2048]{1,0:T(8,128)(2,1)S(1)} %closing.3), channel_id=1, source_target_pairs={{0,1},{1,0},{2,3},{3,2},{4,5},{5,4},{6,7},{7,6},{8,9},{9,8},{10,11... | collective-permute-start | bytes 1572872 | tf_op jit(solution)/shard_map/ppermute | solution.py:739

commit v6 on v5

--- a/solution.py
+++ b/solution.py
@@ -86,7 +86,7 @@
     whole = pl.BlockSpec(memory_space=pltpu.VMEM)
     return pl.pallas_call(
         attention_kernel,
-        out_shape=jax.ShapeDtypeStruct((count, HEAD_CHANNELS, width), BF16),
+        out_shape=pltpu.HBM((count, HEAD_CHANNELS, width), BF16),
         in_specs=[whole, whole],
         out_specs=whole,
         scratch_shapes=[
@@ -258,7 +258,7 @@
         maps_kernel,
         grid=(seqs // group,),
         out_shape=(
-            jax.ShapeDtypeStruct((rows, lanes), BF16),
+            pltpu.HBM((rows, lanes), BF16),
             jax.ShapeDtypeStruct((rows, lanes), F32),
             jax.ShapeDtypeStruct((seqs * heads, HEAD_CHANNELS, lanes), BF16),
         ),
@@ -317,26 +317,24 @@
 def pack_kernel(groups, *refs):
     *piece_refs, out_ref, sems = refs
     leading, weights = piece_refs[:-3], piece_refs[-3:]
-    rows = out_ref.shape[1]
+    _, _, rows, wide = out_ref.shape
     lanes = weights[0].shape[1] // groups
     copies = []
 
-    def send(source, group, at, width):
-        copies.append(
-            pltpu.make_async_copy(
-                source, out_ref.at[group, :, at : at + width], sems.at[len(copies)]
-            )
-        )
+    def send(source, group, at):
+        block, start = at // wide, at % wide
+        target = out_ref.at[group, block, :, start : start + source.shape[1]]
+        copies.append(pltpu.make_async_copy(source, target, sems.at[len(copies)]))
 
     for g in range(groups):
         at = 0
         for ref in leading:
-            send(ref, g, at, ref.shape[1])
-            at += ref.shape[1]
+            for start in range(0, ref.shape[1], wide):
+                send(ref.at[:, start : start + wide], g, at)
+                at += wide
         for k in range(2):
             for ref in weights:
-                block = ref.at[k * rows : (k + 1) * rows, g * lanes : (g + 1) * lanes]
-                send(block, g, at, lanes)
+                send(ref.at[k * rows : (k + 1) * rows, g * lanes : (g + 1) * lanes], g, at)
                 at += lanes
     for copy in copies:
         copy.start()
@@ -346,17 +344,18 @@
 
 def packed(leading, weights, groups):
     rows, cols = weights[0].shape
-    width = sum(x.shape[1] for x in leading) + 6 * cols // groups
+    wide = 2 * cols // groups
+    blocks = sum(x.shape[1] for x in leading) // wide + 3
     whole = pl.BlockSpec(memory_space=pltpu.VMEM)
     return pl.pallas_call(
         functools.partial(pack_kernel, groups),
-        out_shape=jax.ShapeDtypeStruct((groups, rows // 2, width), BF16),
+        out_shape=jax.ShapeDtypeStruct((groups, blocks, rows // 2, wide), BF16),
         in_specs=[whole] * (len(leading) + 3),
         out_specs=pl.BlockSpec(memory_space=pl.ANY),
-        scratch_shapes=[pltpu.SemaphoreType.DMA((groups * (len(leading) + 6),))],
+        scratch_shapes=[pltpu.SemaphoreType.DMA((groups * (blocks + 3),))],
         compiler_params=pltpu.CompilerParams(vmem_limit_bytes=VMEM_BYTES),
         cost_estimate=pl.CostEstimate(
-            flops=1 << 20, bytes_accessed=4 * groups * rows * width, transcendentals=0
+            flops=1 << 20, bytes_accessed=2 * groups * blocks * rows * wide, transcendentals=0
         ),
         name="packed",
     )(*leading, *weights)
@@ -376,7 +375,7 @@
 ):
     n = HEAD_CHANNELS
     groups = first_ref.shape[0]
-    _, rows, width = other_ref.shape
+    _, blocks, rows, wide = other_ref.shape
     pairs, _, tok_count = fox_ref.shape
     heads = pairs * tok_count // rows
     lanes = heads * n
@@ -387,17 +386,17 @@
             source = lax.rem(i + at_ref[0] * (groups // 2), groups)
             upper = slice(2 * i * rows, (2 * i + 1) * rows)
             lower = slice((2 * i + 1) * rows, (2 * i + 2) * rows)
-            weight_scr[upper, : 2 * lanes] = first_ref[source]
-            weight_scr[upper, 2 * lanes :] = second_ref[source, :, :lanes]
-            weight_scr[lower, :lanes] = second_ref[source, :, lanes:]
-            weight_scr[lower, lanes:] = third_ref[source]
-
-    pieces = [mine_ref[0].astype(F32), other_ref[0].astype(F32)]
+            weight_scr[upper, : 2 * lanes] = first_ref[source, 0]
+            weight_scr[upper, 2 * lanes :] = second_ref[source, 0, :, :lanes]
+            weight_scr[lower, :lanes] = second_ref[source, 0, :, lanes:]
+            weight_scr[lower, lanes:] = third_ref[source, 0]
+
+    pieces = [ref[0, i].astype(F32) for ref in (mine_ref, other_ref) for i in range(blocks)]
     square = sum(jnp.sum(x * x, axis=1, keepdims=True) for x in pieces)
-    scaling = lax.rsqrt(square / (2 * width) + 1e-06)
+    scaling = lax.rsqrt(square / (2 * blocks * wide) + 1e-06)
     normed = jnp.concatenate(
         [
-            (x * scaling * gain_ref[:, i * width : (i + 1) * width].astype(F32)).astype(BF16)
+            (x * scaling * gain_ref[:, i * wide : (i + 1) * wide].astype(F32)).astype(BF16)
             for i, x in enumerate(pieces)
         ],
         1,
@@ -413,8 +412,8 @@
 
 
 def fox_projections(at, mine, other, gain, tok_count):
-    groups, rows, width = other.shape
-    lanes = (mine.shape[2] - width) // 6
+    groups, blocks, rows, wide = other.shape
+    width, lanes = blocks * wide, wide // 2
     heads = lanes // HEAD_CHANNELS
     pairs = rows // tok_count * heads
     whole = pl.BlockSpec(memory_space=pltpu.VMEM)
@@ -423,15 +422,15 @@
         grid=(groups,),
         out_shape=(
             jax.ShapeDtypeStruct((groups * pairs, 3 * HEAD_CHANNELS, tok_count), BF16),
-            jax.ShapeDtypeStruct((groups * rows, 2 * width), BF16),
+            pltpu.HBM((groups * rows, 2 * width), BF16),
         ),
         in_specs=[
             pl.BlockSpec(memory_space=pltpu.SMEM),
-            pl.BlockSpec((1, rows, width), lambda g: (g, 0, 0)),
-            pl.BlockSpec((1, rows, width), lambda g: (g, 0, 0)),
+            pl.BlockSpec((1, blocks, rows, wide), lambda g: (g, 0, 0, 0)),
+            pl.BlockSpec((1, blocks, rows, wide), lambda g: (g, 0, 0, 0)),
             *(
-                pl.BlockSpec((groups, rows, 2 * lanes), lambda g, at=at: (0, 0, at))
-                for at in range(width // (2 * lanes), width // (2 * lanes) + 3)
+                pl.BlockSpec((groups, 1, rows, wide), lambda g, at=at: (0, at, 0, 0))
+                for at in range(blocks, blocks + 3)
             ),
             whole,
         ],
@@ -453,17 +452,20 @@
 def lin_kernel(at_ref, normed_ref, low_ref, decay_up_ref, rate_up_ref, base_ref, *rest):
     sent_refs, (lin_ref, log_ref, rate_ref, weight_scr) = rest[:-4], rest[-4:]
     groups = len(sent_refs)
-    rows, both = sent_refs[0].shape
-    lanes = both // 6
+    _, rows, wide = sent_refs[0].shape
+    lanes = wide // 2
 
     @pl.when(pl.program_id(0) == 0)
     def _():
         for d, ref in enumerate(sent_refs):
             source = lax.rem(at_ref[1] + (groups - d), groups)
             place = lax.rem(source + at_ref[0] * (groups // 2), groups)
-            for k in range(2):
-                start = pl.multiple_of((2 * place + k) * rows, rows)
-                weight_scr[pl.ds(start, rows), :] = ref[:, 3 * k * lanes : 3 * (k + 1) * lanes]
+            upper = pl.ds(pl.multiple_of(2 * place * rows, rows), rows)
+            lower = pl.ds(pl.multiple_of((2 * place + 1) * rows, rows), rows)
+            weight_scr[upper, : 2 * lanes] = ref[0]
+            weight_scr[upper, 2 * lanes :] = ref[1, :, :lanes]
+            weight_scr[lower, :lanes] = ref[1, :, lanes:]
+            weight_scr[lower, lanes:] = ref[2]
 
     normed = normed_ref[...]
     lin_ref[...] = lax.dot_general(
@@ -479,7 +481,7 @@
 
 def lin_projections(at, normed, low, decay_up, rate_up, bases, sent):
     rows, width = normed.shape
-    lanes = sent[0].shape[1] // 6
+    lanes = sent[0].shape[2] // 2
     tall = rows // 4
     whole = pl.BlockSpec(memory_space=pltpu.VMEM)
     return pl.pallas_call(
@@ -557,7 +559,7 @@
     whole = pl.BlockSpec(memory_space=pltpu.VMEM)
     return pl.pallas_call(
         heads_kernel,
-        out_shape=jax.ShapeDtypeStruct((groups, rows // groups, 2 * lanes), BF16),
+        out_shape=pltpu.HBM((groups, rows // groups, 2 * lanes), BF16),
         in_specs=[whole] * 4,
         out_specs=whole,
         compiler_params=pltpu.CompilerParams(vmem_limit_bytes=16 * MIB),
@@ -713,7 +715,7 @@
         return jnp.where(side == 0, table, jnp.roll(table, half_width, axis))
 
     swap = [(i, tp - 1 - i) for i in range(tp)]
-    other = lax.ppermute(mine[:, :, :half_width], "tp", swap)
+    other = lax.ppermute(mine[:, : half_width // (2 * lanes)], "tp", swap)
     fox, normed = fox_projections(
         at, mine, other, own_first(input_norm_gain.reshape(1, -1), 1), tok_count
     )

time: 225 us -> 223 us (level)
  local copies, waits for them, and re-layouts: 19 us -> 14.2 us
    unnamed x35 -> x25, local copies, waits for them, and re-layouts: 9.28 us -> 5.82 us
where the time goes in v6:
time: 223 us; the launch traced here: 222 us
  starting transfers between devices  92.5 us (41%)
  waiting for transfers between devices  69.1 us (31%)
  Pallas kernels  44.8 us (20%)
  local copies, waits for them, and re-layouts  14.2 us (6%)
    all_to_all x5, starting transfers between devices, exchange(): return lax.all_to_all(x, axis, 0, 0, tiled=True)  56.4 us
    all_to_all x5, waiting for transfers between devices, exchange(): return lax.all_to_all(x, axis, 0, 0, tiled=True)  49.7 us
    ppermute x1, starting transfers between devices, per_device(): other = lax.ppermute(mine[:, :half_width // (2 * lanes)], 'tp', swap)  20.7 us
    ppermute x6, waiting for transfers between devices, by_permutes(): lax.ppermute(block, axis, [(i, (i + d) % size) for i in range(size)])  15.8 us
    pallas_call x1, Pallas kernels, position_maps(): pl.pallas_call(maps_kernel, grid=(seqs // group,), out_shape=(pltpu.HBM((...  10.7 us
    ppermute x1, starting transfers between devices, per_device(): theirs = lax.ppermute(theirs, 'tp', swap)  8.15 us
    ppermute x6, starting transfers between devices, by_permutes(): lax.ppermute(block, axis, [(i, (i + d) % size) for i in range(size)])  7.25 us
    pallas_call x1, Pallas kernels, fox_projections(): pl.pallas_call(fox_kernel, grid=(groups,), out_shape=(jax.ShapeDtypeStruc...  6.84 us
  transfers between devices with their start and end apart: 13, of which 8 were waited for; matrix products, arithmetic and copies ran while one was open for 3% of the time, Pallas kernels for 12%

profile of v6, /device:TPU:33, one launch (start us, length us, event | category | flops | bytes accessed | tf_op | source)
XLA Modules:
  0.0 222.3 jit_solution(5303571874343494675)
XLA Ops:
  0.0 3.8 %packed.2 = bf16[4,7,256,256]{3,2,1,0:T(8,128)(2,1)} custom-call(bf16[256,1024]{1,0:T(8,128)(2,1)} %bitcast.62, bf16[512,512]{1,0:T(8,128)(2,1)} %refs_1_.2, bf16[512,512]{1,0:T(8,128)(2,1)} %refs_2_.2, bf16[512,512]{1,0:T(8,128)(2,1)} %refs_3_.1), custom_call_target="tpu_custom_call" | custom-call | flops 1048576 | bytes 7340032 | tf_op jit(solution)/shard_map/packed/pallas_call | solution.py:350
  3.8 5.1 %all-to-all-start = ((bf16[4,7,256,256]{3,2,1,0:T(8,128)(2,1)}), bf16[4,7,256,256]{3,2,1,0:T(8,128)(2,1)}, u32[]{:S(2)}, u32[]{:S(2)}) async-start(bf16[4,7,256,256]{3,2,1,0:T(8,128)(2,1)} %packed.2), calls=%async_computation | async-start | bytes 7340032 | tf_op jit(solution)/shard_map/all_to_all | solution.py:620
  8.9 2.8 %packed.3 = bf16[4,3,256,256]{3,2,1,0:T(8,128)(2,1)} custom-call(bf16[512,512]{1,0:T(8,128)(2,1)} %refs_0_.1, bf16[512,512]{1,0:T(8,128)(2,1)} %refs_1_.3, bf16[512,512]{1,0:T(8,128)(2,1)} %refs_2_.3), custom_call_target="tpu_custom_call" | custom-call | flops 1048576 | bytes 3145728 | tf_op jit(solution)/shard_map/packed/pallas_call | solution.py:350
  11.7 2.4 %dynamic-slice_bitcast_fusion = (bf16[3,256,256]{2,1,0:T(8,128)(2,1)}, bf16[3,256,256]{2,1,0:T(8,128)(2,1)}, bf16[3,256,256]{2,1,0:T(8,128)(2,1)}, bf16[3,256,256]{2,1,0:T(8,128)(2,1)S(1)}) fusion(bf16[4,3,256,256]{3,2,1,0:T(8,128)(2,1)} %packed.3, s32[]{:T(128)S(6)} %select_n.75, s32[]{:T(128)S(6)} %select_n.74, s32[]{:T(128)S(6)} %select_n.73, s32[]{:T(128)S(6)} %select_n.72), kind=kLoop, calls=%fused_computation.3 | loop fusion | bytes 3145744 | tf_op jit(solution)/shard_map/jit(dynamic_index_in_dim)/squeeze | solution.py:626
  14.1 19.2 %all-to-all-done.mine_ref.first_ref.second_ref.third_ref = bf16[4,7,256,256]{3,2,1,0:T(8,128)(2,1)} async-done(((bf16[4,7,256,256]{3,2,1,0:T(8,128)(2,1)}), bf16[4,7,256,256]{3,2,1,0:T(8,128)(2,1)}, u32[]{:S(2)}, u32[]{:S(2)}) %all-to-all-start) | async-done | bytes 3670048 | tf_op jit(solution)/shard_map/all_to_all | solution.py:620
  33.3 3.2 %slice.61 = bf16[4,4,256,256]{3,2,1,0:T(8,128)(2,1)} slice(bf16[4,7,256,256]{3,2,1,0:T(8,128)(2,1)} %all-to-all-done.mine_ref.first_ref.second_ref.third_ref), slice={[0:4], [0:4], [0:256], [0:256]} | slice | bytes 4194304 | tf_op jit(solution)/shard_map/slice | solution.py:718
  36.5 20.7 %collective-permute-start = (bf16[4,4,256,256]{3,2,1,0:T(8,128)(2,1)}, bf16[4,4,256,256]{3,2,1,0:T(8,128)(2,1)S(1)}, u32[]{:S(2)}, u32[]{:S(2)}) collective-permute-start(bf16[4,4,256,256]{3,2,1,0:T(8,128)(2,1)} %slice.61), channel_id=1, source_target_pairs={{0,1},{1,0},{2,3},{3,2},{4,5},{5,4},{6,7},{7,6},{8,9},{9,8},{10,11... | collective-permute-start | bytes 6291464 | tf_op jit(solution)/shard_map/ppermute | solution.py:718
  57.5 3.6 %collective-permute-done.other_ref = bf16[4,4,256,256]{3,2,1,0:T(8,128)(2,1)S(1)} collective-permute-done((bf16[4,4,256,256]{3,2,1,0:T(8,128)(2,1)}, bf16[4,4,256,256]{3,2,1,0:T(8,128)(2,1)S(1)}, u32[]{:S(2)}, u32[]{:S(2)}) %collective-permute-start) | collective-permute-done | bytes 2097184 | tf_op jit(solution)/shard_map/ppermute | solution.py:718
  61.1 6.8 %fox_projections.1 = (bf16[16,192,128]{2,1,0:T(8,128)(2,1)}, bf16[1024,2048]{1,0:T(8,128)(2,1)}) custom-call(s32[2]{0:T(128)S(1)} %pad_add_fusion.at_ref, bf16[4,7,256,256]{3,2,1,0:T(8,128)(2,1)} %all-to-all-done.mine_ref.first_ref.second_ref.third_ref, bf16[4,4,256,256]{3,2,1,0:T(8,128)(2,1)S(1)} %collective-permute-done.other_ref, ...), custom_call_target="tpu_custom_call" | custom-call | flops 1610612736 | bytes 8388608 | tf_op jit(solution)/shard_map/fox_projections/pallas_call | solution.py:420
  68.0 23.5 %all-to-all-start.1 = ((bf16[16,192,128]{2,1,0:T(8,128)(2,1)}), bf16[16,192,128]{2,1,0:T(8,128)(2,1)S(1)}, u32[]{:S(2)}, u32[]{:S(2)}) async-start(bf16[16,192,128]{2,1,0:T(8,128)(2,1)} %get-tuple-element.30), calls=%async_computation.1 | async-start | bytes 1572864 | tf_op jit(solution)/shard_map/all_to_all | solution.py:620
  92.7 1.4 collective-permute-start.5
  96.2 1.2 collective-permute-start.1
  97.5 2.6 %collective-permute-start.2 = (bf16[3,256,256]{2,1,0:T(8,128)(2,1)}, bf16[3,256,256]{2,1,0:T(8,128)(2,1)}, u32[]{:S(2)}, u32[]{:S(2)}) collective-permute-start(bf16[3,256,256]{2,1,0:T(8,128)(2,1)} %get-tuple-element.24), channel_id=1, source_target_pairs={{0,4},{2,6},{4,0},{6,2},{1,5},{3,7},{5,1},{7,3},{8,12},{10,14},{12... | collective-permute-start | bytes 1179656 | tf_op jit(solution)/shard_map/ppermute | solution.py:632
  100.1 1.0 collective-permute-start.3
  101.2 5.9 %collective-permute-done.1.rest_1_ = bf16[3,256,256]{2,1,0:T(8,128)(2,1)S(1)} collective-permute-done((bf16[3,256,256]{2,1,0:T(8,128)(2,1)}, bf16[3,256,256]{2,1,0:T(8,128)(2,1)S(1)}, u32[]{:S(2)}, u32[]{:S(2)}) %collective-permute-start.1) | collective-permute-done | bytes 393248 | tf_op jit(solution)/shard_map/ppermute | solution.py:632
  107.2 9.4 %collective-permute-done.2.rest_2_ = bf16[3,256,256]{2,1,0:T(8,128)(2,1)} collective-permute-done((bf16[3,256,256]{2,1,0:T(8,128)(2,1)}, bf16[3,256,256]{2,1,0:T(8,128)(2,1)}, u32[]{:S(2)}, u32[]{:S(2)}) %collective-permute-start.2) | collective-permute-done | bytes 393248 | tf_op jit(solution)/shard_map/ppermute | solution.py:632
  117.0 2.2 copy-done.5
  119.2 6.1 %lin_projections.1 = (bf16[1024,384]{1,0:T(8,128)(2,1)S(1)}, f32[1024,128]{1,0:T(8,128)S(1)}, f32[1024,128]{1,0:T(8,128)S(1)}) custom-call(s32[2]{0:T(128)S(1)} %pad_add_fusion.at_ref, bf16[1024,2048]{1,0:T(8,128)(2,1)S(1)} %copy-done.5, bf16[2048,256]{1,0:T(8,128)(2,1)S(1)} %maximum_select_fusion.low_ref, ...), custom_call_target="tpu_custom_call" | custom-call | flops 2684354560 | bytes 4194304 | tf_op jit(solution)/shard_map/lin_projections/pallas_call | solution.py:487
  125.2 10.7 %position_maps.1 = (bf16[1024,128]{1,0:T(8,128)(2,1)}, f32[1024,128]{1,0:T(8,128)S(1)}, bf16[16,64,128]{2,1,0:T(8,128)(2,1)}) custom-call(bf16[1024,384]{1,0:T(8,128)(2,1)S(1)} %get-tuple-element.26.proj_ref, f32[1024,128]{1,0:T(8,128)S(1)} %get-tuple-element.27.log_ref, f32[1024,128]{1,0:T(8,128)S(1)} %get-tuple-element.28.rate_ref, f32[8,2,128]{2,1,0:T(2,128)S(1)} %bitcast.60), custom_call_target="tpu_custom_call" | custom-call | flops 1342177280 | bytes 2621440 | tf_op jit(solution)/shard_map/position_maps/pallas_call | solution.py:257
  136.0 11.5 %all-to-all-start.2 = ((bf16[16,64,128]{2,1,0:T(8,128)(2,1)}), bf16[16,64,128]{2,1,0:T(8,128)(2,1)S(1)}, u32[]{:S(2)}, u32[]{:S(2)}) async-start(bf16[16,64,128]{2,1,0:T(8,128)(2,1)} %get-tuple-element.31), calls=%async_computation.2 | async-start | bytes 524288 | tf_op jit(solution)/shard_map/all_to_all | solution.py:620
  147.5 5.9 %attention.1.fox_ref = bf16[16,64,128]{2,1,0:T(8,128)(2,1)} custom-call(bf16[16,192,128]{2,1,0:T(8,128)(2,1)S(1)} %all-to-all-done.1.blocks_ref, f32[16,128]{1,0:T(8,128)S(1)} %dynamic-slice_bitcast_fusion.9.gate_ref), custom_call_target="tpu_custom_call" | custom-call | flops 1073741824 | bytes 1572864 | tf_op jit(solution)/shard_map/attention/pallas_call | solution.py:87
  153.4 6.5 %all-to-all-done.2.maps_ref = bf16[16,64,128]{2,1,0:T(8,128)(2,1)S(1)} async-done(((bf16[16,64,128]{2,1,0:T(8,128)(2,1)}), bf16[16,64,128]{2,1,0:T(8,128)(2,1)S(1)}, u32[]{:S(2)}, u32[]{:S(2)}) %all-to-all-start.2) | async-done | bytes 262176 | tf_op jit(solution)/shard_map/all_to_all | solution.py:620
  160.9 2.8 %states_ahead.1 = bf16[16,96,128]{2,1,0:T(8,128)(2,1)} custom-call(bf16[16,64,128]{2,1,0:T(8,128)(2,1)S(1)} %all-to-all-done.2.maps_ref, f32[32,128]{1,0:T(8,128)S(1)} %dynamic-slice_bitcast_fusion.8.start_ref, bf16[16,64,128]{2,1,0:T(8,128)(2,1)S(1)} %copy-done.4), custom_call_target="tpu_custom_call" | custom-call | flops 16777216 | bytes 524288 | tf_op jit(solution)/shard_map/states_ahead/pallas_call | solution.py:304
  163.7 10.1 %all-to-all-start.3 = ((bf16[16,96,128]{2,1,0:T(8,128)(2,1)}), bf16[16,96,128]{2,1,0:T(8,128)(2,1)S(1)}, u32[]{:S(2)}, u32[]{:S(2)}) async-start(bf16[16,96,128]{2,1,0:T(8,128)(2,1)} %states_ahead.1), calls=%async_computation.3 | async-start | bytes 786432 | tf_op jit(solution)/shard_map/all_to_all | solution.py:620
  174.5 17.1 %all-to-all-done.3.back_ref = bf16[16,96,128]{2,1,0:T(8,128)(2,1)S(1)} async-done(((bf16[16,96,128]{2,1,0:T(8,128)(2,1)}), bf16[16,96,128]{2,1,0:T(8,128)(2,1)S(1)}, u32[]{:S(2)}, u32[]{:S(2)}) %all-to-all-start.3) | async-done | bytes 393248 | tf_op jit(solution)/shard_map/all_to_all | solution.py:620
  192.6 1.5 heads_out.1
  194.1 6.3 %all-to-all-start.4 = ((bf16[4,256,256]{2,1,0:T(8,128)(2,1)}), bf16[4,256,256]{2,1,0:T(8,128)(2,1)S(1)}, u32[]{:S(2)}, u32[]{:S(2)}) async-start(bf16[4,256,256]{2,1,0:T(8,128)(2,1)} %heads_out.1), calls=%async_computation.4 | async-start | bytes 1048576 | tf_op jit(solution)/shard_map/all_to_all | solution.py:620
  200.3 6.9 %all-to-all-done.4.acts_ref = bf16[4,256,256]{2,1,0:T(8,128)(2,1)S(1)} async-done(((bf16[4,256,256]{2,1,0:T(8,128)(2,1)}), bf16[4,256,256]{2,1,0:T(8,128)(2,1)S(1)}, u32[]{:S(2)}, u32[]{:S(2)}) %all-to-all-start.4) | async-done | bytes 524320 | tf_op jit(solution)/shard_map/all_to_all | solution.py:620
  207.3 1.6 copy-done.2
  208.8 2.2 closing.3
  211.0 8.1 %collective-permute-start.7 = (bf16[128,2048]{1,0:T(8,128)(2,1)S(1)}, bf16[128,2048]{1,0:T(8,128)(2,1)S(1)}, u32[]{:S(2)}, u32[]{:S(2)}) collective-permute-start(bf16[128,2048]{1,0:T(8,128)(2,1)S(1)} %closing.3), channel_id=1, source_target_pairs={{0,1},{1,0},{2,3},{3,2},{4,5},{5,4},{6,7},{7,6},{8,9},{9,8},{10,11... | collective-permute-start | bytes 1572872 | tf_op jit(solution)/shard_map/ppermute | solution.py:741
  219.2 2.2 closing.2
  (58 shorter events, 7.6 us)
Async XLA Ops:
  0.0 91.5 %copy-start = (f32[2,8,64,64]{3,2,1,0:T(8,128)S(1)}, f32[2,8,64,64]{3,2,1,0:T(8,128)}, u32[]{:S(2)}) copy-start(f32[2,8,64,64]{3,2,1,0:T(8,128)} %param.37) | copy-start | bytes 786436
  3.8 29.5 %all-to-all-start = ((bf16[4,7,256,256]{3,2,1,0:T(8,128)(2,1)}), bf16[4,7,256,256]{3,2,1,0:T(8,128)(2,1)}, u32[]{:S(2)}, u32[]{:S(2)}) async-start(bf16[4,7,256,256]{3,2,1,0:T(8,128)(2,1)} %packed.2), calls=%async_computation | async-start | bytes 7340032 | tf_op jit(solution)/shard_map/all_to_all | solution.py:620
  33.3 23.9 %copy-start.9 = (bf16[2048]{0:T(1024)(128)(2,1)S(1)}, bf16[2048]{0:T(1024)(128)(2,1)}, u32[]{:S(2)}) copy-start(bf16[2048]{0:T(1024)(128)(2,1)} %param.21) | copy-start | bytes 12292
  33.3 24.0 %copy-start.10 = (f32[2,128,8]{1,2,0:T(8,128)S(1)}, f32[2,128,8]{1,2,0:T(8,128)}, u32[]{:S(2)}) copy-start(f32[2,128,8]{1,2,0:T(8,128)} %param.32) | copy-start | bytes 24580
  33.3 24.0 %copy-start.8 = (f32[2,2048,8]{1,2,0:T(8,128)S(1)}, f32[2,2048,8]{1,2,0:T(8,128)}, u32[]{:S(2)}) copy-start(f32[2,2048,8]{1,2,0:T(8,128)} %param.25) | copy-start | bytes 393220
  36.5 24.7 %collective-permute-start = (bf16[4,4,256,256]{3,2,1,0:T(8,128)(2,1)}, bf16[4,4,256,256]{3,2,1,0:T(8,128)(2,1)S(1)}, u32[]{:S(2)}, u32[]{:S(2)}) collective-permute-start(bf16[4,4,256,256]{3,2,1,0:T(8,128)(2,1)} %slice.61), channel_id=1, source_target_pairs={{0,1},{1,0},{2,3},{3,2},{4,5},{5,4},{6,7},{7,6},{8,9},{9,8},{10,11... | collective-permute-start | bytes 6291464 | tf_op jit(solution)/shard_map/ppermute | solution.py:718
  68.0 26.9 %copy-start.6 = (bf16[2048,128]{1,0:T(8,128)(2,1)S(1)}, bf16[2048,128]{1,0:T(8,128)(2,1)}, u32[]{:S(2)}) copy-start(bf16[2048,128]{1,0:T(8,128)(2,1)} %param.29) | copy-start | bytes 1572868
  68.0 27.0 %copy-start.7 = (bf16[2048,128]{1,0:T(8,128)(2,1)S(1)}, bf16[2048,128]{1,0:T(8,128)(2,1)}, u32[]{:S(2)}) copy-start(bf16[2048,128]{1,0:T(8,128)(2,1)} %param.33) | copy-start | bytes 1572868
  68.0 68.0 %all-to-all-start.1 = ((bf16[16,192,128]{2,1,0:T(8,128)(2,1)}), bf16[16,192,128]{2,1,0:T(8,128)(2,1)S(1)}, u32[]{:S(2)}, u32[]{:S(2)}) async-start(bf16[16,192,128]{2,1,0:T(8,128)(2,1)} %get-tuple-element.30), calls=%async_computation.1 | async-start | bytes 1572864 | tf_op jit(solution)/shard_map/all_to_all | solution.py:620
  91.7 8.4 %collective-permute-start.6 = (f32[52,128]{1,0:T(8,128)S(1)}, f32[52,128]{1,0:T(8,128)S(1)}, u32[]{:S(2)}, u32[]{:S(2)}) collective-permute-start(f32[52,128]{1,0:T(8,128)S(1)} %get-tuple-element.50), channel_id=1, source_target_pairs={{0,6},{2,0},{4,2},{6,4},{1,7},{3,1},{5,3},{7,5},{8,14},{10,8},{12,... | collective-permute-start | bytes 79880 | tf_op jit(solution)/shard_map/ppermute | solution.py:632
  92.7 8.5 %collective-permute-start.5 = (f32[52,128]{1,0:T(8,128)S(1)}, f32[52,128]{1,0:T(8,128)S(1)}, u32[]{:S(2)}, u32[]{:S(2)}) collective-permute-start(f32[52,128]{1,0:T(8,128)S(1)} %get-tuple-element.51), channel_id=1, source_target_pairs={{0,4},{2,6},{4,0},{6,2},{1,5},{3,7},{5,1},{7,3},{8,12},{10,14},{12... | collective-permute-start | bytes 79880 | tf_op jit(solution)/shard_map/ppermute | solution.py:632
  94.1 7.1 %collective-permute-start.4 = (f32[52,128]{1,0:T(8,128)S(1)}, f32[52,128]{1,0:T(8,128)S(1)}, u32[]{:S(2)}, u32[]{:S(2)}) collective-permute-start(f32[52,128]{1,0:T(8,128)S(1)} %get-tuple-element.52), channel_id=1, source_target_pairs={{0,2},{2,4},{4,6},{6,0},{1,3},{3,5},{5,7},{7,1},{8,10},{10,12},{12... | collective-permute-start | bytes 79880 | tf_op jit(solution)/shard_map/ppermute | solution.py:632
  96.2 10.9 %collective-permute-start.1 = (bf16[3,256,256]{2,1,0:T(8,128)(2,1)}, bf16[3,256,256]{2,1,0:T(8,128)(2,1)S(1)}, u32[]{:S(2)}, u32[]{:S(2)}) collective-permute-start(bf16[3,256,256]{2,1,0:T(8,128)(2,1)} %get-tuple-element.23), channel_id=1, source_target_pairs={{0,2},{2,4},{4,6},{6,0},{1,3},{3,5},{5,7},{7,1},{8,10},{10,12},{12... | collective-permute-start | bytes 1179656 | tf_op jit(solution)/shard_map/ppermute | solution.py:632
  97.5 19.1 %collective-permute-start.2 = (bf16[3,256,256]{2,1,0:T(8,128)(2,1)}, bf16[3,256,256]{2,1,0:T(8,128)(2,1)}, u32[]{:S(2)}, u32[]{:S(2)}) collective-permute-start(bf16[3,256,256]{2,1,0:T(8,128)(2,1)} %get-tuple-element.24), channel_id=1, source_target_pairs={{0,4},{2,6},{4,0},{6,2},{1,5},{3,7},{5,1},{7,3},{8,12},{10,14},{12... | collective-permute-start | bytes 1179656 | tf_op jit(solution)/shard_map/ppermute | solution.py:632
  100.1 16.8 %collective-permute-start.3 = (bf16[3,256,256]{2,1,0:T(8,128)(2,1)}, bf16[3,256,256]{2,1,0:T(8,128)(2,1)}, u32[]{:S(2)}, u32[]{:S(2)}) collective-permute-start(bf16[3,256,256]{2,1,0:T(8,128)(2,1)} %get-tuple-element.25), channel_id=1, source_target_pairs={{0,6},{2,0},{4,2},{6,4},{1,7},{3,1},{5,3},{7,5},{8,14},{10,8},{12,... | collective-permute-start | bytes 1179656 | tf_op jit(solution)/shard_map/ppermute | solution.py:632
  117.0 2.2 copy-start.5
  136.0 24.0 %all-to-all-start.2 = ((bf16[16,64,128]{2,1,0:T(8,128)(2,1)}), bf16[16,64,128]{2,1,0:T(8,128)(2,1)S(1)}, u32[]{:S(2)}, u32[]{:S(2)}) async-start(bf16[16,64,128]{2,1,0:T(8,128)(2,1)} %get-tuple-element.31), calls=%async_computation.2 | async-start | bytes 524288 | tf_op jit(solution)/shard_map/all_to_all | solution.py:620
  153.4 53.8 %copy-start.1 = (bf16[2048,512]{1,0:T(8,128)(2,1)S(1)}, bf16[2048,512]{1,0:T(8,128)(2,1)}, u32[]{:S(2)}) copy-start(bf16[2048,512]{1,0:T(8,128)(2,1)} %fox_w_ref.3) | copy-start | bytes 6291460
  160.0 1.0 copy-start.4
  163.7 27.9 %all-to-all-start.3 = ((bf16[16,96,128]{2,1,0:T(8,128)(2,1)}), bf16[16,96,128]{2,1,0:T(8,128)(2,1)S(1)}, u32[]{:S(2)}, u32[]{:S(2)}) async-start(bf16[16,96,128]{2,1,0:T(8,128)(2,1)} %states_ahead.1), calls=%async_computation.3 | async-start | bytes 786432 | tf_op jit(solution)/shard_map/all_to_all | solution.py:620
  191.6 1.0 copy-start.3
  194.1 13.2 %all-to-all-start.4 = ((bf16[4,256,256]{2,1,0:T(8,128)(2,1)}), bf16[4,256,256]{2,1,0:T(8,128)(2,1)S(1)}, u32[]{:S(2)}, u32[]{:S(2)}) async-start(bf16[4,256,256]{2,1,0:T(8,128)(2,1)} %heads_out.1), calls=%async_computation.4 | async-start | bytes 1048576 | tf_op jit(solution)/shard_map/all_to_all | solution.py:620
  207.3 1.6 copy-start.2
  211.0 10.4 %collective-permute-start.7 = (bf16[128,2048]{1,0:T(8,128)(2,1)S(1)}, bf16[128,2048]{1,0:T(8,128)(2,1)S(1)}, u32[]{:S(2)}, u32[]{:S(2)}) collective-permute-start(bf16[128,2048]{1,0:T(8,128)(2,1)S(1)} %closing.3), channel_id=1, source_target_pairs={{0,1},{1,0},{2,3},{3,2},{4,5},{5,4},{6,7},{7,6},{8,9},{9,8},{10,11... | collective-permute-start | bytes 1572872 | tf_op jit(solution)/shard_map/ppermute | solution.py:741
